TPU v7x, 256 devices: a 2x2x32 block of a 4x8x32 slice. The times are simulated.
256 devices in a mesh: grp: 4 (over y, x), sp: 32 (over z), tp: 2 (over core).
Axes of the slice: x: 2, y: 2, z: 32, core: 2. Of those that a mesh axis runs over, the one named last changes fastest.
The devices are a block of a 4x8x32 slice.
Arguments:
- gate_in: bfloat16 [49152, 2048], P(('grp', 'sp'), 'tp'), parts along dimension 0, may hold values from -6 to 6
- values_in: bfloat16 [49152, 2048], P(('grp', 'sp'), 'tp'), parts along dimension 0, may hold values from -6 to 6
- input_state_in: bfloat16 [49152, 512], P(('grp', 'sp'), 'tp'), parts along dimension 0, may hold values from -6 to 6
- output_state_in: bfloat16 [49152, 512], P(('grp', 'sp'), 'tp'), parts along dimension 0, may hold values from -6 to 6
- step_in: bfloat16 [49152, 32], P(('grp', 'sp'), 'tp'), parts along dimension 0, may hold values from -6 to 6
- conv_x: bfloat16 [4, 2048], P(None, 'tp'), may hold values from -3 to 3
- conv_b: bfloat16 [4, 512], P(None, 'tp'), may hold values from -3 to 3
- conv_c: bfloat16 [4, 512], P(None, 'tp'), may hold values from -3 to 3
- dt_bias: float32 [32], P('tp'), may hold values from -1 to 1
- decay_rate: float32 [32], P('tp'), may hold values from 0 to 1, as said below
- log_decay_extra: float32 [49152, 32], P(('grp', 'sp'), 'tp'), parts along dimension 0, may hold values from -1 to 0
- out_gain: bfloat16 [2048], P('tp'), may hold values from 0.099609375 to 1.8984375
- w_out: bfloat16 [2048, 2048], P('tp'), may hold values from -0.125 to 0.125
Outputs:
- mixed: bfloat16 [49152, 2048], P(('grp', 'sp', 'tp')), parts along dimension 0
There are 4 independent parts, one for each index of `grp`. A program takes and returns all parts, laid end to end along the dimension named above; an argument that names none is the same for every part. Nothing has to cross between parts.
Inputs may be any that keep to these rules, and one draw needn't show every extreme that they name: `decay_rate`: positive rates.
All inputs are finite; a program needn't handle non-finite values.
Results may differ from a plain program's by a relative error of at most 0.01.
Values may be sent and summed in bfloat16 or wider, within the bound.
No kernel may reach another device: no remote copies, remote signals or barrier semaphores. Data moves between devices by JAX's collectives and lax.ppermute only.
A program may use at most 128 MiB of HBM per device.

v0:
```python
import functools

import jax
import jax.numpy as jnp
from jax import lax
from jax.experimental import pallas as pl
from jax.experimental.pallas import tpu as pltpu
from jax.sharding import PartitionSpec as P


HEAD_DIM = 64
STATE = 128
CONV = 4
BLOCK = 128
QUAD = 4
EXTRA = 16
EPS = 1e-05
F32 = jnp.float32
BF16 = jnp.bfloat16
EDGE = 16
FILL = 4_000_000_000
SMALL = 4 * 1024 * 1024
LARGE = 16 * 1024 * 1024


def dot(a, b, dims=((1,), (0,))):
    return lax.dot_general(a, b, (dims, ((), ())), preferred_element_type=F32)


def parts_of(x, count):
    out = []
    for _ in range(count):
        part = x.astype(BF16)
        out.append(part)
        x = x - part.astype(F32)
    return out


def spread_matrix(heads):
    row = lax.broadcasted_iota(jnp.int32, (heads, heads * HEAD_DIM), 0)
    col = lax.broadcasted_iota(jnp.int32, (heads, heads * HEAD_DIM), 1)
    return (row == col // HEAD_DIM).astype(F32).astype(BF16)


def spread(x, matrix, count=2):
    return dot(jnp.concatenate(parts_of(x, count), axis=0), jnp.concatenate([matrix] * count, axis=0), ((0,), (0,)))


def column(row):
    size = row.shape[1]
    same = lax.broadcasted_iota(jnp.int32, (size, size), 0) == lax.broadcasted_iota(jnp.int32, (size, size), 1)
    return jnp.sum(jnp.where(same, row, 0.0), axis=1, keepdims=True)


def softplus(x):
    return jnp.maximum(x, 0.0) + jnp.log1p(jnp.exp(-jnp.abs(x)))


def silu(x):
    return x / (1.0 + jnp.exp(-x))


def convolved(ext, first, rows, taps):
    summed = jnp.zeros((rows, ext.shape[1]), F32)
    for tap in range(CONV):
        summed = summed + taps[tap : tap + 1].astype(F32) * ext[first + tap : first + tap + rows, :]
    return silu(summed).astype(BF16)


def local_kernel(
    values_hbm, b_hbm, c_hbm, step_hbm, extra_hbm, conv_x_hbm, conv_b_hbm, conv_c_hbm, dt_hbm, rate_hbm,
    x_act, b_act, c_act, cum_out, step_out, state_out, logs_out, edge_weight,
    ext, values, b_in, c_in, step_in, extra, conv_x, conv_b, conv_c, dt_bias, rate, sems,
):
    sources = (step_hbm, extra_hbm, dt_hbm, rate_hbm, b_hbm, conv_b_hbm, c_hbm, conv_c_hbm, values_hbm, conv_x_hbm)
    targets = (step_in, extra, dt_bias, rate, b_in, conv_b, c_in, conv_c, values, conv_x)
    copies = [pltpu.make_async_copy(source, target, sems.at[turn]) for turn, (source, target) in enumerate(zip(sources, targets, strict=True))]
    for copy in copies:
        copy.start()
    for copy in copies[:4]:
        copy.wait()
    span, inner = values.shape
    heads = step_in.shape[0]
    step = softplus(step_in[...].astype(F32) + column(dt_bias[...]))
    log_step = extra[...] - step * column(rate[...])
    step_out[...] = step
    row = lax.broadcasted_iota(jnp.int32, (BLOCK, BLOCK), 0)
    upper = (row <= lax.broadcasted_iota(jnp.int32, (BLOCK, BLOCK), 1)).astype(F32).astype(BF16)
    total = jnp.zeros((heads, 1), F32)
    for start in range(0, span, BLOCK):
        summed = dot(jnp.concatenate(parts_of(log_step[:, start : start + BLOCK], 3), axis=0), upper)
        cum = summed[:heads] + summed[heads : 2 * heads] + summed[2 * heads :] + total
        cum_out[:, start : start + BLOCK] = cum
        total = cum[:, BLOCK - 1 :]
    matrix = spread_matrix(heads)
    weight = jnp.exp(total - cum_out[...]) * step
    edge_weight[...] = spread(weight[:, 0:BLOCK], matrix)[0:EDGE]
    lane = lax.broadcasted_iota(jnp.int32, (heads, BLOCK), 1)
    high, middle, low = (part.astype(F32) for part in parts_of(total, 3))
    logs = jnp.where(lane == 0, high, jnp.where(lane == 1, middle, jnp.where(lane == 2, low, 0.0)))
    logs_out[...] = dot(logs.astype(BF16), matrix, ((0,), (0,)))[0:EXTRA].astype(BF16)
    weight = jnp.where(lax.broadcasted_iota(jnp.int32, (heads, span), 1) < EDGE, 0.0, weight)
    width = ext.shape[1]
    ext[0:8, :] = jnp.zeros((8, width), F32)
    per_group = inner // (b_in.shape[1] // STATE)
    for turn, (source, taps, target) in enumerate(((b_in, conv_b, b_act), (c_in, conv_c, c_act), (values, conv_x, x_act))):
        for copy in copies[4 + 2 * turn : 6 + 2 * turn]:
            copy.wait()
        for start in range(0, source.shape[1], width):
            lanes = slice(start, start + width)
            ext[8 : 8 + span, :] = source[:, lanes].astype(F32)
            active = convolved(ext, 8 - (CONV - 1), span, taps[:, lanes])
            target[:, lanes] = active
            if source is values:
                group = start // per_group
                weighted = (active.astype(F32) * spread(weight, matrix[:, lanes])).astype(BF16)
                state_out[:, lanes] = dot(b_act[:, group * STATE : (group + 1) * STATE], weighted, ((0,), (0,)))


def edge_kernel(
    values, b_in, c_in, halo, conv_x, conv_b, conv_c, state_in, logs_in, edge_weight,
    edge_x, edge_b, edge_c, slot0, slot1, slot2, slot3, ext, packed,
):
    inner, shared = values.shape[1], b_in.shape[1]
    offset = 0
    for source, taps, target in ((b_in, conv_b, edge_b), (c_in, conv_c, edge_c), (values, conv_x, edge_x)):
        lanes = slice(offset, offset + source.shape[1])
        part = ext.at[:, lanes]
        part[0:EDGE, :] = halo[:, lanes].astype(F32)
        part[EDGE : 2 * EDGE, :] = source[...].astype(F32)
        target[...] = convolved(part, EDGE - (CONV - 1), EDGE, taps[...])
        offset += source.shape[1]
    groups = shared // STATE
    weighted = (edge_x[...].astype(F32) * edge_weight[...]).astype(BF16)
    for group in range(groups):
        lanes = slice(group * (inner // groups), (group + 1) * (inner // groups))
        added = dot(edge_b[:, group * STATE : (group + 1) * STATE], weighted[:, lanes], ((0,), (0,)))
        packed[0:STATE, lanes] = (state_in[:, lanes] + added).astype(BF16)
    packed[STATE:, :] = logs_in[...]
    me = lax.rem(lax.axis_index("sp"), QUAD)
    quarter = inner // QUAD
    for bits, slot in enumerate((slot0, slot1, slot2, slot3)):
        slot[...] = packed[:, pl.ds(pl.multiple_of((me ^ bits) * quarter, 128), quarter)]


def whole(count):
    return [pl.BlockSpec(memory_space=pltpu.VMEM)] * count


def local_call(kernel, outs, args, scratch=(), flops=0, limit=None):
    many = isinstance(outs, (list, tuple))
    size = sum(a.size * a.dtype.itemsize for a in args)
    return pl.pallas_call(
        kernel,
        out_shape=outs,
        in_specs=whole(len(args)),
        out_specs=whole(len(outs)) if many else whole(1)[0],
        scratch_shapes=list(scratch),
        compiler_params=pltpu.CompilerParams(vmem_limit_bytes=limit or LARGE),
        cost_estimate=pl.CostEstimate(flops=flops, bytes_accessed=size, transcendentals=0),
    )(*args)


def load(ref):
    logs = ref[STATE:, :].astype(F32)
    return ref[0:STATE, :].astype(F32), logs[0:1] + logs[1:2] + logs[2:3]


def quad_order(ordered, refs):
    me = lax.rem(lax.axis_index("sp"), QUAD)
    for bits, ref in enumerate(refs):
        ordered[me ^ bits] = ref[...]


def store(ref, state, log):
    ref[0:STATE, :] = state.astype(BF16)
    high, middle, low = (part.astype(F32) for part in parts_of(log, 3))
    row = lax.broadcasted_iota(jnp.int32, (EXTRA, log.shape[1]), 0)
    logs = jnp.where(row == 0, high, jnp.where(row == 1, middle, jnp.where(row == 2, low, 0.0)))
    ref[STATE:, :] = logs.astype(BF16)


def quad_total_kernel(own, r1, r2, r3, sent, state_out, log_out, ordered):
    quad_order(ordered, (own, r1, r2, r3))
    state, log = load(ordered.at[0])
    for place in range(1, QUAD):
        part, part_log = load(ordered.at[place])
        state, log = state * jnp.exp(part_log) + part, log + part_log
    store(sent, state, log)
    state_out[...] = state
    log_out[...] = log


def hop_kernel(half, turn, before, total, total_log, out):
    @pl.when(lax.rem(lax.axis_index("sp") // QUAD, half) == turn)
    def _():
        state, log = load(before)
        store(out, state * jnp.exp(total_log[...]) + total[...], log + total_log[...])


def top_kernel(half, before, total, total_log, out):
    @pl.when(lax.axis_index("sp") // QUAD == half - 1)
    def _():
        out[...] = (before[0:STATE, :].astype(F32) * jnp.exp(total_log[...]) + total[...]).astype(BF16)


def relay_kernel(half, own, got, out):
    @pl.when(lax.axis_index("sp") // QUAD == half - 1)
    def _():
        out[...] = own[...]

    @pl.when(lax.axis_index("sp") // QUAD == half + 1)
    def _():
        out[...] = got[...]


def prefix_kernel(half, *refs):
    passed, tops, quad, outs = refs[: half - 1], refs[half - 1 : half + 2], refs[half + 2 : half + 6], refs[half + 6 : half + 10]
    ordered, ends, held, top = refs[half + 10 :]
    place = lax.axis_index("sp")
    group = place // QUAD
    quad_order(ordered, quad)
    held[...] = jnp.zeros_like(held)
    top[...] = jnp.zeros_like(top)
    for turn, ref in enumerate(passed):

        @pl.when(lax.rem(group, half) == turn + 1)
        def _(ref=ref):
            held[...] = ref[...]

    for ref, targets in zip(tops, ((half + 1,), (half + 3,), (half, half + 2)), strict=True):
        for target in targets:

            @pl.when(group == target)
            def _(ref=ref):
                top[...] = ref[...]

    state, log = load(held)
    state = top[...].astype(F32) * jnp.exp(log) + state
    ends[0] = state.astype(BF16)
    for turn in range(QUAD - 1):
        part, log = load(ordered.at[turn])
        state = state * jnp.exp(log) + part
        ends[turn + 1] = state.astype(BF16)
    me = lax.rem(place, QUAD)
    for bits, out in enumerate(outs):
        out[...] = ends[me ^ bits]


def gate_kernel(gate, cum_all, gate_out, grow_out):
    matrix = spread_matrix(cum_all.shape[0])
    width = 256
    grow = jnp.exp(cum_all[...])
    for start in range(0, gate.shape[1], width):
        lanes = slice(start, start + width)
        gated = silu(gate[:, lanes].astype(F32))
        gate_out[:, lanes] = gated
        grow_out[:, lanes] = gated * spread(grow, matrix[:, lanes])


def inside_kernel(
    x_act, b_act, c_act, edge_x, edge_b, edge_c, cum_all, step_all, gate,
    y_out, c_out, b_all, x_first, padded, turned, entering,
):
    span, _ = x_act.shape
    heads = step_all.shape[0]
    groups = b_act.shape[1] // STATE
    per_group = heads // groups
    matrix = spread_matrix(heads)
    keep = lax.broadcasted_iota(jnp.int32, (BLOCK, BLOCK), 0) >= lax.broadcasted_iota(jnp.int32, (BLOCK, BLOCK), 1)
    left = lax.broadcasted_iota(jnp.int32, (BLOCK, 2 * HEAD_DIM), 1) < HEAD_DIM
    c_out[...] = c_act[...]
    c_out[0:EDGE, :] = edge_c[...]
    b_all[...] = b_act[...]
    b_all[0:EDGE, :] = edge_b[...]
    x_first[...] = x_act[0:BLOCK, :]
    x_first[0:EDGE, :] = edge_x[...]
    padded[...] = jnp.zeros_like(padded)
    before = jnp.zeros((heads, 1), F32)
    for start in range(0, span, BLOCK):
        rows = slice(start, start + BLOCK)
        x_blk = x_first if start == 0 else x_act.at[rows]
        cum = cum_all[:, rows] - before
        step = step_all[:, rows]
        padded[0:heads, :] = cum
        turned[...] = jnp.transpose(padded[...])
        total = cum[:, BLOCK - 1 :]
        before = before + total
        grow = jnp.exp(cum)
        weight = jnp.exp(total - cum) * step
        for group in range(groups):
            lanes = slice(group * STATE, (group + 1) * STATE)
            channels = slice(group * per_group * HEAD_DIM, (group + 1) * per_group * HEAD_DIM)
            b_blk, c_blk = b_all[rows, lanes], c_out[rows, lanes]
            scores = dot(c_blk, b_blk, ((1,), (1,)))
            if start > 0:
                read = dot(c_blk, entering[:, channels].astype(BF16)) * spread(grow, matrix[:, channels])
            for pair in range(per_group // 2):
                first = (group * per_group + 2 * pair) * HEAD_DIM
                results = []
                for head in (group * per_group + 2 * pair, group * per_group + 2 * pair + 1):
                    difference = turned[:, head : head + 1] - cum[head : head + 1, :]
                    decay = jnp.exp(jnp.where(keep, difference, -jnp.inf))
                    mixing = (scores * decay * step[head : head + 1, :]).astype(BF16)
                    results.append(dot(mixing, x_blk[:, first : first + 2 * HEAD_DIM]))
                y = jnp.where(left, results[0], results[1])
                if start > 0:
                    y = y + read[:, 2 * pair * HEAD_DIM : 2 * (pair + 1) * HEAD_DIM]
                y_out[rows, first : first + 2 * HEAD_DIM] = y * gate[rows, first : first + 2 * HEAD_DIM]
            if start + BLOCK < span:
                weighted = (x_blk[:, channels].astype(F32) * spread(weight, matrix[:, channels])).astype(BF16)
                added = dot(b_blk, weighted, ((0,), (0,)))
                if start > 0:
                    grown = spread(jnp.broadcast_to(jnp.exp(total), (heads, BLOCK)), matrix[:, channels], 3)
                    added = entering[:, channels] * grown + added
                entering[:, channels] = added


def output_kernel(own, y_in, grow, c_all, gain, p0, p1, p2, p3, out, ends):
    span, inner = y_in.shape
    groups = c_all.shape[1] // STATE
    quarter = inner // QUAD
    half = span // 2
    core = lax.axis_index("tp")
    rows = pl.ds(pl.multiple_of((core if own else 1 - core) * half, 64), half)
    me = lax.rem(lax.axis_index("sp"), QUAD)
    for bits, ref in enumerate((p0, p1, p2, p3)):
        ends[:, pl.ds(pl.multiple_of((me ^ bits) * quarter, 128), quarter)] = ref[...]
    place = lax.broadcasted_iota(jnp.int32, (quarter, quarter), 0) // HEAD_DIM
    same = place == lax.broadcasted_iota(jnp.int32, (quarter, quarter), 1) // HEAD_DIM
    mean = (same.astype(F32) * (1.0 / HEAD_DIM)).astype(BF16)
    for start in range(0, inner, quarter):
        lanes = slice(start, start + quarter)
        group = start // (inner // groups)
        read = dot(c_all[rows, group * STATE : (group + 1) * STATE], ends[:, lanes])
        gated = y_in[rows, lanes] + read * grow[rows, lanes]
        square = sum(dot(part, mean) for part in parts_of(gated * gated, 2))
        out[:, lanes] = (gated * lax.rsqrt(square + EPS) * gain[:, lanes].astype(F32)).astype(BF16)


def own_kernel(mine, w_own, out):
    out[...] = dot(mine[...], w_own[...])


def sum_kernel(own, other, w_other, out):
    out[...] = (own[...] + dot(other[...], w_other[...])).astype(BF16)


def tail_kernel(values, b_in, c_in, out, sems):
    offset, copies = 0, []
    for turn, source in enumerate((b_in, c_in, values)):
        rows, lanes = pl.ds(source.shape[0] - EDGE, EDGE), pl.ds(offset, source.shape[1])
        copies.append(pltpu.make_async_copy(source.at[rows, :], out.at[:, lanes], sems.at[turn]))
        offset += source.shape[1]
    for copy in copies:
        copy.start()
    for copy in copies:
        copy.wait()


def body(
    gate_in, values_in, input_state_in, output_state_in, step_in, conv_x, conv_b, conv_c, dt_bias, decay_rate, log_decay_extra,
    out_gain, w_out,
):
    span, inner = values_in.shape
    shared = input_state_in.shape[1]
    heads = step_in.shape[1]
    places = lax.axis_size("sp")
    quarter = inner // QUAD
    shape = jax.ShapeDtypeStruct
    vmem = pltpu.VMEM

    def move(x, route):
        return lax.ppermute(x, "sp", route)

    def exchange(x, bits, count=places):
        return move(x, [(i, i ^ bits) for i in range(count)])

    def edge_specs(block):
        return [pl.BlockSpec((EDGE, a.shape[1]), lambda i: (block, 0)) for a in (values_in, input_state_in, output_state_in)]

    tail = pl.pallas_call(
        tail_kernel,
        out_shape=shape((EDGE, inner + 2 * shared), BF16),
        in_specs=[pl.BlockSpec(memory_space=pl.ANY)] * 3,
        out_specs=whole(1)[0],
        scratch_shapes=[pltpu.SemaphoreType.DMA((3,))],
        compiler_params=pltpu.CompilerParams(vmem_limit_bytes=SMALL),
        name="tail",
    )(*(pltpu.with_memory_space_constraint(a, pltpu.HBM) for a in (values_in, input_state_in, output_state_in)))
    halo = move(tail, [(i, i + 1) for i in range(places - 1)])

    args = [
        values_in, input_state_in, output_state_in, step_in.T, log_decay_extra.T, conv_x, conv_b, conv_c,
        dt_bias.reshape(1, heads), decay_rate.reshape(1, heads),
    ]
    outs = [
        shape((span, inner), BF16), shape((span, shared), BF16), shape((span, shared), BF16), shape((heads, span), F32),
        shape((heads, span), F32), shape((STATE, inner), F32), shape((EXTRA, inner), BF16), shape((EDGE, inner), F32),
    ]
    x_act, b_act, c_act, cum, step, state, logs, edge_weight = pl.pallas_call(
        local_kernel,
        out_shape=outs,
        in_specs=[pl.BlockSpec(memory_space=pltpu.HBM)] * len(args),
        out_specs=whole(len(outs)),
        scratch_shapes=[vmem((span + 8, 256), F32)] + [vmem(a.shape, a.dtype) for a in args] + [pltpu.SemaphoreType.DMA((len(args),))],
        compiler_params=pltpu.CompilerParams(vmem_limit_bytes=LARGE),
        cost_estimate=pl.CostEstimate(flops=FILL, bytes_accessed=4_000_000, transcendentals=0),
        name="local",
    )(*(pltpu.with_memory_space_constraint(a, pltpu.HBM) for a in args))
    w_other, _ = lax.optimization_barrier((w_out, logs))
    w_other = lax.ppermute(w_other, "tp", [(0, 1), (1, 0)])
    payload = shape((STATE + EXTRA, quarter), BF16)
    edge_x, edge_b, edge_c, *slots = pl.pallas_call(
        edge_kernel,
        out_shape=[
            shape((EDGE, inner), BF16), shape((EDGE, shared), BF16), shape((EDGE, shared), BF16), payload, payload, payload, payload,
        ],
        grid=(1,),
        in_specs=edge_specs(0) + whole(7),
        out_specs=whole(7),
        scratch_shapes=[vmem((2 * EDGE, inner + 2 * shared), F32), vmem((STATE + EXTRA, inner), BF16)],
        compiler_params=pltpu.CompilerParams(vmem_limit_bytes=SMALL),
        name="edge",
    )(values_in, input_state_in, output_state_in, halo, conv_x, conv_b, conv_c, state, logs, edge_weight)
    gate, grow = local_call(gate_kernel, [shape((span, inner), F32)] * 2, [gate_in, cum], flops=FILL)
    y_inside, c_all = local_call(
        inside_kernel,
        [shape((span, inner), F32), shape((span, shared), BF16)],
        [x_act, b_act, c_act, edge_x, edge_b, edge_c, cum, step, gate],
        [
            vmem((span, shared), BF16), vmem((BLOCK, inner), BF16), vmem((BLOCK, BLOCK), F32), vmem((BLOCK, BLOCK), F32),
            vmem((STATE, inner), F32),
        ],
        flops=FILL,
    )

    order = vmem((QUAD, STATE + EXTRA, quarter), BF16)
    arrived = {bits: exchange(slots[bits], bits) for bits in (3, 2, 1)}
    quad = [slots[0], arrived[1], arrived[2], arrived[3]]
    slice_of = shape((STATE, quarter), BF16)
    kept = [shape((STATE, quarter), F32), shape((1, quarter), F32)]
    sent, total, log = local_call(quad_total_kernel, [payload, *kept], quad, [order], limit=SMALL)
    half = places // QUAD // 2

    def up(x, sources, fours):
        return move(x, [(i, i + fours * QUAD) for four in sources for i in range(four * QUAD, (four + 1) * QUAD)])

    passed = []
    for turn in range(half - 1):
        if turn:
            sent = local_call(functools.partial(hop_kernel, half, turn), payload, [passed[-1], total, log], limit=SMALL)
        passed.append(up(sent, (turn, half + turn), 1))
    lower = local_call(functools.partial(top_kernel, half), slice_of, [passed[-1], total, log], limit=SMALL)
    second = up(lower, (half - 1,), 2)
    fourth = up(lower, (half - 1,), 4)
    relayed = local_call(functools.partial(relay_kernel, half), slice_of, [lower, second], limit=SMALL)
    first = up(relayed, (half - 1, half + 1), 1)
    ends = local_call(
        functools.partial(prefix_kernel, half),
        [slice_of] * QUAD,
        [*passed, second, fourth, first, *quad],
        [order, vmem((QUAD, STATE, quarter), BF16), vmem(payload.shape, BF16), vmem(slice_of.shape, BF16)],
        limit=SMALL,
    )
    carried = {bits: exchange(ends[bits], bits) for bits in (3, 2, 1)}

    def normalized(own):
        return local_call(
            functools.partial(output_kernel, own),
            shape((span // 2, inner), BF16),
            [y_inside, grow, c_all, out_gain.reshape(1, inner), ends[0], carried[1], carried[2], carried[3]],
            [vmem((STATE, inner), BF16)],
        )

    theirs = normalized(False)
    other_rows = lax.ppermute(theirs, "tp", [(0, 1), (1, 0)])
    mine = normalized(True)
    wide = shape((span // 2, w_out.shape[1]), F32)
    own = local_call(own_kernel, wide, [mine, w_out], flops=FILL)
    return local_call(sum_kernel, shape(wide.shape, BF16), [own, other_rows, w_other])


def solution(mesh):
    rows = P(("grp", "sp"), "tp")
    placed = (rows, rows, rows, rows, rows, P(None, "tp"), P(None, "tp"), P(None, "tp"), P("tp"), P("tp"), rows, P("tp"), P("tp", None))
    return jax.shard_map(body, mesh=mesh, in_specs=placed, out_specs=P(("grp", "sp", "tp"), None), check_vma=False)
```

profile of v0, /device:TPU:2021, one launch (start us, length us, event | category | flops | bytes accessed | tf_op | source)
XLA Modules:
  0.0 88.0 jit_solution(12835227654681607870)
XLA Ops:
  0.0 4.9 %local.1 = (bf16[384,1024]{1,0:T(8,128)(2,1)S(1)}, bf16[384,256]{1,0:T(8,128)(2,1)S(1)}, bf16[384,256]{1,0:T(8,128)(2,1)S(1)}, f32[16,384]{1,0:T(8,128)S(1)}, f3...) custom-call(bf16[384,1024]{1,0:T(8,128)(2,1)} %values.3, ...), custom_call_target="tpu_custom_call" | custom-call | flops 4000000000 | bytes 4000000 | tf_op jit(solution)/shard_map/local/pallas_call | solution.py:401
  5.0 0.0 copy-start
  5.0 0.7 collective-permute-start.14
  5.7 0.8 tail.1
  6.6 1.3 %collective-permute-start = (bf16[16,1536]{1,0:T(8,128)(2,1)S(1)}, bf16[16,1536]{1,0:T(8,128)(2,1)S(1)}, u32[]{:S(2)}, u32[]{:S(2)}) collective-permute-start(bf16[16,1536]{1,0:T(8,128)(2,1)S(1)} %tail.1), channel_id=1, source_target_pairs={{0,2},{2,4},{4,6},{6,8},{8,10},{10,12},{12,14},{14,16},{16,18},{18... | collective-permute-start | bytes 147464 | tf_op jit(solution)/shard_map/ppermute | solution.py:374
  7.9 3.5 %collective-permute-done.halo = bf16[16,1536]{1,0:T(8,128)(2,1)S(1)} collective-permute-done((bf16[16,1536]{1,0:T(8,128)(2,1)S(1)}, bf16[16,1536]{1,0:T(8,128)(2,1)S(1)}, u32[]{:S(2)}, u32[]{:S(2)}) %collective-permute-start) | collective-permute-done | bytes 49184 | tf_op jit(solution)/shard_map/ppermute | solution.py:374
  11.4 0.0 copy-done.4
  11.4 0.0 copy-done.5
  11.5 0.0 copy-done
  11.5 0.0 copy-start.7
  11.5 0.4 edge.1
  11.9 0.6 collective-permute-start.1
  12.5 2.0 %collective-permute-start.2 = (bf16[144,256]{1,0:T(8,128)(2,1)S(1)}, bf16[144,256]{1,0:T(8,128)(2,1)S(1)}, u32[]{:S(2)}, u32[]{:S(2)}) collective-permute-start(bf16[144,256]{1,0:T(8,128)(2,1)S(1)} %get-tuple-element.49), channel_id=1, source_target_pairs={{0,4},{2,6},{4,0},{6,2},{8,12},{10,14},{12,8},{14,10},{16,20},{18,... | collective-permute-start | bytes 221192 | tf_op jit(solution)/shard_map/ppermute | solution.py:374
  14.5 1.1 %collective-permute-start.3 = (bf16[144,256]{1,0:T(8,128)(2,1)S(1)}, bf16[144,256]{1,0:T(8,128)(2,1)S(1)}, u32[]{:S(2)}, u32[]{:S(2)}) collective-permute-start(bf16[144,256]{1,0:T(8,128)(2,1)S(1)} %get-tuple-element.50), channel_id=1, source_target_pairs={{0,6},{2,4},{4,2},{6,0},{8,14},{10,12},{12,10},{14,8},{16,22},{18,... | collective-permute-start | bytes 221192 | tf_op jit(solution)/shard_map/ppermute | solution.py:374
  15.5 0.0 collective-permute-done.1.r1.refs_7_
  15.5 1.3 %collective-permute-done.2.r2.refs_8_ = bf16[144,256]{1,0:T(8,128)(2,1)S(1)} collective-permute-done((bf16[144,256]{1,0:T(8,128)(2,1)S(1)}, bf16[144,256]{1,0:T(8,128)(2,1)S(1)}, u32[]{:S(2)}, u32[]{:S(2)}) %collective-permute-start.2) | collective-permute-done | bytes 73760 | tf_op jit(solution)/shard_map/ppermute | solution.py:374
  16.8 3.3 %collective-permute-done.3.r3.refs_9_ = bf16[144,256]{1,0:T(8,128)(2,1)S(1)} collective-permute-done((bf16[144,256]{1,0:T(8,128)(2,1)S(1)}, bf16[144,256]{1,0:T(8,128)(2,1)S(1)}, u32[]{:S(2)}, u32[]{:S(2)}) %collective-permute-start.3) | collective-permute-done | bytes 73760 | tf_op jit(solution)/shard_map/ppermute | solution.py:374
  20.2 0.1 shard_map.129
  20.3 0.7 collective-permute-start.4
  20.9 0.0 collective-permute-done.4.before.refs_0_
  21.0 0.7 collective-permute-start.5
  21.7 0.0 collective-permute-done.5.before.refs_1_
  21.7 1.3 %collective-permute-start.6 = (bf16[144,256]{1,0:T(8,128)(2,1)S(1)}, bf16[144,256]{1,0:T(8,128)(2,1)S(1)}, u32[]{:S(2)}, u32[]{:S(2)}) collective-permute-start(bf16[144,256]{1,0:T(8,128)(2,1)S(1)} %shard_map.131), channel_id=1, source_target_pairs={{16,24},{18,26},{20,28},{22,30},{48,56},{50,58},{52,60},{54,62},{1... | collective-permute-start | bytes 221192 | tf_op jit(solution)/shard_map/ppermute | solution.py:374
  23.0 20.2 %collective-permute-done.6.before.refs_2_ = bf16[144,256]{1,0:T(8,128)(2,1)S(1)} collective-permute-done((bf16[144,256]{1,0:T(8,128)(2,1)S(1)}, bf16[144,256]{1,0:T(8,128)(2,1)S(1)}, u32[]{:S(2)}, u32[]{:S(2)}) %collective-permute-start.6) | collective-permute-done | bytes 73760 | tf_op jit(solution)/shard_map/ppermute | solution.py:374
  43.2 0.7 collective-permute-start.7
  43.9 1.3 %collective-permute-start.8 = (bf16[128,256]{1,0:T(8,128)(2,1)S(1)}, bf16[128,256]{1,0:T(8,128)(2,1)S(1)}, u32[]{:S(2)}, u32[]{:S(2)}) collective-permute-start(bf16[128,256]{1,0:T(8,128)(2,1)S(1)} %shard_map.132.own), channel_id=1, source_target_pairs={{24,56},{26,58},{28,60},{30,62},{25,57},{27,59},{29,61},{31,63},{8... | collective-permute-start | bytes 196616 | tf_op jit(solution)/shard_map/ppermute | solution.py:374
  45.2 0.0 collective-permute-done.7.got.refs_3_
  45.3 0.7 collective-permute-start.9
  45.9 0.0 copy-start.8
  46.0 0.6 shard_map.127
  46.6 0.1 copy-done.8
  46.6 20.7 %collective-permute-done.8.refs_4_ = bf16[128,256]{1,0:T(8,128)(2,1)S(1)} collective-permute-done((bf16[128,256]{1,0:T(8,128)(2,1)S(1)}, bf16[128,256]{1,0:T(8,128)(2,1)S(1)}, u32[]{:S(2)}, u32[]{:S(2)}) %collective-permute-start.8) | collective-permute-done | bytes 65568 | tf_op jit(solution)/shard_map/ppermute | solution.py:374
  67.3 0.0 collective-permute-done.9.refs_5_
  67.3 0.2 shard_map.134
  67.5 0.1 collective-permute-start.10
  67.6 0.1 collective-permute-start.11
  67.8 3.4 %collective-permute-start.12 = (bf16[128,256]{1,0:T(8,128)(2,1)S(1)}, bf16[128,256]{1,0:T(8,128)(2,1)S(1)}, u32[]{:S(2)}, u32[]{:S(2)}) collective-permute-start(bf16[128,256]{1,0:T(8,128)(2,1)S(1)} %get-tuple-element.57), channel_id=1, source_target_pairs={{0,6},{2,4},{4,2},{6,0},{8,14},{10,12},{12,10},{14,8},{16,22},{18,... | collective-permute-start | bytes 196616 | tf_op jit(solution)/shard_map/ppermute | solution.py:374
  71.1 2.6 %shard_map.128 = (f32[384,1024]{1,0:T(8,128)S(1)}, bf16[384,256]{1,0:T(8,128)(2,1)S(1)}) custom-call(bf16[384,1024]{1,0:T(8,128)(2,1)S(1)} %get-tuple-element.32.x_act, bf16[384,256]{1,0:T(8,128)(2,1)S(1)} %get-tuple-element.33.b_act, bf16[384,256]{1,0:T(8,128)(2,1)S(1)} %get-tuple-element.34.c_act, bf16[16,1024]{1,0:T(8,128)(2,1)S(1)} %get-tuple-element.38.edge_x, ...), custom_call_target="tpu_custom_call" | custom-call | flops 4000000000 | bytes 2850816 | tf_op jit(solution)/shard_map/pallas_call | solution.py:153
  73.7 0.0 collective-permute-done.10.p1
  73.7 0.0 collective-permute-done.11.p2
  73.7 0.5 collective-permute-done.12.p3
  74.3 0.7 shard_map.137
  75.0 9.4 %collective-permute-start.13 = (bf16[192,1024]{1,0:T(8,128)(2,1)S(1)}, bf16[192,1024]{1,0:T(8,128)(2,1)S(1)}, u32[]{:S(2)}, u32[]{:S(2)}) collective-permute-start(bf16[192,1024]{1,0:T(8,128)(2,1)S(1)} %shard_map.137), channel_id=1, source_target_pairs={{0,1},{1,0},{2,3},{3,2},{4,5},{5,4},{6,7},{7,6},{8,9},{9,8},{10,11... | collective-permute-start | bytes 1179656 | tf_op jit(solution)/shard_map/ppermute | solution.py:477
  84.4 0.7 shard_map.135.mine
  85.1 1.0 %shard_map.136.own = f32[192,2048]{1,0:T(8,128)S(1)} custom-call(bf16[192,1024]{1,0:T(8,128)(2,1)S(1)} %shard_map.135.mine, bf16[1024,2048]{1,0:T(8,128)(2,1)S(1)} %copy-done.6), custom_call_target="tpu_custom_call" | custom-call | flops 4000000000 | bytes 4587520 | tf_op jit(solution)/shard_map/pallas_call | solution.py:153
  86.1 0.0 collective-permute-done.13.other
  86.1 0.0 collective-permute-done.14.w_other
  86.2 1.9 %shard_map.138 = bf16[192,2048]{1,0:T(8,128)(2,1)} custom-call(f32[192,2048]{1,0:T(8,128)S(1)} %shard_map.136.own, bf16[192,1024]{1,0:T(8,128)(2,1)S(1)} %collective-permute-done.13.other, bf16[1024,2048]{1,0:T(8,128)(2,1)S(1)} %collective-permute-done.14.w_other), custom_call_target="tpu_custom_call" | custom-call | bytes 6160384 | tf_op jit(solution)/shard_map/pallas_call | solution.py:153
  (16 shorter events, 0.1 us)
Async XLA Ops:
  0.0 5.0 %copy-start.6 = (bf16[1024,2048]{1,0:T(8,128)(2,1)S(1)}, bf16[1024,2048]{1,0:T(8,128)(2,1)}, u32[]{:S(2)}) copy-start(bf16[1024,2048]{1,0:T(8,128)(2,1)} %w_own.1) | copy-start | bytes 12582916
  0.0 11.4 %copy-start.1 = (bf16[384,256]{1,0:T(8,128)(2,1)S(1)}, bf16[384,256]{1,0:T(8,128)(2,1)}, u32[]{:S(2)}) copy-start(bf16[384,256]{1,0:T(8,128)(2,1)} %b_in.3) | copy-start | bytes 589828
  0.0 11.4 %copy-start.2 = (bf16[384,256]{1,0:T(8,128)(2,1)S(1)}, bf16[384,256]{1,0:T(8,128)(2,1)}, u32[]{:S(2)}) copy-start(bf16[384,256]{1,0:T(8,128)(2,1)} %c_in.3) | copy-start | bytes 589828
  0.0 11.4 %copy-start.3 = (bf16[4,1024]{1,0:T(4,128)(2,1)S(1)}, bf16[4,1024]{1,0:T(4,128)(2,1)}, u32[]{:S(2)}) copy-start(bf16[4,1024]{1,0:T(4,128)(2,1)} %conv_x.1) | copy-start | bytes 24580
  0.0 11.4 %copy-start.4 = (bf16[4,256]{1,0:T(4,128)(2,1)S(1)}, bf16[4,256]{1,0:T(4,128)(2,1)}, u32[]{:S(2)}) copy-start(bf16[4,256]{1,0:T(4,128)(2,1)} %conv_b.1) | copy-start | bytes 6148
  0.0 11.4 %copy-start.5 = (bf16[4,256]{1,0:T(4,128)(2,1)S(1)}, bf16[4,256]{1,0:T(4,128)(2,1)}, u32[]{:S(2)}) copy-start(bf16[4,256]{1,0:T(4,128)(2,1)} %conv_c.1) | copy-start | bytes 6148
  5.0 6.5 %copy-start = (bf16[384,1024]{1,0:T(8,128)(2,1)S(1)}, bf16[384,1024]{1,0:T(8,128)(2,1)}, u32[]{:S(2)}) copy-start(bf16[384,1024]{1,0:T(8,128)(2,1)} %values.3) | copy-start | bytes 2359300
  5.0 81.1 %collective-permute-start.14 = (bf16[1024,2048]{1,0:T(8,128)(2,1)S(1)}, bf16[1024,2048]{1,0:T(8,128)(2,1)S(1)}, u32[]{:S(2)}, u32[]{:S(2)}) collective-permute-start(bf16[1024,2048]{1,0:T(8,128)(2,1)S(1)} %copy-done.6), channel_id=1, source_target_pairs={{0,1},{1,0},{2,3},{3,2},{4,5},{5,4},{6,7},{7,6},{8,9},{9,8},{10,11... | collective-permute-start | bytes 12582920 | tf_op jit(solution)/shard_map/ppermute | solution.py:412
  6.6 4.9 %collective-permute-start = (bf16[16,1536]{1,0:T(8,128)(2,1)S(1)}, bf16[16,1536]{1,0:T(8,128)(2,1)S(1)}, u32[]{:S(2)}, u32[]{:S(2)}) collective-permute-start(bf16[16,1536]{1,0:T(8,128)(2,1)S(1)} %tail.1), channel_id=1, source_target_pairs={{0,2},{2,4},{4,6},{6,8},{8,10},{10,12},{12,14},{14,16},{16,18},{18... | collective-permute-start | bytes 147464 | tf_op jit(solution)/shard_map/ppermute | solution.py:374
  11.5 34.5 %copy-start.7 = (bf16[384,1024]{1,0:T(8,128)(2,1)S(1)}, bf16[384,1024]{1,0:T(8,128)(2,1)}, u32[]{:S(2)}) copy-start(bf16[384,1024]{1,0:T(8,128)(2,1)} %gate.1) | copy-start | bytes 2359300
  11.9 3.7 %collective-permute-start.1 = (bf16[144,256]{1,0:T(8,128)(2,1)S(1)}, bf16[144,256]{1,0:T(8,128)(2,1)S(1)}, u32[]{:S(2)}, u32[]{:S(2)}) collective-permute-start(bf16[144,256]{1,0:T(8,128)(2,1)S(1)} %get-tuple-element.48), channel_id=1, source_target_pairs={{0,2},{2,0},{4,6},{6,4},{8,10},{10,8},{12,14},{14,12},{16,18},{18,... | collective-permute-start | bytes 221192 | tf_op jit(solution)/shard_map/ppermute | solution.py:374
  12.5 4.3 %collective-permute-start.2 = (bf16[144,256]{1,0:T(8,128)(2,1)S(1)}, bf16[144,256]{1,0:T(8,128)(2,1)S(1)}, u32[]{:S(2)}, u32[]{:S(2)}) collective-permute-start(bf16[144,256]{1,0:T(8,128)(2,1)S(1)} %get-tuple-element.49), channel_id=1, source_target_pairs={{0,4},{2,6},{4,0},{6,2},{8,12},{10,14},{12,8},{14,10},{16,20},{18,... | collective-permute-start | bytes 221192 | tf_op jit(solution)/shard_map/ppermute | solution.py:374
  14.5 5.7 %collective-permute-start.3 = (bf16[144,256]{1,0:T(8,128)(2,1)S(1)}, bf16[144,256]{1,0:T(8,128)(2,1)S(1)}, u32[]{:S(2)}, u32[]{:S(2)}) collective-permute-start(bf16[144,256]{1,0:T(8,128)(2,1)S(1)} %get-tuple-element.50), channel_id=1, source_target_pairs={{0,6},{2,4},{4,2},{6,0},{8,14},{10,12},{12,10},{14,8},{16,22},{18,... | collective-permute-start | bytes 221192 | tf_op jit(solution)/shard_map/ppermute | solution.py:374
  20.3 0.7 collective-permute-start.4
  21.0 0.7 collective-permute-start.5
  21.7 21.5 %collective-permute-start.6 = (bf16[144,256]{1,0:T(8,128)(2,1)S(1)}, bf16[144,256]{1,0:T(8,128)(2,1)S(1)}, u32[]{:S(2)}, u32[]{:S(2)}) collective-permute-start(bf16[144,256]{1,0:T(8,128)(2,1)S(1)} %shard_map.131), channel_id=1, source_target_pairs={{16,24},{18,26},{20,28},{22,30},{48,56},{50,58},{52,60},{54,62},{1... | collective-permute-start | bytes 221192 | tf_op jit(solution)/shard_map/ppermute | solution.py:374
  43.2 2.0 %collective-permute-start.7 = (bf16[128,256]{1,0:T(8,128)(2,1)S(1)}, bf16[128,256]{1,0:T(8,128)(2,1)S(1)}, u32[]{:S(2)}, u32[]{:S(2)}) collective-permute-start(bf16[128,256]{1,0:T(8,128)(2,1)S(1)} %shard_map.132.own), channel_id=1, source_target_pairs={{24,40},{26,42},{28,44},{30,46},{25,41},{27,43},{29,45},{31,47},{8... | collective-permute-start | bytes 196616 | tf_op jit(solution)/shard_map/ppermute | solution.py:374
  43.9 23.4 %collective-permute-start.8 = (bf16[128,256]{1,0:T(8,128)(2,1)S(1)}, bf16[128,256]{1,0:T(8,128)(2,1)S(1)}, u32[]{:S(2)}, u32[]{:S(2)}) collective-permute-start(bf16[128,256]{1,0:T(8,128)(2,1)S(1)} %shard_map.132.own), channel_id=1, source_target_pairs={{24,56},{26,58},{28,60},{30,62},{25,57},{27,59},{29,61},{31,63},{8... | collective-permute-start | bytes 196616 | tf_op jit(solution)/shard_map/ppermute | solution.py:374
  45.3 22.0 %collective-permute-start.9 = (bf16[128,256]{1,0:T(8,128)(2,1)S(1)}, bf16[128,256]{1,0:T(8,128)(2,1)S(1)}, u32[]{:S(2)}, u32[]{:S(2)}) collective-permute-start(bf16[128,256]{1,0:T(8,128)(2,1)S(1)} %shard_map.133), channel_id=1, source_target_pairs={{24,32},{26,34},{28,36},{30,38},{40,48},{42,50},{44,52},{46,54},{2... | collective-permute-start | bytes 196616 | tf_op jit(solution)/shard_map/ppermute | solution.py:374
  45.9 0.7 copy-start.8
  67.5 6.3 %collective-permute-start.10 = (bf16[128,256]{1,0:T(8,128)(2,1)S(1)}, bf16[128,256]{1,0:T(8,128)(2,1)S(1)}, u32[]{:S(2)}, u32[]{:S(2)}) collective-permute-start(bf16[128,256]{1,0:T(8,128)(2,1)S(1)} %get-tuple-element.55), channel_id=1, source_target_pairs={{0,2},{2,0},{4,6},{6,4},{8,10},{10,8},{12,14},{14,12},{16,18},{18,... | collective-permute-start | bytes 196616 | tf_op jit(solution)/shard_map/ppermute | solution.py:374
  67.6 6.1 %collective-permute-start.11 = (bf16[128,256]{1,0:T(8,128)(2,1)S(1)}, bf16[128,256]{1,0:T(8,128)(2,1)S(1)}, u32[]{:S(2)}, u32[]{:S(2)}) collective-permute-start(bf16[128,256]{1,0:T(8,128)(2,1)S(1)} %get-tuple-element.56), channel_id=1, source_target_pairs={{0,4},{2,6},{4,0},{6,2},{8,12},{10,14},{12,8},{14,10},{16,20},{18,... | collective-permute-start | bytes 196616 | tf_op jit(solution)/shard_map/ppermute | solution.py:374
  67.8 6.5 %collective-permute-start.12 = (bf16[128,256]{1,0:T(8,128)(2,1)S(1)}, bf16[128,256]{1,0:T(8,128)(2,1)S(1)}, u32[]{:S(2)}, u32[]{:S(2)}) collective-permute-start(bf16[128,256]{1,0:T(8,128)(2,1)S(1)} %get-tuple-element.57), channel_id=1, source_target_pairs={{0,6},{2,4},{4,2},{6,0},{8,14},{10,12},{12,10},{14,8},{16,22},{18,... | collective-permute-start | bytes 196616 | tf_op jit(solution)/shard_map/ppermute | solution.py:374
  75.0 11.1 %collective-permute-start.13 = (bf16[192,1024]{1,0:T(8,128)(2,1)S(1)}, bf16[192,1024]{1,0:T(8,128)(2,1)S(1)}, u32[]{:S(2)}, u32[]{:S(2)}) collective-permute-start(bf16[192,1024]{1,0:T(8,128)(2,1)S(1)} %shard_map.137), channel_id=1, source_target_pairs={{0,1},{1,0},{2,3},{3,2},{4,5},{5,4},{6,7},{7,6},{8,9},{9,8},{10,11... | collective-permute-start | bytes 1179656 | tf_op jit(solution)/shard_map/ppermute | solution.py:477
where the time goes:
time: 89.5 us; the launch traced here: 88 us
  waiting for transfers between devices  49.6 us (55%)
  starting transfers between devices  24 us (27%)
  Pallas kernels  14 us (16%)
    ppermute x13, waiting for transfers between devices, move(): return lax.ppermute(x, 'sp', route)  49.6 us
    ppermute x13, starting transfers between devices, move(): return lax.ppermute(x, 'sp', route)  13.9 us
    ppermute x1, starting transfers between devices, body(): other_rows = lax.ppermute(theirs, 'tp', [(0, 1), (1, 0)])  9.39 us
    pallas_call x12, Pallas kernels, local_call(): pl.pallas_call(kernel, out_shape=outs, in_specs=whole(len(args)), out_spe...  7.87 us
    pallas_call x1, Pallas kernels, body(): pl.pallas_call(local_kernel, out_shape=outs, in_specs=[pl.BlockSpec(memor...  4.94 us
  transfers between devices with their start and end apart: 15, of which 6 were waited for; matrix products, arithmetic and copies ran while one was open for 0% of the time, Pallas kernels for 8%

commit v1 on v0

--- a/solution.py
+++ b/solution.py
@@ -191,52 +191,37 @@
     log_out[...] = log
 
 
-def hop_kernel(half, turn, before, total, total_log, out):
-    @pl.when(lax.rem(lax.axis_index("sp") // QUAD, half) == turn)
+def jump_kernel(four, before, last, total, total_log, out):
+    @pl.when(lax.axis_index("sp") // QUAD == four)
     def _():
-        state, log = load(before)
-        store(out, state * jnp.exp(total_log[...]) + total[...], log + total_log[...])
-
-
-def top_kernel(half, before, total, total_log, out):
-    @pl.when(lax.axis_index("sp") // QUAD == half - 1)
-    def _():
-        out[...] = (before[0:STATE, :].astype(F32) * jnp.exp(total_log[...]) + total[...]).astype(BF16)
-
-
-def relay_kernel(half, own, got, out):
-    @pl.when(lax.axis_index("sp") // QUAD == half - 1)
-    def _():
-        out[...] = own[...]
-
-    @pl.when(lax.axis_index("sp") // QUAD == half + 1)
-    def _():
-        out[...] = got[...]
-
-
-def prefix_kernel(half, *refs):
-    passed, tops, quad, outs = refs[: half - 1], refs[half - 1 : half + 2], refs[half + 2 : half + 6], refs[half + 6 : half + 10]
-    ordered, ends, held, top = refs[half + 10 :]
+        state = before[0:STATE, :].astype(F32)
+        if last is not None:
+            part, log = load(last)
+            state = state * jnp.exp(log) + part
+        out[...] = (state * jnp.exp(total_log[...]) + total[...]).astype(BF16)
+
+
+def prefix_kernel(targets, *refs):
+    ordered, ends, held, got = refs[-4:]
+    quad, outs = refs[-12:-8], refs[-8:-4]
+    arrived, pairs = refs[:-13], refs[-13]
     place = lax.axis_index("sp")
     group = place // QUAD
     quad_order(ordered, quad)
     held[...] = jnp.zeros_like(held)
-    top[...] = jnp.zeros_like(top)
-    for turn, ref in enumerate(passed):
-
-        @pl.when(lax.rem(group, half) == turn + 1)
+    got[...] = jnp.zeros_like(got)
+    for target, ref in zip(targets, arrived, strict=True):
+
+        @pl.when(group == target)
         def _(ref=ref):
-            held[...] = ref[...]
-
-    for ref, targets in zip(tops, ((half + 1,), (half + 3,), (half, half + 2)), strict=True):
-        for target in targets:
-
-            @pl.when(group == target)
-            def _(ref=ref):
-                top[...] = ref[...]
+            got[...] = ref[0:STATE, :]
+
+    @pl.when(jnp.logical_and(group > max(targets) // 2, lax.rem(group, 2) == 1))
+    def _():
+        held[...] = pairs[...]
 
     state, log = load(held)
-    state = top[...].astype(F32) * jnp.exp(log) + state
+    state = got[...].astype(F32) * jnp.exp(log) + state
     ends[0] = state.astype(BF16)
     for turn in range(QUAD - 1):
         part, log = load(ordered.at[turn])
@@ -316,7 +301,7 @@
                 entering[:, channels] = added
 
 
-def output_kernel(own, y_in, grow, c_all, gain, p0, p1, p2, p3, out, ends):
+def output_kernel(own, y_in, grow, c_all, gain, p0, p1, p2, p3, w_out, out, ends, normalized):
     span, inner = y_in.shape
     groups = c_all.shape[1] // STATE
     quarter = inner // QUAD
@@ -335,15 +320,15 @@
         read = dot(c_all[rows, group * STATE : (group + 1) * STATE], ends[:, lanes])
         gated = y_in[rows, lanes] + read * grow[rows, lanes]
         square = sum(dot(part, mean) for part in parts_of(gated * gated, 2))
-        out[:, lanes] = (gated * lax.rsqrt(square + EPS) * gain[:, lanes].astype(F32)).astype(BF16)
-
-
-def own_kernel(mine, w_own, out):
-    out[...] = dot(mine[...], w_own[...])
-
-
-def sum_kernel(own, other, w_other, out):
-    out[...] = (own[...] + dot(other[...], w_other[...])).astype(BF16)
+        normalized[:, lanes] = (gated * lax.rsqrt(square + EPS) * gain[:, lanes].astype(F32)).astype(BF16)
+    width = 512
+    for start in range(0, w_out.shape[1], width):
+        lanes = slice(start, start + width)
+        out[:, lanes] = dot(normalized[...], w_out[:, lanes]).astype(out.dtype)
+
+
+def sum_kernel(own, other, out):
+    out[...] = (own[...] + other[...].astype(F32)).astype(BF16)
 
 
 def tail_kernel(values, b_in, c_in, out, sems):
@@ -408,8 +393,6 @@
         cost_estimate=pl.CostEstimate(flops=FILL, bytes_accessed=4_000_000, transcendentals=0),
         name="local",
     )(*(pltpu.with_memory_space_constraint(a, pltpu.HBM) for a in args))
-    w_other, _ = lax.optimization_barrier((w_out, logs))
-    w_other = lax.ppermute(w_other, "tp", [(0, 1), (1, 0)])
     payload = shape((STATE + EXTRA, quarter), BF16)
     edge_x, edge_b, edge_c, *slots = pl.pallas_call(
         edge_kernel,
@@ -441,44 +424,57 @@
     slice_of = shape((STATE, quarter), BF16)
     kept = [shape((STATE, quarter), F32), shape((1, quarter), F32)]
     sent, total, log = local_call(quad_total_kernel, [payload, *kept], quad, [order], limit=SMALL)
-    half = places // QUAD // 2
-
-    def up(x, sources, fours):
-        return move(x, [(i, i + fours * QUAD) for four in sources for i in range(four * QUAD, (four + 1) * QUAD)])
-
-    passed = []
-    for turn in range(half - 1):
-        if turn:
-            sent = local_call(functools.partial(hop_kernel, half, turn), payload, [passed[-1], total, log], limit=SMALL)
-        passed.append(up(sent, (turn, half + turn), 1))
-    lower = local_call(functools.partial(top_kernel, half), slice_of, [passed[-1], total, log], limit=SMALL)
-    second = up(lower, (half - 1,), 2)
-    fourth = up(lower, (half - 1,), 4)
-    relayed = local_call(functools.partial(relay_kernel, half), slice_of, [lower, second], limit=SMALL)
-    first = up(relayed, (half - 1, half + 1), 1)
+    fours = places // QUAD
+    half = fours // 2
+
+    def up(x, sources, distance):
+        return move(x, [(i, i + distance * QUAD) for four in sources for i in range(four * QUAD, (four + 1) * QUAD)])
+
+    def jump(four, before, last=None):
+        if last is None:
+            kernel = lambda *refs: jump_kernel(four, refs[0], None, *refs[1:])
+            return local_call(kernel, slice_of, [before, total, log], limit=SMALL)
+        return local_call(functools.partial(jump_kernel, four), slice_of, [before, last, total, log], limit=SMALL)
+
+    pairs = up(sent, range(half, fours, 2), 1)
+    arrived, targets = [], []
+
+    def send(x, four, distance):
+        arrived.append(up(x, (four,), distance))
+        targets.append(four + distance)
+        return arrived[-1]
+
+    before = send(sent, 0, 1)
+    for four in range(1, half - 1):
+        before = send(jump(four, before), four, 1)
+    lower = jump(half - 1, before)
+    for four in range(half - 1, fours - 1, 2):
+        before = send(lower, four, 2)
+        send(lower, four, 1)
+        if four + 2 < fours - 1:
+            lower = jump(four + 2, before, pairs)
     ends = local_call(
-        functools.partial(prefix_kernel, half),
+        functools.partial(prefix_kernel, tuple(targets)),
         [slice_of] * QUAD,
-        [*passed, second, fourth, first, *quad],
+        [*arrived, pairs, *quad],
         [order, vmem((QUAD, STATE, quarter), BF16), vmem(payload.shape, BF16), vmem(slice_of.shape, BF16)],
         limit=SMALL,
     )
     carried = {bits: exchange(ends[bits], bits) for bits in (3, 2, 1)}
 
-    def normalized(own):
+    def projected(own):
         return local_call(
             functools.partial(output_kernel, own),
-            shape((span // 2, inner), BF16),
-            [y_inside, grow, c_all, out_gain.reshape(1, inner), ends[0], carried[1], carried[2], carried[3]],
-            [vmem((STATE, inner), BF16)],
+            shape((span // 2, w_out.shape[1]), F32 if own else BF16),
+            [y_inside, grow, c_all, out_gain.reshape(1, inner), ends[0], carried[1], carried[2], carried[3], w_out],
+            [vmem((STATE, inner), BF16), vmem((span // 2, inner), BF16)],
+            flops=FILL,
         )
 
-    theirs = normalized(False)
-    other_rows = lax.ppermute(theirs, "tp", [(0, 1), (1, 0)])
-    mine = normalized(True)
-    wide = shape((span // 2, w_out.shape[1]), F32)
-    own = local_call(own_kernel, wide, [mine, w_out], flops=FILL)
-    return local_call(sum_kernel, shape(wide.shape, BF16), [own, other_rows, w_other])
+    theirs = projected(False)
+    other = lax.ppermute(theirs, "tp", [(0, 1), (1, 0)])
+    mine = projected(True)
+    return local_call(sum_kernel, shape(mine.shape, BF16), [mine, other])
 
 
 def solution(mesh):

time: 89.5 us -> 72.2 us (0.81)
  the two profiles are of different devices: /device:TPU:2021 before, /device:TPU:1831 now
where the time goes in v1:
time: 72.2 us; the launch traced here: 71.9 us
  starting transfers between devices  32.7 us (45%)
  waiting for transfers between devices  25 us (35%)
  Pallas kernels  13.7 us (19%)
    ppermute x15, starting transfers between devices, move(): return lax.ppermute(x, 'sp', route)  27.4 us
    ppermute x15, waiting for transfers between devices, move(): return lax.ppermute(x, 'sp', route)  24.7 us
    pallas_call x11, Pallas kernels, local_call(): pl.pallas_call(kernel, out_shape=outs, in_specs=whole(len(args)), out_spe...  7.64 us
    ppermute x1, starting transfers between devices, body(): other = lax.ppermute(theirs, 'tp', [(0, 1), (1, 0)])  5.35 us
    pallas_call x1, Pallas kernels, body(): pl.pallas_call(local_kernel, out_shape=outs, in_specs=[pl.BlockSpec(memor...  4.87 us
  transfers between devices with their start and end apart: 16, of which 6 were waited for; matrix products, arithmetic and copies ran while one was open for 0% of the time, Pallas kernels for 13%

profile of v1, /device:TPU:1831, one launch (start us, length us, event | category | flops | bytes accessed | tf_op | source)
XLA Modules:
  0.0 71.9 jit_solution(17393410143412556803)
XLA Ops:
  0.0 0.8 %tail.1 = bf16[16,1536]{1,0:T(8,128)(2,1)S(1)} custom-call(bf16[384,1024]{1,0:T(8,128)(2,1)} %values.3, bf16[384,256]{1,0:T(8,128)(2,1)} %b_in.3, bf16[384,256]{1,0:T(8,128)(2,1)} %c_in.3), custom_call_target="tpu_custom_call" | custom-call | tf_op jit(solution)/shard_map/tail/pallas_call | solution.py:367
  0.8 2.9 %collective-permute-start = (bf16[16,1536]{1,0:T(8,128)(2,1)S(1)}, bf16[16,1536]{1,0:T(8,128)(2,1)S(1)}, u32[]{:S(2)}, u32[]{:S(2)}) collective-permute-start(bf16[16,1536]{1,0:T(8,128)(2,1)S(1)} %tail.1), channel_id=1, source_target_pairs={{0,2},{2,4},{4,6},{6,8},{8,10},{10,12},{12,14},{14,16},{16,18},{18... | collective-permute-start | bytes 147464 | tf_op jit(solution)/shard_map/ppermute | solution.py:359
  3.7 0.0 copy-start
  3.7 0.0 copy-start.1
  3.7 0.0 copy-start.2
  3.7 0.0 copy-start.3
  3.8 0.0 copy-start.4
  3.8 0.0 copy-start.5
  3.8 4.9 %local.1 = (bf16[384,1024]{1,0:T(8,128)(2,1)S(1)}, bf16[384,256]{1,0:T(8,128)(2,1)S(1)}, bf16[384,256]{1,0:T(8,128)(2,1)S(1)}, f32[16,384]{1,0:T(8,128)S(1)}, f3...) custom-call(bf16[384,1024]{1,0:T(8,128)(2,1)} %values.3, ...), custom_call_target="tpu_custom_call" | custom-call | flops 4000000000 | bytes 4000000 | tf_op jit(solution)/shard_map/local/pallas_call | solution.py:386
  8.7 0.0 collective-permute-done.halo
  8.7 0.0 copy-start.7
  8.7 0.4 edge.1
  9.1 1.1 %collective-permute-start.1 = (bf16[144,256]{1,0:T(8,128)(2,1)S(1)}, bf16[144,256]{1,0:T(8,128)(2,1)S(1)}, u32[]{:S(2)}, u32[]{:S(2)}) collective-permute-start(bf16[144,256]{1,0:T(8,128)(2,1)S(1)} %get-tuple-element.47), channel_id=1, source_target_pairs={{0,2},{2,0},{4,6},{6,4},{8,10},{10,8},{12,14},{14,12},{16,18},{18,... | collective-permute-start | bytes 221192 | tf_op jit(solution)/shard_map/ppermute | solution.py:359
  10.2 0.8 %collective-permute-start.2 = (bf16[144,256]{1,0:T(8,128)(2,1)S(1)}, bf16[144,256]{1,0:T(8,128)(2,1)S(1)}, u32[]{:S(2)}, u32[]{:S(2)}) collective-permute-start(bf16[144,256]{1,0:T(8,128)(2,1)S(1)} %get-tuple-element.48), channel_id=1, source_target_pairs={{0,4},{2,6},{4,0},{6,2},{8,12},{10,14},{12,8},{14,10},{16,20},{18,... | collective-permute-start | bytes 221192 | tf_op jit(solution)/shard_map/ppermute | solution.py:359
  11.0 1.8 %collective-permute-start.3 = (bf16[144,256]{1,0:T(8,128)(2,1)S(1)}, bf16[144,256]{1,0:T(8,128)(2,1)S(1)}, u32[]{:S(2)}, u32[]{:S(2)}) collective-permute-start(bf16[144,256]{1,0:T(8,128)(2,1)S(1)} %get-tuple-element.49), channel_id=1, source_target_pairs={{0,6},{2,4},{4,2},{6,0},{8,14},{10,12},{12,10},{14,8},{16,22},{18,... | collective-permute-start | bytes 221192 | tf_op jit(solution)/shard_map/ppermute | solution.py:359
  12.8 2.3 %collective-permute-done.2.r2.refs_10_ = bf16[144,256]{1,0:T(8,128)(2,1)S(1)} collective-permute-done((bf16[144,256]{1,0:T(8,128)(2,1)S(1)}, bf16[144,256]{1,0:T(8,128)(2,1)S(1)}, u32[]{:S(2)}, u32[]{:S(2)}) %collective-permute-start.2) | collective-permute-done | bytes 73760 | tf_op jit(solution)/shard_map/ppermute | solution.py:359
  15.1 1.7 %collective-permute-done.3.r3.refs_11_ = bf16[144,256]{1,0:T(8,128)(2,1)S(1)} collective-permute-done((bf16[144,256]{1,0:T(8,128)(2,1)S(1)}, bf16[144,256]{1,0:T(8,128)(2,1)S(1)}, u32[]{:S(2)}, u32[]{:S(2)}) %collective-permute-start.3) | collective-permute-done | bytes 73760 | tf_op jit(solution)/shard_map/ppermute | solution.py:359
  16.8 0.1 shard_map.129
  16.9 0.7 collective-permute-start.4
  17.6 0.0 collective-permute-done.4.refs_0_
  17.6 0.7 collective-permute-start.5
  18.3 0.0 collective-permute-done.5.refs_0_.refs_1_
  18.3 0.7 collective-permute-start.6
  19.0 1.3 %collective-permute-start.9 = (bf16[144,256]{1,0:T(8,128)(2,1)S(1)}, bf16[144,256]{1,0:T(8,128)(2,1)S(1)}, u32[]{:S(2)}, u32[]{:S(2)}) collective-permute-start(bf16[144,256]{1,0:T(8,128)(2,1)S(1)} %get-tuple-element.50), channel_id=1, source_target_pairs={{32,40},{34,42},{36,44},{38,46},{48,56},{50,58},{52,60},{54,62},{3... | collective-permute-start | bytes 221192 | tf_op jit(solution)/shard_map/ppermute | solution.py:359
  20.3 0.0 collective-permute-done.6.refs_0_.refs_2_
  20.3 0.7 collective-permute-start.7
  21.0 0.7 collective-permute-start.8
  21.7 6.3 %collective-permute-done.9.last.refs_7_ = bf16[144,256]{1,0:T(8,128)(2,1)S(1)} collective-permute-done((bf16[144,256]{1,0:T(8,128)(2,1)S(1)}, bf16[144,256]{1,0:T(8,128)(2,1)S(1)}, u32[]{:S(2)}, u32[]{:S(2)}) %collective-permute-start.9) | collective-permute-done | bytes 73760 | tf_op jit(solution)/shard_map/ppermute | solution.py:359
  28.0 0.0 collective-permute-done.7.before.refs_3_
  28.0 1.3 %collective-permute-start.10 = (bf16[128,256]{1,0:T(8,128)(2,1)S(1)}, bf16[128,256]{1,0:T(8,128)(2,1)S(1)}, u32[]{:S(2)}, u32[]{:S(2)}) collective-permute-start(bf16[128,256]{1,0:T(8,128)(2,1)S(1)} %shard_map.133), channel_id=1, source_target_pairs={{40,56},{42,58},{44,60},{46,62},{41,57},{43,59},{45,61},{47,63},{1... | collective-permute-start | bytes 196616 | tf_op jit(solution)/shard_map/ppermute | solution.py:359
  29.3 0.7 collective-permute-start.11
  30.0 0.0 copy-start.8
  30.0 0.6 shard_map.127
  30.6 0.1 copy-done.8
  30.7 0.0 collective-permute-done.8.refs_4_
  30.7 12.8 %collective-permute-done.10.refs_5_ = bf16[128,256]{1,0:T(8,128)(2,1)S(1)} collective-permute-done((bf16[128,256]{1,0:T(8,128)(2,1)S(1)}, bf16[128,256]{1,0:T(8,128)(2,1)S(1)}, u32[]{:S(2)}, u32[]{:S(2)}) %collective-permute-start.10) | collective-permute-done | bytes 65568 | tf_op jit(solution)/shard_map/ppermute | solution.py:359
  43.5 0.2 shard_map.134
  43.7 5.2 %collective-permute-start.12 = (bf16[128,256]{1,0:T(8,128)(2,1)S(1)}, bf16[128,256]{1,0:T(8,128)(2,1)S(1)}, u32[]{:S(2)}, u32[]{:S(2)}) collective-permute-start(bf16[128,256]{1,0:T(8,128)(2,1)S(1)} %get-tuple-element.54), channel_id=1, source_target_pairs={{0,2},{2,0},{4,6},{6,4},{8,10},{10,8},{12,14},{14,12},{16,18},{18,... | collective-permute-start | bytes 196616 | tf_op jit(solution)/shard_map/ppermute | solution.py:359
  48.9 7.9 %collective-permute-start.13 = (bf16[128,256]{1,0:T(8,128)(2,1)S(1)}, bf16[128,256]{1,0:T(8,128)(2,1)S(1)}, u32[]{:S(2)}, u32[]{:S(2)}) collective-permute-start(bf16[128,256]{1,0:T(8,128)(2,1)S(1)} %get-tuple-element.55), channel_id=1, source_target_pairs={{0,4},{2,6},{4,0},{6,2},{8,12},{10,14},{12,8},{14,10},{16,20},{18,... | collective-permute-start | bytes 196616 | tf_op jit(solution)/shard_map/ppermute | solution.py:359
  56.9 1.0 %collective-permute-start.14 = (bf16[128,256]{1,0:T(8,128)(2,1)S(1)}, bf16[128,256]{1,0:T(8,128)(2,1)S(1)}, u32[]{:S(2)}, u32[]{:S(2)}) collective-permute-start(bf16[128,256]{1,0:T(8,128)(2,1)S(1)} %get-tuple-element.56), channel_id=1, source_target_pairs={{0,6},{2,4},{4,2},{6,0},{8,14},{10,12},{12,10},{14,8},{16,22},{18,... | collective-permute-start | bytes 196616 | tf_op jit(solution)/shard_map/ppermute | solution.py:359
  57.9 2.6 %shard_map.128 = (f32[384,1024]{1,0:T(8,128)S(1)}, bf16[384,256]{1,0:T(8,128)(2,1)S(1)}) custom-call(bf16[384,1024]{1,0:T(8,128)(2,1)S(1)} %get-tuple-element.31.x_act, bf16[384,256]{1,0:T(8,128)(2,1)S(1)} %get-tuple-element.32.b_act, bf16[384,256]{1,0:T(8,128)(2,1)S(1)} %get-tuple-element.33.c_act, bf16[16,1024]{1,0:T(8,128)(2,1)S(1)} %get-tuple-element.37.edge_x, ...), custom_call_target="tpu_custom_call" | custom-call | flops 4000000000 | bytes 2850816 | tf_op jit(solution)/shard_map/pallas_call | solution.py:153
  60.5 0.0 collective-permute-done.12.p1
  60.5 1.6 %collective-permute-done.14.p3 = bf16[128,256]{1,0:T(8,128)(2,1)S(1)} collective-permute-done((bf16[128,256]{1,0:T(8,128)(2,1)S(1)}, bf16[128,256]{1,0:T(8,128)(2,1)S(1)}, u32[]{:S(2)}, u32[]{:S(2)}) %collective-permute-start.14) | collective-permute-done | bytes 65568 | tf_op jit(solution)/shard_map/ppermute | solution.py:359
  62.0 1.6 %shard_map.136 = bf16[192,2048]{1,0:T(8,128)(2,1)S(1)} custom-call(f32[384,1024]{1,0:T(8,128)S(1)} %get-tuple-element.43.y_in, f32[384,1024]{1,0:T(8,128)S(1)} %get-tuple-element.44.grow, bf16[384,256]{1,0:T(8,128)(2,1)S(1)} %get-tuple-element.45.c_all, bf16[1,1024]{1,0:T(2,128)(2,1)S(1)} %reshape.12.gain, bf16[128,256]{1,0:T(8,128)(2,1)S(1)} %get-tuple-element.53.p0, ...), custom_call_target="tpu_custom_call" | custom-call | flops 4000000000 | bytes 7800832 | tf_op jit(solution)/shard_map/pallas_call | solution.py:153
  63.6 5.4 %collective-permute-start.15 = (bf16[192,2048]{1,0:T(8,128)(2,1)S(1)}, bf16[192,2048]{1,0:T(8,128)(2,1)S(1)}, u32[]{:S(2)}, u32[]{:S(2)}) collective-permute-start(bf16[192,2048]{1,0:T(8,128)(2,1)S(1)} %shard_map.136), channel_id=1, source_target_pairs={{0,1},{1,0},{2,3},{3,2},{4,5},{5,4},{6,7},{7,6},{8,9},{9,8},{10,11... | collective-permute-start | bytes 2359304 | tf_op jit(solution)/shard_map/ppermute | solution.py:475
  69.0 1.6 %shard_map.135.own = f32[192,2048]{1,0:T(8,128)S(1)} custom-call(f32[384,1024]{1,0:T(8,128)S(1)} %get-tuple-element.43.y_in, f32[384,1024]{1,0:T(8,128)S(1)} %get-tuple-element.44.grow, bf16[384,256]{1,0:T(8,128)(2,1)S(1)} %get-tuple-element.45.c_all, bf16[1,1024]{1,0:T(2,128)(2,1)S(1)} %reshape.12.gain, bf16[128,256]{1,0:T(8,128)(2,1)S(1)} %get-tuple-element.53.p0, ...), custom_call_target="tpu_custom_call" | custom-call | flops 4000000000 | bytes 7800832 | tf_op jit(solution)/shard_map/pallas_call | solution.py:153
  70.5 0.3 collective-permute-done.15.other
  70.9 1.0 %shard_map.137 = bf16[192,2048]{1,0:T(8,128)(2,1)} custom-call(f32[192,2048]{1,0:T(8,128)S(1)} %shard_map.135.own, bf16[192,2048]{1,0:T(8,128)(2,1)S(1)} %collective-permute-done.15.other), custom_call_target="tpu_custom_call" | custom-call | bytes 2359296 | tf_op jit(solution)/shard_map/pallas_call | solution.py:153
  (17 shorter events, 0.1 us)
Async XLA Ops:
  0.8 7.8 %collective-permute-start = (bf16[16,1536]{1,0:T(8,128)(2,1)S(1)}, bf16[16,1536]{1,0:T(8,128)(2,1)S(1)}, u32[]{:S(2)}, u32[]{:S(2)}) collective-permute-start(bf16[16,1536]{1,0:T(8,128)(2,1)S(1)} %tail.1), channel_id=1, source_target_pairs={{0,2},{2,4},{4,6},{6,8},{8,10},{10,12},{12,14},{14,16},{16,18},{18... | collective-permute-start | bytes 147464 | tf_op jit(solution)/shard_map/ppermute | solution.py:359
  3.7 5.0 %copy-start = (bf16[384,1024]{1,0:T(8,128)(2,1)S(1)}, bf16[384,1024]{1,0:T(8,128)(2,1)}, u32[]{:S(2)}) copy-start(bf16[384,1024]{1,0:T(8,128)(2,1)} %values.3) | copy-start | bytes 2359300
  3.7 5.0 %copy-start.1 = (bf16[384,256]{1,0:T(8,128)(2,1)S(1)}, bf16[384,256]{1,0:T(8,128)(2,1)}, u32[]{:S(2)}) copy-start(bf16[384,256]{1,0:T(8,128)(2,1)} %b_in.3) | copy-start | bytes 589828
  3.7 5.0 %copy-start.2 = (bf16[384,256]{1,0:T(8,128)(2,1)S(1)}, bf16[384,256]{1,0:T(8,128)(2,1)}, u32[]{:S(2)}) copy-start(bf16[384,256]{1,0:T(8,128)(2,1)} %c_in.3) | copy-start | bytes 589828
  3.7 5.0 %copy-start.3 = (bf16[4,1024]{1,0:T(4,128)(2,1)S(1)}, bf16[4,1024]{1,0:T(4,128)(2,1)}, u32[]{:S(2)}) copy-start(bf16[4,1024]{1,0:T(4,128)(2,1)} %conv_x.1) | copy-start | bytes 24580
  3.8 5.0 %copy-start.4 = (bf16[4,256]{1,0:T(4,128)(2,1)S(1)}, bf16[4,256]{1,0:T(4,128)(2,1)}, u32[]{:S(2)}) copy-start(bf16[4,256]{1,0:T(4,128)(2,1)} %conv_b.1) | copy-start | bytes 6148
  3.8 5.0 %copy-start.5 = (bf16[4,256]{1,0:T(4,128)(2,1)S(1)}, bf16[4,256]{1,0:T(4,128)(2,1)}, u32[]{:S(2)}) copy-start(bf16[4,256]{1,0:T(4,128)(2,1)} %conv_c.1) | copy-start | bytes 6148
  8.7 21.3 %copy-start.7 = (bf16[384,1024]{1,0:T(8,128)(2,1)S(1)}, bf16[384,1024]{1,0:T(8,128)(2,1)}, u32[]{:S(2)}) copy-start(bf16[384,1024]{1,0:T(8,128)(2,1)} %gate.1) | copy-start | bytes 2359300
  9.1 3.7 %collective-permute-start.1 = (bf16[144,256]{1,0:T(8,128)(2,1)S(1)}, bf16[144,256]{1,0:T(8,128)(2,1)S(1)}, u32[]{:S(2)}, u32[]{:S(2)}) collective-permute-start(bf16[144,256]{1,0:T(8,128)(2,1)S(1)} %get-tuple-element.47), channel_id=1, source_target_pairs={{0,2},{2,0},{4,6},{6,4},{8,10},{10,8},{12,14},{14,12},{16,18},{18,... | collective-permute-start | bytes 221192 | tf_op jit(solution)/shard_map/ppermute | solution.py:359
  10.2 4.9 %collective-permute-start.2 = (bf16[144,256]{1,0:T(8,128)(2,1)S(1)}, bf16[144,256]{1,0:T(8,128)(2,1)S(1)}, u32[]{:S(2)}, u32[]{:S(2)}) collective-permute-start(bf16[144,256]{1,0:T(8,128)(2,1)S(1)} %get-tuple-element.48), channel_id=1, source_target_pairs={{0,4},{2,6},{4,0},{6,2},{8,12},{10,14},{12,8},{14,10},{16,20},{18,... | collective-permute-start | bytes 221192 | tf_op jit(solution)/shard_map/ppermute | solution.py:359
  11.0 5.8 %collective-permute-start.3 = (bf16[144,256]{1,0:T(8,128)(2,1)S(1)}, bf16[144,256]{1,0:T(8,128)(2,1)S(1)}, u32[]{:S(2)}, u32[]{:S(2)}) collective-permute-start(bf16[144,256]{1,0:T(8,128)(2,1)S(1)} %get-tuple-element.49), channel_id=1, source_target_pairs={{0,6},{2,4},{4,2},{6,0},{8,14},{10,12},{12,10},{14,8},{16,22},{18,... | collective-permute-start | bytes 221192 | tf_op jit(solution)/shard_map/ppermute | solution.py:359
  16.9 0.7 collective-permute-start.4
  17.6 0.7 collective-permute-start.5
  18.3 2.0 %collective-permute-start.6 = (bf16[128,256]{1,0:T(8,128)(2,1)S(1)}, bf16[128,256]{1,0:T(8,128)(2,1)S(1)}, u32[]{:S(2)}, u32[]{:S(2)}) collective-permute-start(bf16[128,256]{1,0:T(8,128)(2,1)S(1)} %shard_map.131), channel_id=1, source_target_pairs={{16,24},{18,26},{20,28},{22,30},{17,25},{19,27},{21,29},{23,31},{8... | collective-permute-start | bytes 196616 | tf_op jit(solution)/shard_map/ppermute | solution.py:359
  19.0 9.0 %collective-permute-start.9 = (bf16[144,256]{1,0:T(8,128)(2,1)S(1)}, bf16[144,256]{1,0:T(8,128)(2,1)S(1)}, u32[]{:S(2)}, u32[]{:S(2)}) collective-permute-start(bf16[144,256]{1,0:T(8,128)(2,1)S(1)} %get-tuple-element.50), channel_id=1, source_target_pairs={{32,40},{34,42},{36,44},{38,46},{48,56},{50,58},{52,60},{54,62},{3... | collective-permute-start | bytes 221192 | tf_op jit(solution)/shard_map/ppermute | solution.py:359
  20.3 7.7 %collective-permute-start.7 = (bf16[128,256]{1,0:T(8,128)(2,1)S(1)}, bf16[128,256]{1,0:T(8,128)(2,1)S(1)}, u32[]{:S(2)}, u32[]{:S(2)}) collective-permute-start(bf16[128,256]{1,0:T(8,128)(2,1)S(1)} %shard_map.132), channel_id=1, source_target_pairs={{24,40},{26,42},{28,44},{30,46},{25,41},{27,43},{29,45},{31,47},{8... | collective-permute-start | bytes 196616 | tf_op jit(solution)/shard_map/ppermute | solution.py:359
  21.0 9.7 %collective-permute-start.8 = (bf16[128,256]{1,0:T(8,128)(2,1)S(1)}, bf16[128,256]{1,0:T(8,128)(2,1)S(1)}, u32[]{:S(2)}, u32[]{:S(2)}) collective-permute-start(bf16[128,256]{1,0:T(8,128)(2,1)S(1)} %shard_map.132), channel_id=1, source_target_pairs={{24,32},{26,34},{28,36},{30,38},{25,33},{27,35},{29,37},{31,39},{8... | collective-permute-start | bytes 196616 | tf_op jit(solution)/shard_map/ppermute | solution.py:359
  28.0 15.5 %collective-permute-start.10 = (bf16[128,256]{1,0:T(8,128)(2,1)S(1)}, bf16[128,256]{1,0:T(8,128)(2,1)S(1)}, u32[]{:S(2)}, u32[]{:S(2)}) collective-permute-start(bf16[128,256]{1,0:T(8,128)(2,1)S(1)} %shard_map.133), channel_id=1, source_target_pairs={{40,56},{42,58},{44,60},{46,62},{41,57},{43,59},{45,61},{47,63},{1... | collective-permute-start | bytes 196616 | tf_op jit(solution)/shard_map/ppermute | solution.py:359
  29.3 14.2 %collective-permute-start.11 = (bf16[128,256]{1,0:T(8,128)(2,1)S(1)}, bf16[128,256]{1,0:T(8,128)(2,1)S(1)}, u32[]{:S(2)}, u32[]{:S(2)}) collective-permute-start(bf16[128,256]{1,0:T(8,128)(2,1)S(1)} %shard_map.133), channel_id=1, source_target_pairs={{40,48},{42,50},{44,52},{46,54},{41,49},{43,51},{45,53},{47,55},{1... | collective-permute-start | bytes 196616 | tf_op jit(solution)/shard_map/ppermute | solution.py:359
  30.0 0.7 copy-start.8
  43.7 16.8 %collective-permute-start.12 = (bf16[128,256]{1,0:T(8,128)(2,1)S(1)}, bf16[128,256]{1,0:T(8,128)(2,1)S(1)}, u32[]{:S(2)}, u32[]{:S(2)}) collective-permute-start(bf16[128,256]{1,0:T(8,128)(2,1)S(1)} %get-tuple-element.54), channel_id=1, source_target_pairs={{0,2},{2,0},{4,6},{6,4},{8,10},{10,8},{12,14},{14,12},{16,18},{18,... | collective-permute-start | bytes 196616 | tf_op jit(solution)/shard_map/ppermute | solution.py:359
  48.9 11.6 %collective-permute-start.13 = (bf16[128,256]{1,0:T(8,128)(2,1)S(1)}, bf16[128,256]{1,0:T(8,128)(2,1)S(1)}, u32[]{:S(2)}, u32[]{:S(2)}) collective-permute-start(bf16[128,256]{1,0:T(8,128)(2,1)S(1)} %get-tuple-element.55), channel_id=1, source_target_pairs={{0,4},{2,6},{4,0},{6,2},{8,12},{10,14},{12,8},{14,10},{16,20},{18,... | collective-permute-start | bytes 196616 | tf_op jit(solution)/shard_map/ppermute | solution.py:359
  56.9 5.2 %collective-permute-start.14 = (bf16[128,256]{1,0:T(8,128)(2,1)S(1)}, bf16[128,256]{1,0:T(8,128)(2,1)S(1)}, u32[]{:S(2)}, u32[]{:S(2)}) collective-permute-start(bf16[128,256]{1,0:T(8,128)(2,1)S(1)} %get-tuple-element.56), channel_id=1, source_target_pairs={{0,6},{2,4},{4,2},{6,0},{8,14},{10,12},{12,10},{14,8},{16,22},{18,... | collective-permute-start | bytes 196616 | tf_op jit(solution)/shard_map/ppermute | solution.py:359
  57.9 4.1 %copy-start.6 = (bf16[1024,2048]{1,0:T(8,128)(2,1)S(1)}, bf16[1024,2048]{1,0:T(8,128)(2,1)}, u32[]{:S(2)}) copy-start(bf16[1024,2048]{1,0:T(8,128)(2,1)} %w_out.3) | copy-start | bytes 12582916
  63.6 7.3 %collective-permute-start.15 = (bf16[192,2048]{1,0:T(8,128)(2,1)S(1)}, bf16[192,2048]{1,0:T(8,128)(2,1)S(1)}, u32[]{:S(2)}, u32[]{:S(2)}) collective-permute-start(bf16[192,2048]{1,0:T(8,128)(2,1)S(1)} %shard_map.136), channel_id=1, source_target_pairs={{0,1},{1,0},{2,3},{3,2},{4,5},{5,4},{6,7},{7,6},{8,9},{9,8},{10,11... | collective-permute-start | bytes 2359304 | tf_op jit(solution)/shard_map/ppermute | solution.py:475

commit v2 on v1

--- a/solution.py
+++ b/solution.py
@@ -57,7 +57,8 @@
 
 
 def silu(x):
-    return x / (1.0 + jnp.exp(-x))
+    half = 0.5 * x
+    return half + half * jnp.tanh(half)
 
 
 def convolved(ext, first, rows, taps):
@@ -69,7 +70,7 @@
 
 def local_kernel(
     values_hbm, b_hbm, c_hbm, step_hbm, extra_hbm, conv_x_hbm, conv_b_hbm, conv_c_hbm, dt_hbm, rate_hbm,
-    x_act, b_act, c_act, cum_out, step_out, state_out, logs_out, edge_weight,
+    x_act, b_act, c_act, cum_out, step_out, state_out, logs_out, edge_weight, head, tail,
     ext, values, b_in, c_in, step_in, extra, conv_x, conv_b, conv_c, dt_bias, rate, sems,
 ):
     sources = (step_hbm, extra_hbm, dt_hbm, rate_hbm, b_hbm, conv_b_hbm, c_hbm, conv_c_hbm, values_hbm, conv_x_hbm)
@@ -103,9 +104,13 @@
     width = ext.shape[1]
     ext[0:8, :] = jnp.zeros((8, width), F32)
     per_group = inner // (b_in.shape[1] // STATE)
+    offset = 0
     for turn, (source, taps, target) in enumerate(((b_in, conv_b, b_act), (c_in, conv_c, c_act), (values, conv_x, x_act))):
         for copy in copies[4 + 2 * turn : 6 + 2 * turn]:
             copy.wait()
+        head[:, offset : offset + source.shape[1]] = source[0:EDGE, :]
+        tail[:, offset : offset + source.shape[1]] = source[span - EDGE :, :]
+        offset += source.shape[1]
         for start in range(0, source.shape[1], width):
             lanes = slice(start, start + width)
             ext[8 : 8 + span, :] = source[:, lanes].astype(F32)
@@ -118,18 +123,17 @@
 
 
 def edge_kernel(
-    values, b_in, c_in, halo, conv_x, conv_b, conv_c, state_in, logs_in, edge_weight,
+    head, halo, conv_x, conv_b, conv_c, state_in, logs_in, edge_weight,
     edge_x, edge_b, edge_c, slot0, slot1, slot2, slot3, ext, packed,
 ):
-    inner, shared = values.shape[1], b_in.shape[1]
+    inner, shared = edge_x.shape[1], edge_b.shape[1]
+    ext[0:EDGE, :] = halo[...].astype(F32)
+    ext[EDGE : 2 * EDGE, :] = head[...].astype(F32)
     offset = 0
-    for source, taps, target in ((b_in, conv_b, edge_b), (c_in, conv_c, edge_c), (values, conv_x, edge_x)):
-        lanes = slice(offset, offset + source.shape[1])
-        part = ext.at[:, lanes]
-        part[0:EDGE, :] = halo[:, lanes].astype(F32)
-        part[EDGE : 2 * EDGE, :] = source[...].astype(F32)
-        target[...] = convolved(part, EDGE - (CONV - 1), EDGE, taps[...])
-        offset += source.shape[1]
+    for taps, target in ((conv_b, edge_b), (conv_c, edge_c), (conv_x, edge_x)):
+        lanes = slice(offset, offset + target.shape[1])
+        target[...] = convolved(ext.at[:, lanes], EDGE - (CONV - 1), EDGE, taps[...])
+        offset += target.shape[1]
     groups = shared // STATE
     weighted = (edge_x[...].astype(F32) * edge_weight[...]).astype(BF16)
     for group in range(groups):
@@ -180,12 +184,13 @@
     ref[STATE:, :] = logs.astype(BF16)
 
 
-def quad_total_kernel(own, r1, r2, r3, sent, state_out, log_out, ordered):
+def quad_total_kernel(own, r1, r2, r3, first, sent, state_out, log_out, ordered):
     quad_order(ordered, (own, r1, r2, r3))
     state, log = load(ordered.at[0])
     for place in range(1, QUAD):
         part, part_log = load(ordered.at[place])
         state, log = state * jnp.exp(part_log) + part, log + part_log
+    first[...] = state.astype(BF16)
     store(sent, state, log)
     state_out[...] = state
     log_out[...] = log
@@ -199,6 +204,14 @@
             part, log = load(last)
             state = state * jnp.exp(log) + part
         out[...] = (state * jnp.exp(total_log[...]) + total[...]).astype(BF16)
+
+
+def choose_kernel(fours, *refs):
+    for four, ref in zip(fours, refs, strict=False):
+
+        @pl.when(lax.axis_index("sp") // QUAD == four)
+        def _(ref=ref):
+            refs[-1][...] = ref[...]
 
 
 def prefix_kernel(targets, *refs):
@@ -331,18 +344,6 @@
     out[...] = (own[...] + other[...].astype(F32)).astype(BF16)
 
 
-def tail_kernel(values, b_in, c_in, out, sems):
-    offset, copies = 0, []
-    for turn, source in enumerate((b_in, c_in, values)):
-        rows, lanes = pl.ds(source.shape[0] - EDGE, EDGE), pl.ds(offset, source.shape[1])
-        copies.append(pltpu.make_async_copy(source.at[rows, :], out.at[:, lanes], sems.at[turn]))
-        offset += source.shape[1]
-    for copy in copies:
-        copy.start()
-    for copy in copies:
-        copy.wait()
-
-
 def body(
     gate_in, values_in, input_state_in, output_state_in, step_in, conv_x, conv_b, conv_c, dt_bias, decay_rate, log_decay_extra,
     out_gain, w_out,
@@ -361,20 +362,6 @@
     def exchange(x, bits, count=places):
         return move(x, [(i, i ^ bits) for i in range(count)])
 
-    def edge_specs(block):
-        return [pl.BlockSpec((EDGE, a.shape[1]), lambda i: (block, 0)) for a in (values_in, input_state_in, output_state_in)]
-
-    tail = pl.pallas_call(
-        tail_kernel,
-        out_shape=shape((EDGE, inner + 2 * shared), BF16),
-        in_specs=[pl.BlockSpec(memory_space=pl.ANY)] * 3,
-        out_specs=whole(1)[0],
-        scratch_shapes=[pltpu.SemaphoreType.DMA((3,))],
-        compiler_params=pltpu.CompilerParams(vmem_limit_bytes=SMALL),
-        name="tail",
-    )(*(pltpu.with_memory_space_constraint(a, pltpu.HBM) for a in (values_in, input_state_in, output_state_in)))
-    halo = move(tail, [(i, i + 1) for i in range(places - 1)])
-
     args = [
         values_in, input_state_in, output_state_in, step_in.T, log_decay_extra.T, conv_x, conv_b, conv_c,
         dt_bias.reshape(1, heads), decay_rate.reshape(1, heads),
@@ -382,8 +369,9 @@
     outs = [
         shape((span, inner), BF16), shape((span, shared), BF16), shape((span, shared), BF16), shape((heads, span), F32),
         shape((heads, span), F32), shape((STATE, inner), F32), shape((EXTRA, inner), BF16), shape((EDGE, inner), F32),
+        shape((EDGE, inner + 2 * shared), BF16), shape((EDGE, inner + 2 * shared), BF16),
     ]
-    x_act, b_act, c_act, cum, step, state, logs, edge_weight = pl.pallas_call(
+    x_act, b_act, c_act, cum, step, state, logs, edge_weight, head, tail = pl.pallas_call(
         local_kernel,
         out_shape=outs,
         in_specs=[pl.BlockSpec(memory_space=pltpu.HBM)] * len(args),
@@ -393,19 +381,18 @@
         cost_estimate=pl.CostEstimate(flops=FILL, bytes_accessed=4_000_000, transcendentals=0),
         name="local",
     )(*(pltpu.with_memory_space_constraint(a, pltpu.HBM) for a in args))
+    halo = move(tail, [(i, i + 1) for i in range(places - 1)])
     payload = shape((STATE + EXTRA, quarter), BF16)
-    edge_x, edge_b, edge_c, *slots = pl.pallas_call(
+    edge_x, edge_b, edge_c, *slots = local_call(
         edge_kernel,
-        out_shape=[
+        [
             shape((EDGE, inner), BF16), shape((EDGE, shared), BF16), shape((EDGE, shared), BF16), payload, payload, payload, payload,
         ],
-        grid=(1,),
-        in_specs=edge_specs(0) + whole(7),
-        out_specs=whole(7),
-        scratch_shapes=[vmem((2 * EDGE, inner + 2 * shared), F32), vmem((STATE + EXTRA, inner), BF16)],
-        compiler_params=pltpu.CompilerParams(vmem_limit_bytes=SMALL),
-        name="edge",
-    )(values_in, input_state_in, output_state_in, halo, conv_x, conv_b, conv_c, state, logs, edge_weight)
+        [head, halo, conv_x, conv_b, conv_c, state, logs, edge_weight],
+        [vmem((2 * EDGE, inner + 2 * shared), F32), vmem((STATE + EXTRA, inner), BF16)],
+        limit=SMALL,
+    )
+
     gate, grow = local_call(gate_kernel, [shape((span, inner), F32)] * 2, [gate_in, cum], flops=FILL)
     y_inside, c_all = local_call(
         inside_kernel,
@@ -423,7 +410,7 @@
     quad = [slots[0], arrived[1], arrived[2], arrived[3]]
     slice_of = shape((STATE, quarter), BF16)
     kept = [shape((STATE, quarter), F32), shape((1, quarter), F32)]
-    sent, total, log = local_call(quad_total_kernel, [payload, *kept], quad, [order], limit=SMALL)
+    first, sent, total, log = local_call(quad_total_kernel, [slice_of, payload, *kept], quad, [order], limit=SMALL)
     fours = places // QUAD
     half = fours // 2
 
@@ -444,15 +431,18 @@
         targets.append(four + distance)
         return arrived[-1]
 
-    before = send(sent, 0, 1)
+    before = send(first, 0, 1)
     for four in range(1, half - 1):
         before = send(jump(four, before), four, 1)
-    lower = jump(half - 1, before)
-    for four in range(half - 1, fours - 1, 2):
-        before = send(lower, four, 2)
-        send(lower, four, 1)
-        if four + 2 < fours - 1:
-            lower = jump(four + 2, before, pairs)
+    senders, values = list(range(half - 1, fours - 1, 2)), []
+    for four in senders:
+        values.append(jump(four, before, pairs if values else None))
+        before = send(values[-1], four, 2)
+    chosen = local_call(functools.partial(choose_kernel, tuple(senders)), slice_of, values, limit=SMALL)
+    side = up(chosen, senders, 1)
+    for four in senders:
+        arrived.append(side)
+        targets.append(four + 1)
     ends = local_call(
         functools.partial(prefix_kernel, tuple(targets)),
         [slice_of] * QUAD,

time: 72.2 us -> 73.3 us (1.015)
  the two profiles are of different devices: /device:TPU:1831 before, /device:TPU:2021 now
where the time goes in v2:
time: 73.3 us; the launch traced here: 71.8 us
  starting transfers between devices  31.7 us (43%)
  waiting for transfers between devices  27 us (37%)
  Pallas kernels  12.6 us (17%)
    ppermute x14, waiting for transfers between devices, move(): return lax.ppermute(x, 'sp', route)  26.7 us
    ppermute x14, starting transfers between devices, move(): return lax.ppermute(x, 'sp', route)  20.1 us
    ppermute x1, starting transfers between devices, body(): other = lax.ppermute(theirs, 'tp', [(0, 1), (1, 0)])  11.7 us
    pallas_call x13, Pallas kernels, local_call(): pl.pallas_call(kernel, out_shape=outs, in_specs=whole(len(args)), out_spe...  7.86 us
    pallas_call x1, Pallas kernels, body(): pl.pallas_call(local_kernel, out_shape=outs, in_specs=[pl.BlockSpec(memor...  4.75 us
  transfers between devices with their start and end apart: 15, of which 7 were waited for; matrix products, arithmetic and copies ran while one was open for 0% of the time, Pallas kernels for 6%

profile of v2, /device:TPU:2021, one launch (start us, length us, event | category | flops | bytes accessed | tf_op | source)
XLA Modules:
  0.0 71.8 jit_solution(12227482281581846263)
XLA Ops:
  0.0 0.0 copy-start
  0.0 4.7 %local.1 = (bf16[384,1024]{1,0:T(8,128)(2,1)S(1)}, bf16[384,256]{1,0:T(8,128)(2,1)S(1)}, bf16[384,256]{1,0:T(8,128)(2,1)S(1)}, f32[16,384]{1,0:T(8,128)S(1)}, f3...) custom-call(bf16[384,1024]{1,0:T(8,128)(2,1)} %values_hbm.1, ...), custom_call_target="tpu_custom_call" | custom-call | flops 4000000000 | bytes 4000000 | tf_op jit(solution)/shard_map/local/pallas_call | solution.py:374
  4.8 0.0 copy-start.4
  4.8 1.4 %collective-permute-start = (bf16[16,1536]{1,0:T(8,128)(2,1)S(1)}, bf16[16,1536]{1,0:T(8,128)(2,1)S(1)}, u32[]{:S(2)}, u32[]{:S(2)}) collective-permute-start(bf16[16,1536]{1,0:T(8,128)(2,1)S(1)} %get-tuple-element.38), channel_id=1, source_target_pairs={{0,2},{2,4},{4,6},{6,8},{8,10},{10,12},{12,14},{14,16},{16,18},{18... | collective-permute-start | bytes 147464 | tf_op jit(solution)/shard_map/ppermute | solution.py:360
  6.2 3.5 %collective-permute-done.halo = bf16[16,1536]{1,0:T(8,128)(2,1)S(1)} collective-permute-done((bf16[16,1536]{1,0:T(8,128)(2,1)S(1)}, bf16[16,1536]{1,0:T(8,128)(2,1)S(1)}, u32[]{:S(2)}, u32[]{:S(2)}) %collective-permute-start) | collective-permute-done | bytes 49184 | tf_op jit(solution)/shard_map/ppermute | solution.py:360
  9.8 0.0 copy-done
  9.8 0.0 copy-done.1
  9.8 0.0 copy-done.2
  9.8 0.4 shard_map.127
  10.2 0.6 collective-permute-start.1
  10.8 2.0 %collective-permute-start.2 = (bf16[144,256]{1,0:T(8,128)(2,1)S(1)}, bf16[144,256]{1,0:T(8,128)(2,1)S(1)}, u32[]{:S(2)}, u32[]{:S(2)}) collective-permute-start(bf16[144,256]{1,0:T(8,128)(2,1)S(1)} %get-tuple-element.53), channel_id=1, source_target_pairs={{0,4},{2,6},{4,0},{6,2},{8,12},{10,14},{12,8},{14,10},{16,20},{18,... | collective-permute-start | bytes 221192 | tf_op jit(solution)/shard_map/ppermute | solution.py:360
  12.8 1.1 %collective-permute-start.3 = (bf16[144,256]{1,0:T(8,128)(2,1)S(1)}, bf16[144,256]{1,0:T(8,128)(2,1)S(1)}, u32[]{:S(2)}, u32[]{:S(2)}) collective-permute-start(bf16[144,256]{1,0:T(8,128)(2,1)S(1)} %get-tuple-element.54), channel_id=1, source_target_pairs={{0,6},{2,4},{4,2},{6,0},{8,14},{10,12},{12,10},{14,8},{16,22},{18,... | collective-permute-start | bytes 221192 | tf_op jit(solution)/shard_map/ppermute | solution.py:360
  13.8 0.0 collective-permute-done.1.r1.refs_9_
  13.8 1.8 %collective-permute-done.2.r2.refs_10_ = bf16[144,256]{1,0:T(8,128)(2,1)S(1)} collective-permute-done((bf16[144,256]{1,0:T(8,128)(2,1)S(1)}, bf16[144,256]{1,0:T(8,128)(2,1)S(1)}, u32[]{:S(2)}, u32[]{:S(2)}) %collective-permute-start.2) | collective-permute-done | bytes 73760 | tf_op jit(solution)/shard_map/ppermute | solution.py:360
  15.7 2.7 %collective-permute-done.3.r3.refs_11_ = bf16[144,256]{1,0:T(8,128)(2,1)S(1)} collective-permute-done((bf16[144,256]{1,0:T(8,128)(2,1)S(1)}, bf16[144,256]{1,0:T(8,128)(2,1)S(1)}, u32[]{:S(2)}, u32[]{:S(2)}) %collective-permute-start.3) | collective-permute-done | bytes 73760 | tf_op jit(solution)/shard_map/ppermute | solution.py:360
  18.4 0.1 shard_map.130
  18.5 0.7 collective-permute-start.4
  19.2 0.0 collective-permute-done.4.refs_0_
  19.2 0.7 collective-permute-start.5
  19.9 0.0 collective-permute-done.5.refs_0_.refs_1_
  19.9 0.7 collective-permute-start.6
  20.6 1.3 %collective-permute-start.8 = (bf16[144,256]{1,0:T(8,128)(2,1)S(1)}, bf16[144,256]{1,0:T(8,128)(2,1)S(1)}, u32[]{:S(2)}, u32[]{:S(2)}) collective-permute-start(bf16[144,256]{1,0:T(8,128)(2,1)S(1)} %get-tuple-element.58), channel_id=1, source_target_pairs={{32,40},{34,42},{36,44},{38,46},{48,56},{50,58},{52,60},{54,62},{3... | collective-permute-start | bytes 221192 | tf_op jit(solution)/shard_map/ppermute | solution.py:360
  21.9 0.0 collective-permute-done.6.refs_0_.refs_2_
  22.0 0.7 collective-permute-start.7
  22.6 7.0 %collective-permute-done.8.last.refs_7_ = bf16[144,256]{1,0:T(8,128)(2,1)S(1)} collective-permute-done((bf16[144,256]{1,0:T(8,128)(2,1)S(1)}, bf16[144,256]{1,0:T(8,128)(2,1)S(1)}, u32[]{:S(2)}, u32[]{:S(2)}) %collective-permute-start.8) | collective-permute-done | bytes 73760 | tf_op jit(solution)/shard_map/ppermute | solution.py:360
  29.6 0.0 collective-permute-done.7.before.refs_3_
  29.6 1.3 %collective-permute-start.9 = (bf16[128,256]{1,0:T(8,128)(2,1)S(1)}, bf16[128,256]{1,0:T(8,128)(2,1)S(1)}, u32[]{:S(2)}, u32[]{:S(2)}) collective-permute-start(bf16[128,256]{1,0:T(8,128)(2,1)S(1)} %shard_map.134.refs_1_), channel_id=1, source_target_pairs={{40,56},{42,58},{44,60},{46,62},{41,57},{43,59},{45,61},{47,63},{1... | collective-permute-start | bytes 196616 | tf_op jit(solution)/shard_map/ppermute | solution.py:360
  31.0 0.7 collective-permute-start.10
  31.6 0.0 copy-done.4
  31.6 0.0 copy-start.5
  31.6 0.4 shard_map.128
  32.1 0.2 copy-done.5
  32.3 0.0 collective-permute-done.10.refs_5_.refs_6_
  32.3 11.1 %collective-permute-done.9.refs_4_ = bf16[128,256]{1,0:T(8,128)(2,1)S(1)} collective-permute-done((bf16[128,256]{1,0:T(8,128)(2,1)S(1)}, bf16[128,256]{1,0:T(8,128)(2,1)S(1)}, u32[]{:S(2)}, u32[]{:S(2)}) %collective-permute-start.9) | collective-permute-done | bytes 65568 | tf_op jit(solution)/shard_map/ppermute | solution.py:360
  43.4 0.2 shard_map.136
  43.6 6.8 %collective-permute-start.11 = (bf16[128,256]{1,0:T(8,128)(2,1)S(1)}, bf16[128,256]{1,0:T(8,128)(2,1)S(1)}, u32[]{:S(2)}, u32[]{:S(2)}) collective-permute-start(bf16[128,256]{1,0:T(8,128)(2,1)S(1)} %get-tuple-element.60), channel_id=1, source_target_pairs={{0,2},{2,0},{4,6},{6,4},{8,10},{10,8},{12,14},{14,12},{16,18},{18,... | collective-permute-start | bytes 196616 | tf_op jit(solution)/shard_map/ppermute | solution.py:360
  50.4 0.0 collective-permute-start.12
  50.4 2.2 %collective-permute-start.13 = (bf16[128,256]{1,0:T(8,128)(2,1)S(1)}, bf16[128,256]{1,0:T(8,128)(2,1)S(1)}, u32[]{:S(2)}, u32[]{:S(2)}) collective-permute-start(bf16[128,256]{1,0:T(8,128)(2,1)S(1)} %get-tuple-element.62), channel_id=1, source_target_pairs={{0,6},{2,4},{4,2},{6,0},{8,14},{10,12},{12,10},{14,8},{16,22},{18,... | collective-permute-start | bytes 196616 | tf_op jit(solution)/shard_map/ppermute | solution.py:360
  52.6 2.6 %shard_map.129 = (f32[384,1024]{1,0:T(8,128)S(1)}, bf16[384,256]{1,0:T(8,128)(2,1)S(1)}) custom-call(bf16[384,1024]{1,0:T(8,128)(2,1)S(1)} %get-tuple-element.34.x_act, bf16[384,256]{1,0:T(8,128)(2,1)S(1)} %get-tuple-element.35.b_act, bf16[384,256]{1,0:T(8,128)(2,1)S(1)} %get-tuple-element.36.c_act, bf16[16,1024]{1,0:T(8,128)(2,1)S(1)} %get-tuple-element.42.edge_x, ...), custom_call_target="tpu_custom_call" | custom-call | flops 4000000000 | bytes 2850816 | tf_op jit(solution)/shard_map/pallas_call | solution.py:157
  55.2 0.0 collective-permute-done.11.p1
  55.2 0.5 collective-permute-done.12.p2
  55.7 0.0 collective-permute-done.13.p3
  55.7 0.0 copy-done.3
  55.7 1.6 %shard_map.138 = bf16[192,2048]{1,0:T(8,128)(2,1)S(1)} custom-call(f32[384,1024]{1,0:T(8,128)S(1)} %get-tuple-element.48.y_in, f32[384,1024]{1,0:T(8,128)S(1)} %get-tuple-element.49.grow, bf16[384,256]{1,0:T(8,128)(2,1)S(1)} %get-tuple-element.50.c_all, bf16[1,1024]{1,0:T(2,128)(2,1)S(1)} %reshape.12.gain, bf16[128,256]{1,0:T(8,128)(2,1)S(1)} %get-tuple-element.59.p0, ...), custom_call_target="tpu_custom_call" | custom-call | flops 4000000000 | bytes 7800832 | tf_op jit(solution)/shard_map/pallas_call | solution.py:157
  57.3 11.7 %collective-permute-start.14 = (bf16[192,2048]{1,0:T(8,128)(2,1)S(1)}, bf16[192,2048]{1,0:T(8,128)(2,1)S(1)}, u32[]{:S(2)}, u32[]{:S(2)}) collective-permute-start(bf16[192,2048]{1,0:T(8,128)(2,1)S(1)} %shard_map.138), channel_id=1, source_target_pairs={{0,1},{1,0},{2,3},{3,2},{4,5},{5,4},{6,7},{7,6},{8,9},{9,8},{10,11... | collective-permute-start | bytes 2359304 | tf_op jit(solution)/shard_map/ppermute | solution.py:465
  68.9 1.6 %shard_map.137.own = f32[192,2048]{1,0:T(8,128)S(1)} custom-call(f32[384,1024]{1,0:T(8,128)S(1)} %get-tuple-element.48.y_in, f32[384,1024]{1,0:T(8,128)S(1)} %get-tuple-element.49.grow, bf16[384,256]{1,0:T(8,128)(2,1)S(1)} %get-tuple-element.50.c_all, bf16[1,1024]{1,0:T(2,128)(2,1)S(1)} %reshape.12.gain, bf16[128,256]{1,0:T(8,128)(2,1)S(1)} %get-tuple-element.59.p0, ...), custom_call_target="tpu_custom_call" | custom-call | flops 4000000000 | bytes 7800832 | tf_op jit(solution)/shard_map/pallas_call | solution.py:157
  70.5 0.3 collective-permute-done.14.other
  70.8 1.0 %shard_map.139 = bf16[192,2048]{1,0:T(8,128)(2,1)} custom-call(f32[192,2048]{1,0:T(8,128)S(1)} %shard_map.137.own, bf16[192,2048]{1,0:T(8,128)(2,1)S(1)} %collective-permute-done.14.other), custom_call_target="tpu_custom_call" | custom-call | bytes 2359296 | tf_op jit(solution)/shard_map/pallas_call | solution.py:157
  (9 shorter events, 0.1 us)
Async XLA Ops:
  0.0 9.8 %copy-start = (bf16[4,1024]{1,0:T(4,128)(2,1)S(1)}, bf16[4,1024]{1,0:T(4,128)(2,1)}, u32[]{:S(2)}) copy-start(bf16[4,1024]{1,0:T(4,128)(2,1)} %conv_x.1) | copy-start | bytes 24580
  0.0 9.8 %copy-start.1 = (bf16[4,256]{1,0:T(4,128)(2,1)S(1)}, bf16[4,256]{1,0:T(4,128)(2,1)}, u32[]{:S(2)}) copy-start(bf16[4,256]{1,0:T(4,128)(2,1)} %conv_b.1) | copy-start | bytes 6148
  0.0 9.8 %copy-start.2 = (bf16[4,256]{1,0:T(4,128)(2,1)S(1)}, bf16[4,256]{1,0:T(4,128)(2,1)}, u32[]{:S(2)}) copy-start(bf16[4,256]{1,0:T(4,128)(2,1)} %conv_c.1) | copy-start | bytes 6148
  4.8 26.9 %copy-start.4 = (bf16[384,1024]{1,0:T(8,128)(2,1)S(1)}, bf16[384,1024]{1,0:T(8,128)(2,1)}, u32[]{:S(2)}) copy-start(bf16[384,1024]{1,0:T(8,128)(2,1)} %gate.1) | copy-start | bytes 2359300
  4.8 5.0 %collective-permute-start = (bf16[16,1536]{1,0:T(8,128)(2,1)S(1)}, bf16[16,1536]{1,0:T(8,128)(2,1)S(1)}, u32[]{:S(2)}, u32[]{:S(2)}) collective-permute-start(bf16[16,1536]{1,0:T(8,128)(2,1)S(1)} %get-tuple-element.38), channel_id=1, source_target_pairs={{0,2},{2,4},{4,6},{6,8},{8,10},{10,12},{12,14},{14,16},{16,18},{18... | collective-permute-start | bytes 147464 | tf_op jit(solution)/shard_map/ppermute | solution.py:360
  10.2 3.7 %collective-permute-start.1 = (bf16[144,256]{1,0:T(8,128)(2,1)S(1)}, bf16[144,256]{1,0:T(8,128)(2,1)S(1)}, u32[]{:S(2)}, u32[]{:S(2)}) collective-permute-start(bf16[144,256]{1,0:T(8,128)(2,1)S(1)} %get-tuple-element.52), channel_id=1, source_target_pairs={{0,2},{2,0},{4,6},{6,4},{8,10},{10,8},{12,14},{14,12},{16,18},{18,... | collective-permute-start | bytes 221192 | tf_op jit(solution)/shard_map/ppermute | solution.py:360
  10.8 4.9 %collective-permute-start.2 = (bf16[144,256]{1,0:T(8,128)(2,1)S(1)}, bf16[144,256]{1,0:T(8,128)(2,1)S(1)}, u32[]{:S(2)}, u32[]{:S(2)}) collective-permute-start(bf16[144,256]{1,0:T(8,128)(2,1)S(1)} %get-tuple-element.53), channel_id=1, source_target_pairs={{0,4},{2,6},{4,0},{6,2},{8,12},{10,14},{12,8},{14,10},{16,20},{18,... | collective-permute-start | bytes 221192 | tf_op jit(solution)/shard_map/ppermute | solution.py:360
  12.8 5.6 %collective-permute-start.3 = (bf16[144,256]{1,0:T(8,128)(2,1)S(1)}, bf16[144,256]{1,0:T(8,128)(2,1)S(1)}, u32[]{:S(2)}, u32[]{:S(2)}) collective-permute-start(bf16[144,256]{1,0:T(8,128)(2,1)S(1)} %get-tuple-element.54), channel_id=1, source_target_pairs={{0,6},{2,4},{4,2},{6,0},{8,14},{10,12},{12,10},{14,8},{16,22},{18,... | collective-permute-start | bytes 221192 | tf_op jit(solution)/shard_map/ppermute | solution.py:360
  18.5 0.7 collective-permute-start.4
  19.2 0.7 collective-permute-start.5
  19.9 2.0 %collective-permute-start.6 = (bf16[128,256]{1,0:T(8,128)(2,1)S(1)}, bf16[128,256]{1,0:T(8,128)(2,1)S(1)}, u32[]{:S(2)}, u32[]{:S(2)}) collective-permute-start(bf16[128,256]{1,0:T(8,128)(2,1)S(1)} %shard_map.132), channel_id=1, source_target_pairs={{16,24},{18,26},{20,28},{22,30},{17,25},{19,27},{21,29},{23,31},{8... | collective-permute-start | bytes 196616 | tf_op jit(solution)/shard_map/ppermute | solution.py:360
  20.6 9.0 %collective-permute-start.8 = (bf16[144,256]{1,0:T(8,128)(2,1)S(1)}, bf16[144,256]{1,0:T(8,128)(2,1)S(1)}, u32[]{:S(2)}, u32[]{:S(2)}) collective-permute-start(bf16[144,256]{1,0:T(8,128)(2,1)S(1)} %get-tuple-element.58), channel_id=1, source_target_pairs={{32,40},{34,42},{36,44},{38,46},{48,56},{50,58},{52,60},{54,62},{3... | collective-permute-start | bytes 221192 | tf_op jit(solution)/shard_map/ppermute | solution.py:360
  22.0 7.7 %collective-permute-start.7 = (bf16[128,256]{1,0:T(8,128)(2,1)S(1)}, bf16[128,256]{1,0:T(8,128)(2,1)S(1)}, u32[]{:S(2)}, u32[]{:S(2)}) collective-permute-start(bf16[128,256]{1,0:T(8,128)(2,1)S(1)} %shard_map.133.refs_0_), channel_id=1, source_target_pairs={{24,40},{26,42},{28,44},{30,46},{25,41},{27,43},{29,45},{31,47},{8... | collective-permute-start | bytes 196616 | tf_op jit(solution)/shard_map/ppermute | solution.py:360
  29.6 13.7 %collective-permute-start.9 = (bf16[128,256]{1,0:T(8,128)(2,1)S(1)}, bf16[128,256]{1,0:T(8,128)(2,1)S(1)}, u32[]{:S(2)}, u32[]{:S(2)}) collective-permute-start(bf16[128,256]{1,0:T(8,128)(2,1)S(1)} %shard_map.134.refs_1_), channel_id=1, source_target_pairs={{40,56},{42,58},{44,60},{46,62},{41,57},{43,59},{45,61},{47,63},{1... | collective-permute-start | bytes 196616 | tf_op jit(solution)/shard_map/ppermute | solution.py:360
  31.0 1.4 %collective-permute-start.10 = (bf16[128,256]{1,0:T(8,128)(2,1)S(1)}, bf16[128,256]{1,0:T(8,128)(2,1)S(1)}, u32[]{:S(2)}, u32[]{:S(2)}) collective-permute-start(bf16[128,256]{1,0:T(8,128)(2,1)S(1)} %shard_map.135), channel_id=1, source_target_pairs={{24,32},{26,34},{28,36},{30,38},{40,48},{42,50},{44,52},{46,54},{2... | collective-permute-start | bytes 196616 | tf_op jit(solution)/shard_map/ppermute | solution.py:360
  31.6 0.7 copy-start.5
  43.6 11.6 %collective-permute-start.11 = (bf16[128,256]{1,0:T(8,128)(2,1)S(1)}, bf16[128,256]{1,0:T(8,128)(2,1)S(1)}, u32[]{:S(2)}, u32[]{:S(2)}) collective-permute-start(bf16[128,256]{1,0:T(8,128)(2,1)S(1)} %get-tuple-element.60), channel_id=1, source_target_pairs={{0,2},{2,0},{4,6},{6,4},{8,10},{10,8},{12,14},{14,12},{16,18},{18,... | collective-permute-start | bytes 196616 | tf_op jit(solution)/shard_map/ppermute | solution.py:360
  50.4 5.3 %collective-permute-start.12 = (bf16[128,256]{1,0:T(8,128)(2,1)S(1)}, bf16[128,256]{1,0:T(8,128)(2,1)S(1)}, u32[]{:S(2)}, u32[]{:S(2)}) collective-permute-start(bf16[128,256]{1,0:T(8,128)(2,1)S(1)} %get-tuple-element.61), channel_id=1, source_target_pairs={{0,4},{2,6},{4,0},{6,2},{8,12},{10,14},{12,8},{14,10},{16,20},{18,... | collective-permute-start | bytes 196616 | tf_op jit(solution)/shard_map/ppermute | solution.py:360
  50.4 5.3 %collective-permute-start.13 = (bf16[128,256]{1,0:T(8,128)(2,1)S(1)}, bf16[128,256]{1,0:T(8,128)(2,1)S(1)}, u32[]{:S(2)}, u32[]{:S(2)}) collective-permute-start(bf16[128,256]{1,0:T(8,128)(2,1)S(1)} %get-tuple-element.62), channel_id=1, source_target_pairs={{0,6},{2,4},{4,2},{6,0},{8,14},{10,12},{12,10},{14,8},{16,22},{18,... | collective-permute-start | bytes 196616 | tf_op jit(solution)/shard_map/ppermute | solution.py:360
  52.6 3.1 %copy-start.3 = (bf16[1024,2048]{1,0:T(8,128)(2,1)S(1)}, bf16[1024,2048]{1,0:T(8,128)(2,1)}, u32[]{:S(2)}) copy-start(bf16[1024,2048]{1,0:T(8,128)(2,1)} %w_out.3) | copy-start | bytes 12582916
  57.3 13.6 %collective-permute-start.14 = (bf16[192,2048]{1,0:T(8,128)(2,1)S(1)}, bf16[192,2048]{1,0:T(8,128)(2,1)S(1)}, u32[]{:S(2)}, u32[]{:S(2)}) collective-permute-start(bf16[192,2048]{1,0:T(8,128)(2,1)S(1)} %shard_map.138), channel_id=1, source_target_pairs={{0,1},{1,0},{2,3},{3,2},{4,5},{5,4},{6,7},{7,6},{8,9},{9,8},{10,11... | collective-permute-start | bytes 2359304 | tf_op jit(solution)/shard_map/ppermute | solution.py:465

commit v3 on v2

--- a/solution.py
+++ b/solution.py
@@ -70,7 +70,7 @@
 
 def local_kernel(
     values_hbm, b_hbm, c_hbm, step_hbm, extra_hbm, conv_x_hbm, conv_b_hbm, conv_c_hbm, dt_hbm, rate_hbm,
-    x_act, b_act, c_act, cum_out, step_out, state_out, logs_out, edge_weight, head, tail,
+    x_act, b_act, c_act, cum_out, step_out, state_out, logs_out, edge_weight, head,
     ext, values, b_in, c_in, step_in, extra, conv_x, conv_b, conv_c, dt_bias, rate, sems,
 ):
     sources = (step_hbm, extra_hbm, dt_hbm, rate_hbm, b_hbm, conv_b_hbm, c_hbm, conv_c_hbm, values_hbm, conv_x_hbm)
@@ -109,7 +109,6 @@
         for copy in copies[4 + 2 * turn : 6 + 2 * turn]:
             copy.wait()
         head[:, offset : offset + source.shape[1]] = source[0:EDGE, :]
-        tail[:, offset : offset + source.shape[1]] = source[span - EDGE :, :]
         offset += source.shape[1]
         for start in range(0, source.shape[1], width):
             lanes = slice(start, start + width)
@@ -344,6 +343,18 @@
     out[...] = (own[...] + other[...].astype(F32)).astype(BF16)
 
 
+def tail_kernel(values, b_in, c_in, out, sems):
+    offset, copies = 0, []
+    for turn, source in enumerate((b_in, c_in, values)):
+        rows, lanes = pl.ds(source.shape[0] - EDGE, EDGE), pl.ds(offset, source.shape[1])
+        copies.append(pltpu.make_async_copy(source.at[rows, :], out.at[:, lanes], sems.at[turn]))
+        offset += source.shape[1]
+    for copy in copies:
+        copy.start()
+    for copy in copies:
+        copy.wait()
+
+
 def body(
     gate_in, values_in, input_state_in, output_state_in, step_in, conv_x, conv_b, conv_c, dt_bias, decay_rate, log_decay_extra,
     out_gain, w_out,
@@ -362,6 +373,16 @@
     def exchange(x, bits, count=places):
         return move(x, [(i, i ^ bits) for i in range(count)])
 
+    tail = pl.pallas_call(
+        tail_kernel,
+        out_shape=shape((EDGE, inner + 2 * shared), BF16),
+        in_specs=[pl.BlockSpec(memory_space=pl.ANY)] * 3,
+        out_specs=whole(1)[0],
+        scratch_shapes=[pltpu.SemaphoreType.DMA((3,))],
+        compiler_params=pltpu.CompilerParams(vmem_limit_bytes=SMALL),
+        name="tail",
+    )(*(pltpu.with_memory_space_constraint(a, pltpu.HBM) for a in (values_in, input_state_in, output_state_in)))
+    halo = move(tail, [(i, i + 1) for i in range(places - 1)])
     args = [
         values_in, input_state_in, output_state_in, step_in.T, log_decay_extra.T, conv_x, conv_b, conv_c,
         dt_bias.reshape(1, heads), decay_rate.reshape(1, heads),
@@ -369,9 +390,9 @@
     outs = [
         shape((span, inner), BF16), shape((span, shared), BF16), shape((span, shared), BF16), shape((heads, span), F32),
         shape((heads, span), F32), shape((STATE, inner), F32), shape((EXTRA, inner), BF16), shape((EDGE, inner), F32),
-        shape((EDGE, inner + 2 * shared), BF16), shape((EDGE, inner + 2 * shared), BF16),
+        shape((EDGE, inner + 2 * shared), BF16),
     ]
-    x_act, b_act, c_act, cum, step, state, logs, edge_weight, head, tail = pl.pallas_call(
+    x_act, b_act, c_act, cum, step, state, logs, edge_weight, head = pl.pallas_call(
         local_kernel,
         out_shape=outs,
         in_specs=[pl.BlockSpec(memory_space=pltpu.HBM)] * len(args),
@@ -381,7 +402,6 @@
         cost_estimate=pl.CostEstimate(flops=FILL, bytes_accessed=4_000_000, transcendentals=0),
         name="local",
     )(*(pltpu.with_memory_space_constraint(a, pltpu.HBM) for a in args))
-    halo = move(tail, [(i, i + 1) for i in range(places - 1)])
     payload = shape((STATE + EXTRA, quarter), BF16)
     edge_x, edge_b, edge_c, *slots = local_call(
         edge_kernel,
@@ -417,6 +437,13 @@
     def up(x, sources, distance):
         return move(x, [(i, i + distance * QUAD) for four in sources for i in range(four * QUAD, (four + 1) * QUAD)])
 
+    def swap(x, four):
+        first, route = four * QUAD, []
+        for i in range(places):
+            moved = i + QUAD if first <= i < first + QUAD else i - QUAD if first + QUAD <= i < first + 2 * QUAD else i
+            route.append((i, moved))
+        return move(x, route)
+
     def jump(four, before, last=None):
         if last is None:
             kernel = lambda *refs: jump_kernel(four, refs[0], None, *refs[1:])
@@ -427,7 +454,7 @@
     arrived, targets = [], []
 
     def send(x, four, distance):
-        arrived.append(up(x, (four,), distance))
+        arrived.append(swap(x, four) if distance == 1 else up(x, (four,), distance))
         targets.append(four + distance)
         return arrived[-1]
 

time: 73.3 us -> 73.8 us (level)
  the two profiles are of different devices: /device:TPU:2021 before, /device:TPU:1829 now
where the time goes in v3:
time: 73.8 us; the launch traced here: 73.5 us
  starting transfers between devices  32.5 us (44%)
  waiting for transfers between devices  27.1 us (37%)
  Pallas kernels  13.4 us (18%)
    ppermute x14, waiting for transfers between devices, move(): return lax.ppermute(x, 'sp', route)  26.7 us
    ppermute x14, starting transfers between devices, move(): return lax.ppermute(x, 'sp', route)  19.3 us
    ppermute x1, starting transfers between devices, body(): other = lax.ppermute(theirs, 'tp', [(0, 1), (1, 0)])  13.2 us
    pallas_call x13, Pallas kernels, local_call(): pl.pallas_call(kernel, out_shape=outs, in_specs=whole(len(args)), out_spe...  7.87 us
    pallas_call x1, Pallas kernels, body(): pl.pallas_call(local_kernel, out_shape=outs, in_specs=[pl.BlockSpec(memor...  4.73 us
  transfers between devices with their start and end apart: 15, of which 6 were waited for; matrix products, arithmetic and copies ran while one was open for 0% of the time, Pallas kernels for 13%

profile of v3, /device:TPU:1829, one launch (start us, length us, event | category | flops | bytes accessed | tf_op | source)
XLA Modules:
  0.0 73.5 jit_solution(9417179188032339459)
XLA Ops:
  0.0 0.8 %tail.1 = bf16[16,1536]{1,0:T(8,128)(2,1)S(1)} custom-call(bf16[384,1024]{1,0:T(8,128)(2,1)} %values.1, bf16[384,256]{1,0:T(8,128)(2,1)} %b_in.1, bf16[384,256]{1,0:T(8,128)(2,1)} %c_in.1), custom_call_target="tpu_custom_call" | custom-call | tf_op jit(solution)/shard_map/tail/pallas_call | solution.py:376
  0.8 2.9 %collective-permute-start = (bf16[16,1536]{1,0:T(8,128)(2,1)S(1)}, bf16[16,1536]{1,0:T(8,128)(2,1)S(1)}, u32[]{:S(2)}, u32[]{:S(2)}) collective-permute-start(bf16[16,1536]{1,0:T(8,128)(2,1)S(1)} %tail.1), channel_id=1, source_target_pairs={{0,2},{2,4},{4,6},{6,8},{8,10},{10,12},{12,14},{14,16},{16,18},{18... | collective-permute-start | bytes 147464 | tf_op jit(solution)/shard_map/ppermute | solution.py:371
  3.7 0.0 copy-start
  3.7 0.0 copy-start.1
  3.7 0.0 copy-start.2
  3.7 4.7 %local.1 = (bf16[384,1024]{1,0:T(8,128)(2,1)S(1)}, bf16[384,256]{1,0:T(8,128)(2,1)S(1)}, bf16[384,256]{1,0:T(8,128)(2,1)S(1)}, f32[16,384]{1,0:T(8,128)S(1)}, f3...) custom-call(bf16[384,1024]{1,0:T(8,128)(2,1)} %values.1, ...), custom_call_target="tpu_custom_call" | custom-call | flops 4000000000 | bytes 4000000 | tf_op jit(solution)/shard_map/local/pallas_call | solution.py:395
  8.5 0.0 copy-start.4
  8.5 0.0 collective-permute-done.halo
  8.5 0.0 copy-done
  8.5 0.0 copy-done.1
  8.5 0.4 shard_map.127
  8.9 1.1 %collective-permute-start.1 = (bf16[144,256]{1,0:T(8,128)(2,1)S(1)}, bf16[144,256]{1,0:T(8,128)(2,1)S(1)}, u32[]{:S(2)}, u32[]{:S(2)}) collective-permute-start(bf16[144,256]{1,0:T(8,128)(2,1)S(1)} %get-tuple-element.50), channel_id=1, source_target_pairs={{0,2},{2,0},{4,6},{6,4},{8,10},{10,8},{12,14},{14,12},{16,18},{18,... | collective-permute-start | bytes 221192 | tf_op jit(solution)/shard_map/ppermute | solution.py:371
  10.0 0.8 %collective-permute-start.2 = (bf16[144,256]{1,0:T(8,128)(2,1)S(1)}, bf16[144,256]{1,0:T(8,128)(2,1)S(1)}, u32[]{:S(2)}, u32[]{:S(2)}) collective-permute-start(bf16[144,256]{1,0:T(8,128)(2,1)S(1)} %get-tuple-element.51), channel_id=1, source_target_pairs={{0,4},{2,6},{4,0},{6,2},{8,12},{10,14},{12,8},{14,10},{16,20},{18,... | collective-permute-start | bytes 221192 | tf_op jit(solution)/shard_map/ppermute | solution.py:371
  10.8 1.8 %collective-permute-start.3 = (bf16[144,256]{1,0:T(8,128)(2,1)S(1)}, bf16[144,256]{1,0:T(8,128)(2,1)S(1)}, u32[]{:S(2)}, u32[]{:S(2)}) collective-permute-start(bf16[144,256]{1,0:T(8,128)(2,1)S(1)} %get-tuple-element.52), channel_id=1, source_target_pairs={{0,6},{2,4},{4,2},{6,0},{8,14},{10,12},{12,10},{14,8},{16,22},{18,... | collective-permute-start | bytes 221192 | tf_op jit(solution)/shard_map/ppermute | solution.py:371
  12.6 0.0 collective-permute-done.1.r1.refs_9_
  12.6 2.3 %collective-permute-done.2.r2.refs_10_ = bf16[144,256]{1,0:T(8,128)(2,1)S(1)} collective-permute-done((bf16[144,256]{1,0:T(8,128)(2,1)S(1)}, bf16[144,256]{1,0:T(8,128)(2,1)S(1)}, u32[]{:S(2)}, u32[]{:S(2)}) %collective-permute-start.2) | collective-permute-done | bytes 73760 | tf_op jit(solution)/shard_map/ppermute | solution.py:371
  14.8 1.7 %collective-permute-done.3.r3.refs_11_ = bf16[144,256]{1,0:T(8,128)(2,1)S(1)} collective-permute-done((bf16[144,256]{1,0:T(8,128)(2,1)S(1)}, bf16[144,256]{1,0:T(8,128)(2,1)S(1)}, u32[]{:S(2)}, u32[]{:S(2)}) %collective-permute-start.3) | collective-permute-done | bytes 73760 | tf_op jit(solution)/shard_map/ppermute | solution.py:371
  16.6 0.1 shard_map.130
  16.7 0.7 collective-permute-start.4
  17.3 0.0 collective-permute-done.4.refs_0_
  17.4 0.7 collective-permute-start.5
  18.1 0.0 collective-permute-done.5.refs_0_.refs_1_
  18.1 0.7 collective-permute-start.6
  18.8 1.3 %collective-permute-start.8 = (bf16[144,256]{1,0:T(8,128)(2,1)S(1)}, bf16[144,256]{1,0:T(8,128)(2,1)S(1)}, u32[]{:S(2)}, u32[]{:S(2)}) collective-permute-start(bf16[144,256]{1,0:T(8,128)(2,1)S(1)} %get-tuple-element.56), channel_id=1, source_target_pairs={{32,40},{34,42},{36,44},{38,46},{48,56},{50,58},{52,60},{54,62},{3... | collective-permute-start | bytes 221192 | tf_op jit(solution)/shard_map/ppermute | solution.py:371
  20.1 0.0 collective-permute-done.6.refs_0_.refs_2_
  20.1 0.7 collective-permute-start.7
  20.8 7.0 %collective-permute-done.8.last.refs_7_ = bf16[144,256]{1,0:T(8,128)(2,1)S(1)} collective-permute-done((bf16[144,256]{1,0:T(8,128)(2,1)S(1)}, bf16[144,256]{1,0:T(8,128)(2,1)S(1)}, u32[]{:S(2)}, u32[]{:S(2)}) %collective-permute-start.8) | collective-permute-done | bytes 73760 | tf_op jit(solution)/shard_map/ppermute | solution.py:371
  27.8 0.0 collective-permute-done.7.before.refs_3_
  27.8 1.3 %collective-permute-start.9 = (bf16[128,256]{1,0:T(8,128)(2,1)S(1)}, bf16[128,256]{1,0:T(8,128)(2,1)S(1)}, u32[]{:S(2)}, u32[]{:S(2)}) collective-permute-start(bf16[128,256]{1,0:T(8,128)(2,1)S(1)} %shard_map.134.refs_1_), channel_id=1, source_target_pairs={{40,56},{42,58},{44,60},{46,62},{41,57},{43,59},{45,61},{47,63},{1... | collective-permute-start | bytes 196616 | tf_op jit(solution)/shard_map/ppermute | solution.py:371
  29.1 0.7 collective-permute-start.10
  29.8 0.0 copy-start.5
  29.8 0.4 shard_map.128
  30.3 0.2 copy-done.5
  30.5 0.0 collective-permute-done.10.refs_5_.refs_6_
  30.5 14.5 %collective-permute-done.9.refs_4_ = bf16[128,256]{1,0:T(8,128)(2,1)S(1)} collective-permute-done((bf16[128,256]{1,0:T(8,128)(2,1)S(1)}, bf16[128,256]{1,0:T(8,128)(2,1)S(1)}, u32[]{:S(2)}, u32[]{:S(2)}) %collective-permute-start.9) | collective-permute-done | bytes 65568 | tf_op jit(solution)/shard_map/ppermute | solution.py:371
  45.0 0.2 shard_map.136
  45.1 3.5 %collective-permute-start.11 = (bf16[128,256]{1,0:T(8,128)(2,1)S(1)}, bf16[128,256]{1,0:T(8,128)(2,1)S(1)}, u32[]{:S(2)}, u32[]{:S(2)}) collective-permute-start(bf16[128,256]{1,0:T(8,128)(2,1)S(1)} %get-tuple-element.58), channel_id=1, source_target_pairs={{0,2},{2,0},{4,6},{6,4},{8,10},{10,8},{12,14},{14,12},{16,18},{18,... | collective-permute-start | bytes 196616 | tf_op jit(solution)/shard_map/ppermute | solution.py:371
  48.7 2.3 %collective-permute-start.12 = (bf16[128,256]{1,0:T(8,128)(2,1)S(1)}, bf16[128,256]{1,0:T(8,128)(2,1)S(1)}, u32[]{:S(2)}, u32[]{:S(2)}) collective-permute-start(bf16[128,256]{1,0:T(8,128)(2,1)S(1)} %get-tuple-element.59), channel_id=1, source_target_pairs={{0,4},{2,6},{4,0},{6,2},{8,12},{10,14},{12,8},{14,10},{16,20},{18,... | collective-permute-start | bytes 196616 | tf_op jit(solution)/shard_map/ppermute | solution.py:371
  50.9 1.0 %collective-permute-start.13 = (bf16[128,256]{1,0:T(8,128)(2,1)S(1)}, bf16[128,256]{1,0:T(8,128)(2,1)S(1)}, u32[]{:S(2)}, u32[]{:S(2)}) collective-permute-start(bf16[128,256]{1,0:T(8,128)(2,1)S(1)} %get-tuple-element.60), channel_id=1, source_target_pairs={{0,6},{2,4},{4,2},{6,0},{8,14},{10,12},{12,10},{14,8},{16,22},{18,... | collective-permute-start | bytes 196616 | tf_op jit(solution)/shard_map/ppermute | solution.py:371
  52.0 2.6 %shard_map.129 = (f32[384,1024]{1,0:T(8,128)S(1)}, bf16[384,256]{1,0:T(8,128)(2,1)S(1)}) custom-call(bf16[384,1024]{1,0:T(8,128)(2,1)S(1)} %get-tuple-element.33.x_act, bf16[384,256]{1,0:T(8,128)(2,1)S(1)} %get-tuple-element.34.b_act, bf16[384,256]{1,0:T(8,128)(2,1)S(1)} %get-tuple-element.35.c_act, bf16[16,1024]{1,0:T(8,128)(2,1)S(1)} %get-tuple-element.40.edge_x, ...), custom_call_target="tpu_custom_call" | custom-call | flops 4000000000 | bytes 2850816 | tf_op jit(solution)/shard_map/pallas_call | solution.py:156
  54.5 0.0 collective-permute-done.11.p1
  54.6 0.0 collective-permute-done.12.p2
  54.6 1.3 %collective-permute-done.13.p3 = bf16[128,256]{1,0:T(8,128)(2,1)S(1)} collective-permute-done((bf16[128,256]{1,0:T(8,128)(2,1)S(1)}, bf16[128,256]{1,0:T(8,128)(2,1)S(1)}, u32[]{:S(2)}, u32[]{:S(2)}) %collective-permute-start.13) | collective-permute-done | bytes 65568 | tf_op jit(solution)/shard_map/ppermute | solution.py:371
  55.8 1.6 %shard_map.138 = bf16[192,2048]{1,0:T(8,128)(2,1)S(1)} custom-call(f32[384,1024]{1,0:T(8,128)S(1)} %get-tuple-element.46.y_in, f32[384,1024]{1,0:T(8,128)S(1)} %get-tuple-element.47.grow, bf16[384,256]{1,0:T(8,128)(2,1)S(1)} %get-tuple-element.48.c_all, bf16[1,1024]{1,0:T(2,128)(2,1)S(1)} %reshape.12.gain, bf16[128,256]{1,0:T(8,128)(2,1)S(1)} %get-tuple-element.57.p0, ...), custom_call_target="tpu_custom_call" | custom-call | flops 4000000000 | bytes 7800832 | tf_op jit(solution)/shard_map/pallas_call | solution.py:156
  57.4 13.2 %collective-permute-start.14 = (bf16[192,2048]{1,0:T(8,128)(2,1)S(1)}, bf16[192,2048]{1,0:T(8,128)(2,1)S(1)}, u32[]{:S(2)}, u32[]{:S(2)}) collective-permute-start(bf16[192,2048]{1,0:T(8,128)(2,1)S(1)} %shard_map.138), channel_id=1, source_target_pairs={{0,1},{1,0},{2,3},{3,2},{4,5},{5,4},{6,7},{7,6},{8,9},{9,8},{10,11... | collective-permute-start | bytes 2359304 | tf_op jit(solution)/shard_map/ppermute | solution.py:492
  70.6 1.6 %shard_map.137.own = f32[192,2048]{1,0:T(8,128)S(1)} custom-call(f32[384,1024]{1,0:T(8,128)S(1)} %get-tuple-element.46.y_in, f32[384,1024]{1,0:T(8,128)S(1)} %get-tuple-element.47.grow, bf16[384,256]{1,0:T(8,128)(2,1)S(1)} %get-tuple-element.48.c_all, bf16[1,1024]{1,0:T(2,128)(2,1)S(1)} %reshape.12.gain, bf16[128,256]{1,0:T(8,128)(2,1)S(1)} %get-tuple-element.57.p0, ...), custom_call_target="tpu_custom_call" | custom-call | flops 4000000000 | bytes 7800832 | tf_op jit(solution)/shard_map/pallas_call | solution.py:156
  72.2 0.3 collective-permute-done.14.other
  72.5 1.0 %shard_map.139 = bf16[192,2048]{1,0:T(8,128)(2,1)} custom-call(f32[192,2048]{1,0:T(8,128)S(1)} %shard_map.137.own, bf16[192,2048]{1,0:T(8,128)(2,1)S(1)} %collective-permute-done.14.other), custom_call_target="tpu_custom_call" | custom-call | bytes 2359296 | tf_op jit(solution)/shard_map/pallas_call | solution.py:156
  (10 shorter events, 0.1 us)
Async XLA Ops:
  0.8 7.7 %collective-permute-start = (bf16[16,1536]{1,0:T(8,128)(2,1)S(1)}, bf16[16,1536]{1,0:T(8,128)(2,1)S(1)}, u32[]{:S(2)}, u32[]{:S(2)}) collective-permute-start(bf16[16,1536]{1,0:T(8,128)(2,1)S(1)} %tail.1), channel_id=1, source_target_pairs={{0,2},{2,4},{4,6},{6,8},{8,10},{10,12},{12,14},{14,16},{16,18},{18... | collective-permute-start | bytes 147464 | tf_op jit(solution)/shard_map/ppermute | solution.py:371
  3.7 4.8 %copy-start = (bf16[4,1024]{1,0:T(4,128)(2,1)S(1)}, bf16[4,1024]{1,0:T(4,128)(2,1)}, u32[]{:S(2)}) copy-start(bf16[4,1024]{1,0:T(4,128)(2,1)} %conv_x.1) | copy-start | bytes 24580
  3.7 4.8 %copy-start.1 = (bf16[4,256]{1,0:T(4,128)(2,1)S(1)}, bf16[4,256]{1,0:T(4,128)(2,1)}, u32[]{:S(2)}) copy-start(bf16[4,256]{1,0:T(4,128)(2,1)} %conv_b.1) | copy-start | bytes 6148
  3.7 4.8 %copy-start.2 = (bf16[4,256]{1,0:T(4,128)(2,1)S(1)}, bf16[4,256]{1,0:T(4,128)(2,1)}, u32[]{:S(2)}) copy-start(bf16[4,256]{1,0:T(4,128)(2,1)} %conv_c.1) | copy-start | bytes 6148
  8.5 21.3 %copy-start.4 = (bf16[384,1024]{1,0:T(8,128)(2,1)S(1)}, bf16[384,1024]{1,0:T(8,128)(2,1)}, u32[]{:S(2)}) copy-start(bf16[384,1024]{1,0:T(8,128)(2,1)} %gate.1) | copy-start | bytes 2359300
  8.9 3.7 %collective-permute-start.1 = (bf16[144,256]{1,0:T(8,128)(2,1)S(1)}, bf16[144,256]{1,0:T(8,128)(2,1)S(1)}, u32[]{:S(2)}, u32[]{:S(2)}) collective-permute-start(bf16[144,256]{1,0:T(8,128)(2,1)S(1)} %get-tuple-element.50), channel_id=1, source_target_pairs={{0,2},{2,0},{4,6},{6,4},{8,10},{10,8},{12,14},{14,12},{16,18},{18,... | collective-permute-start | bytes 221192 | tf_op jit(solution)/shard_map/ppermute | solution.py:371
  10.0 4.9 %collective-permute-start.2 = (bf16[144,256]{1,0:T(8,128)(2,1)S(1)}, bf16[144,256]{1,0:T(8,128)(2,1)S(1)}, u32[]{:S(2)}, u32[]{:S(2)}) collective-permute-start(bf16[144,256]{1,0:T(8,128)(2,1)S(1)} %get-tuple-element.51), channel_id=1, source_target_pairs={{0,4},{2,6},{4,0},{6,2},{8,12},{10,14},{12,8},{14,10},{16,20},{18,... | collective-permute-start | bytes 221192 | tf_op jit(solution)/shard_map/ppermute | solution.py:371
  10.8 5.8 %collective-permute-start.3 = (bf16[144,256]{1,0:T(8,128)(2,1)S(1)}, bf16[144,256]{1,0:T(8,128)(2,1)S(1)}, u32[]{:S(2)}, u32[]{:S(2)}) collective-permute-start(bf16[144,256]{1,0:T(8,128)(2,1)S(1)} %get-tuple-element.52), channel_id=1, source_target_pairs={{0,6},{2,4},{4,2},{6,0},{8,14},{10,12},{12,10},{14,8},{16,22},{18,... | collective-permute-start | bytes 221192 | tf_op jit(solution)/shard_map/ppermute | solution.py:371
  16.7 0.7 collective-permute-start.4
  17.4 0.7 collective-permute-start.5
  18.1 2.0 %collective-permute-start.6 = (bf16[128,256]{1,0:T(8,128)(2,1)S(1)}, bf16[128,256]{1,0:T(8,128)(2,1)S(1)}, u32[]{:S(2)}, u32[]{:S(2)}) collective-permute-start(bf16[128,256]{1,0:T(8,128)(2,1)S(1)} %shard_map.132), channel_id=1, source_target_pairs={{0,0},{2,2},{4,4},{6,6},{8,8},{10,10},{12,12},{14,14},{16,24},{18,... | collective-permute-start | bytes 196616 | tf_op jit(solution)/shard_map/ppermute | solution.py:371
  18.8 9.0 %collective-permute-start.8 = (bf16[144,256]{1,0:T(8,128)(2,1)S(1)}, bf16[144,256]{1,0:T(8,128)(2,1)S(1)}, u32[]{:S(2)}, u32[]{:S(2)}) collective-permute-start(bf16[144,256]{1,0:T(8,128)(2,1)S(1)} %get-tuple-element.56), channel_id=1, source_target_pairs={{32,40},{34,42},{36,44},{38,46},{48,56},{50,58},{52,60},{54,62},{3... | collective-permute-start | bytes 221192 | tf_op jit(solution)/shard_map/ppermute | solution.py:371
  20.1 7.7 %collective-permute-start.7 = (bf16[128,256]{1,0:T(8,128)(2,1)S(1)}, bf16[128,256]{1,0:T(8,128)(2,1)S(1)}, u32[]{:S(2)}, u32[]{:S(2)}) collective-permute-start(bf16[128,256]{1,0:T(8,128)(2,1)S(1)} %shard_map.133.refs_0_), channel_id=1, source_target_pairs={{24,40},{26,42},{28,44},{30,46},{25,41},{27,43},{29,45},{31,47},{8... | collective-permute-start | bytes 196616 | tf_op jit(solution)/shard_map/ppermute | solution.py:371
  27.8 17.1 %collective-permute-start.9 = (bf16[128,256]{1,0:T(8,128)(2,1)S(1)}, bf16[128,256]{1,0:T(8,128)(2,1)S(1)}, u32[]{:S(2)}, u32[]{:S(2)}) collective-permute-start(bf16[128,256]{1,0:T(8,128)(2,1)S(1)} %shard_map.134.refs_1_), channel_id=1, source_target_pairs={{40,56},{42,58},{44,60},{46,62},{41,57},{43,59},{45,61},{47,63},{1... | collective-permute-start | bytes 196616 | tf_op jit(solution)/shard_map/ppermute | solution.py:371
  29.1 1.4 %collective-permute-start.10 = (bf16[128,256]{1,0:T(8,128)(2,1)S(1)}, bf16[128,256]{1,0:T(8,128)(2,1)S(1)}, u32[]{:S(2)}, u32[]{:S(2)}) collective-permute-start(bf16[128,256]{1,0:T(8,128)(2,1)S(1)} %shard_map.135), channel_id=1, source_target_pairs={{24,32},{26,34},{28,36},{30,38},{40,48},{42,50},{44,52},{46,54},{2... | collective-permute-start | bytes 196616 | tf_op jit(solution)/shard_map/ppermute | solution.py:371
  29.8 0.7 copy-start.5
  45.1 9.4 %collective-permute-start.11 = (bf16[128,256]{1,0:T(8,128)(2,1)S(1)}, bf16[128,256]{1,0:T(8,128)(2,1)S(1)}, u32[]{:S(2)}, u32[]{:S(2)}) collective-permute-start(bf16[128,256]{1,0:T(8,128)(2,1)S(1)} %get-tuple-element.58), channel_id=1, source_target_pairs={{0,2},{2,0},{4,6},{6,4},{8,10},{10,8},{12,14},{14,12},{16,18},{18,... | collective-permute-start | bytes 196616 | tf_op jit(solution)/shard_map/ppermute | solution.py:371
  48.7 5.9 %collective-permute-start.12 = (bf16[128,256]{1,0:T(8,128)(2,1)S(1)}, bf16[128,256]{1,0:T(8,128)(2,1)S(1)}, u32[]{:S(2)}, u32[]{:S(2)}) collective-permute-start(bf16[128,256]{1,0:T(8,128)(2,1)S(1)} %get-tuple-element.59), channel_id=1, source_target_pairs={{0,4},{2,6},{4,0},{6,2},{8,12},{10,14},{12,8},{14,10},{16,20},{18,... | collective-permute-start | bytes 196616 | tf_op jit(solution)/shard_map/ppermute | solution.py:371
  50.9 4.9 %collective-permute-start.13 = (bf16[128,256]{1,0:T(8,128)(2,1)S(1)}, bf16[128,256]{1,0:T(8,128)(2,1)S(1)}, u32[]{:S(2)}, u32[]{:S(2)}) collective-permute-start(bf16[128,256]{1,0:T(8,128)(2,1)S(1)} %get-tuple-element.60), channel_id=1, source_target_pairs={{0,6},{2,4},{4,2},{6,0},{8,14},{10,12},{12,10},{14,8},{16,22},{18,... | collective-permute-start | bytes 196616 | tf_op jit(solution)/shard_map/ppermute | solution.py:371
  52.0 3.9 %copy-start.3 = (bf16[1024,2048]{1,0:T(8,128)(2,1)S(1)}, bf16[1024,2048]{1,0:T(8,128)(2,1)}, u32[]{:S(2)}) copy-start(bf16[1024,2048]{1,0:T(8,128)(2,1)} %w_out.3) | copy-start | bytes 12582916
  57.4 15.1 %collective-permute-start.14 = (bf16[192,2048]{1,0:T(8,128)(2,1)S(1)}, bf16[192,2048]{1,0:T(8,128)(2,1)S(1)}, u32[]{:S(2)}, u32[]{:S(2)}) collective-permute-start(bf16[192,2048]{1,0:T(8,128)(2,1)S(1)} %shard_map.138), channel_id=1, source_target_pairs={{0,1},{1,0},{2,3},{3,2},{4,5},{5,4},{6,7},{7,6},{8,9},{9,8},{10,11... | collective-permute-start | bytes 2359304 | tf_op jit(solution)/shard_map/ppermute | solution.py:492

commit v4 on v3

--- a/solution.py
+++ b/solution.py
@@ -437,13 +437,6 @@
     def up(x, sources, distance):
         return move(x, [(i, i + distance * QUAD) for four in sources for i in range(four * QUAD, (four + 1) * QUAD)])
 
-    def swap(x, four):
-        first, route = four * QUAD, []
-        for i in range(places):
-            moved = i + QUAD if first <= i < first + QUAD else i - QUAD if first + QUAD <= i < first + 2 * QUAD else i
-            route.append((i, moved))
-        return move(x, route)
-
     def jump(four, before, last=None):
         if last is None:
             kernel = lambda *refs: jump_kernel(four, refs[0], None, *refs[1:])
@@ -454,7 +447,7 @@
     arrived, targets = [], []
 
     def send(x, four, distance):
-        arrived.append(swap(x, four) if distance == 1 else up(x, (four,), distance))
+        arrived.append(up(x, (four,), distance))
         targets.append(four + distance)
         return arrived[-1]
 

time: 73.8 us -> 71.8 us (0.973)
  starting transfers between devices: 32.5 us -> 30.6 us
    ppermute x1, starting transfers between devices: 13.2 us -> 5.29 us  [body(): other = lax.ppermute(theirs, 'tp', [(0, 1), (1, 0)])]
    ppermute x14, starting transfers between devices: 19.3 us -> 25.3 us  [move(): return lax.ppermute(x, 'sp', route)]
where the time goes in v4:
time: 71.8 us; the launch traced here: 71.5 us
  starting transfers between devices  30.6 us (43%)
  waiting for transfers between devices  26.9 us (37%)
  Pallas kernels  13.4 us (19%)
    ppermute x14, waiting for transfers between devices, move(): return lax.ppermute(x, 'sp', route)  26.6 us
    ppermute x14, starting transfers between devices, move(): return lax.ppermute(x, 'sp', route)  25.3 us
    pallas_call x13, Pallas kernels, local_call(): pl.pallas_call(kernel, out_shape=outs, in_specs=whole(len(args)), out_spe...  7.85 us
    ppermute x1, starting transfers between devices, body(): other = lax.ppermute(theirs, 'tp', [(0, 1), (1, 0)])  5.29 us
    pallas_call x1, Pallas kernels, body(): pl.pallas_call(local_kernel, out_shape=outs, in_specs=[pl.BlockSpec(memor...  4.73 us
  transfers between devices with their start and end apart: 15, of which 6 were waited for; matrix products, arithmetic and copies ran while one was open for 0% of the time, Pallas kernels for 13%

profile of v4, /device:TPU:1829, one launch (start us, length us, event | category | flops | bytes accessed | tf_op | source)
XLA Modules:
  0.0 71.5 jit_solution(3568157512137141470)
XLA Ops:
  0.0 0.8 %tail.1 = bf16[16,1536]{1,0:T(8,128)(2,1)S(1)} custom-call(bf16[384,1024]{1,0:T(8,128)(2,1)} %values.1, bf16[384,256]{1,0:T(8,128)(2,1)} %b_in.1, bf16[384,256]{1,0:T(8,128)(2,1)} %c_in.1), custom_call_target="tpu_custom_call" | custom-call | tf_op jit(solution)/shard_map/tail/pallas_call | solution.py:376
  0.8 2.9 %collective-permute-start = (bf16[16,1536]{1,0:T(8,128)(2,1)S(1)}, bf16[16,1536]{1,0:T(8,128)(2,1)S(1)}, u32[]{:S(2)}, u32[]{:S(2)}) collective-permute-start(bf16[16,1536]{1,0:T(8,128)(2,1)S(1)} %tail.1), channel_id=1, source_target_pairs={{0,2},{2,4},{4,6},{6,8},{8,10},{10,12},{12,14},{14,16},{16,18},{18... | collective-permute-start | bytes 147464 | tf_op jit(solution)/shard_map/ppermute | solution.py:371
  3.7 0.0 copy-start
  3.7 0.0 copy-start.1
  3.7 0.0 copy-start.2
  3.7 4.7 %local.1 = (bf16[384,1024]{1,0:T(8,128)(2,1)S(1)}, bf16[384,256]{1,0:T(8,128)(2,1)S(1)}, bf16[384,256]{1,0:T(8,128)(2,1)S(1)}, f32[16,384]{1,0:T(8,128)S(1)}, f3...) custom-call(bf16[384,1024]{1,0:T(8,128)(2,1)} %values.1, ...), custom_call_target="tpu_custom_call" | custom-call | flops 4000000000 | bytes 4000000 | tf_op jit(solution)/shard_map/local/pallas_call | solution.py:395
  8.5 0.0 copy-start.4
  8.5 0.0 collective-permute-done.halo
  8.5 0.0 copy-done
  8.5 0.0 copy-done.1
  8.5 0.4 shard_map.127
  8.9 1.1 %collective-permute-start.1 = (bf16[144,256]{1,0:T(8,128)(2,1)S(1)}, bf16[144,256]{1,0:T(8,128)(2,1)S(1)}, u32[]{:S(2)}, u32[]{:S(2)}) collective-permute-start(bf16[144,256]{1,0:T(8,128)(2,1)S(1)} %get-tuple-element.50), channel_id=1, source_target_pairs={{0,2},{2,0},{4,6},{6,4},{8,10},{10,8},{12,14},{14,12},{16,18},{18,... | collective-permute-start | bytes 221192 | tf_op jit(solution)/shard_map/ppermute | solution.py:371
  10.0 0.8 %collective-permute-start.2 = (bf16[144,256]{1,0:T(8,128)(2,1)S(1)}, bf16[144,256]{1,0:T(8,128)(2,1)S(1)}, u32[]{:S(2)}, u32[]{:S(2)}) collective-permute-start(bf16[144,256]{1,0:T(8,128)(2,1)S(1)} %get-tuple-element.51), channel_id=1, source_target_pairs={{0,4},{2,6},{4,0},{6,2},{8,12},{10,14},{12,8},{14,10},{16,20},{18,... | collective-permute-start | bytes 221192 | tf_op jit(solution)/shard_map/ppermute | solution.py:371
  10.8 1.8 %collective-permute-start.3 = (bf16[144,256]{1,0:T(8,128)(2,1)S(1)}, bf16[144,256]{1,0:T(8,128)(2,1)S(1)}, u32[]{:S(2)}, u32[]{:S(2)}) collective-permute-start(bf16[144,256]{1,0:T(8,128)(2,1)S(1)} %get-tuple-element.52), channel_id=1, source_target_pairs={{0,6},{2,4},{4,2},{6,0},{8,14},{10,12},{12,10},{14,8},{16,22},{18,... | collective-permute-start | bytes 221192 | tf_op jit(solution)/shard_map/ppermute | solution.py:371
  12.6 0.0 collective-permute-done.1.r1.refs_9_
  12.6 2.3 %collective-permute-done.2.r2.refs_10_ = bf16[144,256]{1,0:T(8,128)(2,1)S(1)} collective-permute-done((bf16[144,256]{1,0:T(8,128)(2,1)S(1)}, bf16[144,256]{1,0:T(8,128)(2,1)S(1)}, u32[]{:S(2)}, u32[]{:S(2)}) %collective-permute-start.2) | collective-permute-done | bytes 73760 | tf_op jit(solution)/shard_map/ppermute | solution.py:371
  14.8 1.7 %collective-permute-done.3.r3.refs_11_ = bf16[144,256]{1,0:T(8,128)(2,1)S(1)} collective-permute-done((bf16[144,256]{1,0:T(8,128)(2,1)S(1)}, bf16[144,256]{1,0:T(8,128)(2,1)S(1)}, u32[]{:S(2)}, u32[]{:S(2)}) %collective-permute-start.3) | collective-permute-done | bytes 73760 | tf_op jit(solution)/shard_map/ppermute | solution.py:371
  16.6 0.1 shard_map.130
  16.7 0.7 collective-permute-start.4
  17.3 0.0 collective-permute-done.4.refs_0_
  17.4 0.7 collective-permute-start.5
  18.1 0.0 collective-permute-done.5.refs_0_.refs_1_
  18.1 0.7 collective-permute-start.6
  18.8 1.3 %collective-permute-start.8 = (bf16[144,256]{1,0:T(8,128)(2,1)S(1)}, bf16[144,256]{1,0:T(8,128)(2,1)S(1)}, u32[]{:S(2)}, u32[]{:S(2)}) collective-permute-start(bf16[144,256]{1,0:T(8,128)(2,1)S(1)} %get-tuple-element.56), channel_id=1, source_target_pairs={{32,40},{34,42},{36,44},{38,46},{48,56},{50,58},{52,60},{54,62},{3... | collective-permute-start | bytes 221192 | tf_op jit(solution)/shard_map/ppermute | solution.py:371
  20.1 0.0 collective-permute-done.6.refs_0_.refs_2_
  20.1 0.7 collective-permute-start.7
  20.8 7.0 %collective-permute-done.8.last.refs_7_ = bf16[144,256]{1,0:T(8,128)(2,1)S(1)} collective-permute-done((bf16[144,256]{1,0:T(8,128)(2,1)S(1)}, bf16[144,256]{1,0:T(8,128)(2,1)S(1)}, u32[]{:S(2)}, u32[]{:S(2)}) %collective-permute-start.8) | collective-permute-done | bytes 73760 | tf_op jit(solution)/shard_map/ppermute | solution.py:371
  27.8 0.0 collective-permute-done.7.before.refs_3_
  27.8 1.3 %collective-permute-start.9 = (bf16[128,256]{1,0:T(8,128)(2,1)S(1)}, bf16[128,256]{1,0:T(8,128)(2,1)S(1)}, u32[]{:S(2)}, u32[]{:S(2)}) collective-permute-start(bf16[128,256]{1,0:T(8,128)(2,1)S(1)} %shard_map.134.refs_1_), channel_id=1, source_target_pairs={{40,56},{42,58},{44,60},{46,62},{41,57},{43,59},{45,61},{47,63},{1... | collective-permute-start | bytes 196616 | tf_op jit(solution)/shard_map/ppermute | solution.py:371
  29.1 0.7 collective-permute-start.10
  29.8 0.0 copy-start.5
  29.8 0.4 shard_map.128
  30.3 0.2 copy-done.5
  30.5 0.0 collective-permute-done.10.refs_5_.refs_6_
  30.5 14.0 %collective-permute-done.9.refs_4_ = bf16[128,256]{1,0:T(8,128)(2,1)S(1)} collective-permute-done((bf16[128,256]{1,0:T(8,128)(2,1)S(1)}, bf16[128,256]{1,0:T(8,128)(2,1)S(1)}, u32[]{:S(2)}, u32[]{:S(2)}) %collective-permute-start.9) | collective-permute-done | bytes 65568 | tf_op jit(solution)/shard_map/ppermute | solution.py:371
  44.5 0.2 shard_map.136
  44.6 2.3 %collective-permute-start.11 = (bf16[128,256]{1,0:T(8,128)(2,1)S(1)}, bf16[128,256]{1,0:T(8,128)(2,1)S(1)}, u32[]{:S(2)}, u32[]{:S(2)}) collective-permute-start(bf16[128,256]{1,0:T(8,128)(2,1)S(1)} %get-tuple-element.58), channel_id=1, source_target_pairs={{0,2},{2,0},{4,6},{6,4},{8,10},{10,8},{12,14},{14,12},{16,18},{18,... | collective-permute-start | bytes 196616 | tf_op jit(solution)/shard_map/ppermute | solution.py:371
  46.9 9.5 %collective-permute-start.12 = (bf16[128,256]{1,0:T(8,128)(2,1)S(1)}, bf16[128,256]{1,0:T(8,128)(2,1)S(1)}, u32[]{:S(2)}, u32[]{:S(2)}) collective-permute-start(bf16[128,256]{1,0:T(8,128)(2,1)S(1)} %get-tuple-element.59), channel_id=1, source_target_pairs={{0,4},{2,6},{4,0},{6,2},{8,12},{10,14},{12,8},{14,10},{16,20},{18,... | collective-permute-start | bytes 196616 | tf_op jit(solution)/shard_map/ppermute | solution.py:371
  56.5 1.0 %collective-permute-start.13 = (bf16[128,256]{1,0:T(8,128)(2,1)S(1)}, bf16[128,256]{1,0:T(8,128)(2,1)S(1)}, u32[]{:S(2)}, u32[]{:S(2)}) collective-permute-start(bf16[128,256]{1,0:T(8,128)(2,1)S(1)} %get-tuple-element.60), channel_id=1, source_target_pairs={{0,6},{2,4},{4,2},{6,0},{8,14},{10,12},{12,10},{14,8},{16,22},{18,... | collective-permute-start | bytes 196616 | tf_op jit(solution)/shard_map/ppermute | solution.py:371
  57.5 2.6 %shard_map.129 = (f32[384,1024]{1,0:T(8,128)S(1)}, bf16[384,256]{1,0:T(8,128)(2,1)S(1)}) custom-call(bf16[384,1024]{1,0:T(8,128)(2,1)S(1)} %get-tuple-element.33.x_act, bf16[384,256]{1,0:T(8,128)(2,1)S(1)} %get-tuple-element.34.b_act, bf16[384,256]{1,0:T(8,128)(2,1)S(1)} %get-tuple-element.35.c_act, bf16[16,1024]{1,0:T(8,128)(2,1)S(1)} %get-tuple-element.40.edge_x, ...), custom_call_target="tpu_custom_call" | custom-call | flops 4000000000 | bytes 2850816 | tf_op jit(solution)/shard_map/pallas_call | solution.py:156
  60.1 0.0 collective-permute-done.11.p1
  60.1 0.0 collective-permute-done.12.p2
  60.1 1.6 %collective-permute-done.13.p3 = bf16[128,256]{1,0:T(8,128)(2,1)S(1)} collective-permute-done((bf16[128,256]{1,0:T(8,128)(2,1)S(1)}, bf16[128,256]{1,0:T(8,128)(2,1)S(1)}, u32[]{:S(2)}, u32[]{:S(2)}) %collective-permute-start.13) | collective-permute-done | bytes 65568 | tf_op jit(solution)/shard_map/ppermute | solution.py:371
  61.7 1.6 %shard_map.138 = bf16[192,2048]{1,0:T(8,128)(2,1)S(1)} custom-call(f32[384,1024]{1,0:T(8,128)S(1)} %get-tuple-element.46.y_in, f32[384,1024]{1,0:T(8,128)S(1)} %get-tuple-element.47.grow, bf16[384,256]{1,0:T(8,128)(2,1)S(1)} %get-tuple-element.48.c_all, bf16[1,1024]{1,0:T(2,128)(2,1)S(1)} %reshape.12.gain, bf16[128,256]{1,0:T(8,128)(2,1)S(1)} %get-tuple-element.57.p0, ...), custom_call_target="tpu_custom_call" | custom-call | flops 4000000000 | bytes 7800832 | tf_op jit(solution)/shard_map/pallas_call | solution.py:156
  63.3 5.3 %collective-permute-start.14 = (bf16[192,2048]{1,0:T(8,128)(2,1)S(1)}, bf16[192,2048]{1,0:T(8,128)(2,1)S(1)}, u32[]{:S(2)}, u32[]{:S(2)}) collective-permute-start(bf16[192,2048]{1,0:T(8,128)(2,1)S(1)} %shard_map.138), channel_id=1, source_target_pairs={{0,1},{1,0},{2,3},{3,2},{4,5},{5,4},{6,7},{7,6},{8,9},{9,8},{10,11... | collective-permute-start | bytes 2359304 | tf_op jit(solution)/shard_map/ppermute | solution.py:485
  68.5 1.6 %shard_map.137.own = f32[192,2048]{1,0:T(8,128)S(1)} custom-call(f32[384,1024]{1,0:T(8,128)S(1)} %get-tuple-element.46.y_in, f32[384,1024]{1,0:T(8,128)S(1)} %get-tuple-element.47.grow, bf16[384,256]{1,0:T(8,128)(2,1)S(1)} %get-tuple-element.48.c_all, bf16[1,1024]{1,0:T(2,128)(2,1)S(1)} %reshape.12.gain, bf16[128,256]{1,0:T(8,128)(2,1)S(1)} %get-tuple-element.57.p0, ...), custom_call_target="tpu_custom_call" | custom-call | flops 4000000000 | bytes 7800832 | tf_op jit(solution)/shard_map/pallas_call | solution.py:156
  70.1 0.3 collective-permute-done.14.other
  70.5 1.0 %shard_map.139 = bf16[192,2048]{1,0:T(8,128)(2,1)} custom-call(f32[192,2048]{1,0:T(8,128)S(1)} %shard_map.137.own, bf16[192,2048]{1,0:T(8,128)(2,1)S(1)} %collective-permute-done.14.other), custom_call_target="tpu_custom_call" | custom-call | bytes 2359296 | tf_op jit(solution)/shard_map/pallas_call | solution.py:156
  (10 shorter events, 0.1 us)
Async XLA Ops:
  0.8 7.7 %collective-permute-start = (bf16[16,1536]{1,0:T(8,128)(2,1)S(1)}, bf16[16,1536]{1,0:T(8,128)(2,1)S(1)}, u32[]{:S(2)}, u32[]{:S(2)}) collective-permute-start(bf16[16,1536]{1,0:T(8,128)(2,1)S(1)} %tail.1), channel_id=1, source_target_pairs={{0,2},{2,4},{4,6},{6,8},{8,10},{10,12},{12,14},{14,16},{16,18},{18... | collective-permute-start | bytes 147464 | tf_op jit(solution)/shard_map/ppermute | solution.py:371
  3.7 4.8 %copy-start = (bf16[4,1024]{1,0:T(4,128)(2,1)S(1)}, bf16[4,1024]{1,0:T(4,128)(2,1)}, u32[]{:S(2)}) copy-start(bf16[4,1024]{1,0:T(4,128)(2,1)} %conv_x.1) | copy-start | bytes 24580
  3.7 4.8 %copy-start.1 = (bf16[4,256]{1,0:T(4,128)(2,1)S(1)}, bf16[4,256]{1,0:T(4,128)(2,1)}, u32[]{:S(2)}) copy-start(bf16[4,256]{1,0:T(4,128)(2,1)} %conv_b.1) | copy-start | bytes 6148
  3.7 4.8 %copy-start.2 = (bf16[4,256]{1,0:T(4,128)(2,1)S(1)}, bf16[4,256]{1,0:T(4,128)(2,1)}, u32[]{:S(2)}) copy-start(bf16[4,256]{1,0:T(4,128)(2,1)} %conv_c.1) | copy-start | bytes 6148
  8.5 21.3 %copy-start.4 = (bf16[384,1024]{1,0:T(8,128)(2,1)S(1)}, bf16[384,1024]{1,0:T(8,128)(2,1)}, u32[]{:S(2)}) copy-start(bf16[384,1024]{1,0:T(8,128)(2,1)} %gate.1) | copy-start | bytes 2359300
  8.9 3.7 %collective-permute-start.1 = (bf16[144,256]{1,0:T(8,128)(2,1)S(1)}, bf16[144,256]{1,0:T(8,128)(2,1)S(1)}, u32[]{:S(2)}, u32[]{:S(2)}) collective-permute-start(bf16[144,256]{1,0:T(8,128)(2,1)S(1)} %get-tuple-element.50), channel_id=1, source_target_pairs={{0,2},{2,0},{4,6},{6,4},{8,10},{10,8},{12,14},{14,12},{16,18},{18,... | collective-permute-start | bytes 221192 | tf_op jit(solution)/shard_map/ppermute | solution.py:371
  10.0 4.9 %collective-permute-start.2 = (bf16[144,256]{1,0:T(8,128)(2,1)S(1)}, bf16[144,256]{1,0:T(8,128)(2,1)S(1)}, u32[]{:S(2)}, u32[]{:S(2)}) collective-permute-start(bf16[144,256]{1,0:T(8,128)(2,1)S(1)} %get-tuple-element.51), channel_id=1, source_target_pairs={{0,4},{2,6},{4,0},{6,2},{8,12},{10,14},{12,8},{14,10},{16,20},{18,... | collective-permute-start | bytes 221192 | tf_op jit(solution)/shard_map/ppermute | solution.py:371
  10.8 5.8 %collective-permute-start.3 = (bf16[144,256]{1,0:T(8,128)(2,1)S(1)}, bf16[144,256]{1,0:T(8,128)(2,1)S(1)}, u32[]{:S(2)}, u32[]{:S(2)}) collective-permute-start(bf16[144,256]{1,0:T(8,128)(2,1)S(1)} %get-tuple-element.52), channel_id=1, source_target_pairs={{0,6},{2,4},{4,2},{6,0},{8,14},{10,12},{12,10},{14,8},{16,22},{18,... | collective-permute-start | bytes 221192 | tf_op jit(solution)/shard_map/ppermute | solution.py:371
  16.7 0.7 collective-permute-start.4
  17.4 0.7 collective-permute-start.5
  18.1 2.0 %collective-permute-start.6 = (bf16[128,256]{1,0:T(8,128)(2,1)S(1)}, bf16[128,256]{1,0:T(8,128)(2,1)S(1)}, u32[]{:S(2)}, u32[]{:S(2)}) collective-permute-start(bf16[128,256]{1,0:T(8,128)(2,1)S(1)} %shard_map.132), channel_id=1, source_target_pairs={{16,24},{18,26},{20,28},{22,30},{17,25},{19,27},{21,29},{23,31},{8... | collective-permute-start | bytes 196616 | tf_op jit(solution)/shard_map/ppermute | solution.py:371
  18.8 9.0 %collective-permute-start.8 = (bf16[144,256]{1,0:T(8,128)(2,1)S(1)}, bf16[144,256]{1,0:T(8,128)(2,1)S(1)}, u32[]{:S(2)}, u32[]{:S(2)}) collective-permute-start(bf16[144,256]{1,0:T(8,128)(2,1)S(1)} %get-tuple-element.56), channel_id=1, source_target_pairs={{32,40},{34,42},{36,44},{38,46},{48,56},{50,58},{52,60},{54,62},{3... | collective-permute-start | bytes 221192 | tf_op jit(solution)/shard_map/ppermute | solution.py:371
  20.1 7.7 %collective-permute-start.7 = (bf16[128,256]{1,0:T(8,128)(2,1)S(1)}, bf16[128,256]{1,0:T(8,128)(2,1)S(1)}, u32[]{:S(2)}, u32[]{:S(2)}) collective-permute-start(bf16[128,256]{1,0:T(8,128)(2,1)S(1)} %shard_map.133.refs_0_), channel_id=1, source_target_pairs={{24,40},{26,42},{28,44},{30,46},{25,41},{27,43},{29,45},{31,47},{8... | collective-permute-start | bytes 196616 | tf_op jit(solution)/shard_map/ppermute | solution.py:371
  27.8 16.7 %collective-permute-start.9 = (bf16[128,256]{1,0:T(8,128)(2,1)S(1)}, bf16[128,256]{1,0:T(8,128)(2,1)S(1)}, u32[]{:S(2)}, u32[]{:S(2)}) collective-permute-start(bf16[128,256]{1,0:T(8,128)(2,1)S(1)} %shard_map.134.refs_1_), channel_id=1, source_target_pairs={{40,56},{42,58},{44,60},{46,62},{41,57},{43,59},{45,61},{47,63},{1... | collective-permute-start | bytes 196616 | tf_op jit(solution)/shard_map/ppermute | solution.py:371
  29.1 1.4 %collective-permute-start.10 = (bf16[128,256]{1,0:T(8,128)(2,1)S(1)}, bf16[128,256]{1,0:T(8,128)(2,1)S(1)}, u32[]{:S(2)}, u32[]{:S(2)}) collective-permute-start(bf16[128,256]{1,0:T(8,128)(2,1)S(1)} %shard_map.135), channel_id=1, source_target_pairs={{24,32},{26,34},{28,36},{30,38},{40,48},{42,50},{44,52},{46,54},{2... | collective-permute-start | bytes 196616 | tf_op jit(solution)/shard_map/ppermute | solution.py:371
  29.8 0.7 copy-start.5
  44.6 15.4 %collective-permute-start.11 = (bf16[128,256]{1,0:T(8,128)(2,1)S(1)}, bf16[128,256]{1,0:T(8,128)(2,1)S(1)}, u32[]{:S(2)}, u32[]{:S(2)}) collective-permute-start(bf16[128,256]{1,0:T(8,128)(2,1)S(1)} %get-tuple-element.58), channel_id=1, source_target_pairs={{0,2},{2,0},{4,6},{6,4},{8,10},{10,8},{12,14},{14,12},{16,18},{18,... | collective-permute-start | bytes 196616 | tf_op jit(solution)/shard_map/ppermute | solution.py:371
  46.9 13.2 %collective-permute-start.12 = (bf16[128,256]{1,0:T(8,128)(2,1)S(1)}, bf16[128,256]{1,0:T(8,128)(2,1)S(1)}, u32[]{:S(2)}, u32[]{:S(2)}) collective-permute-start(bf16[128,256]{1,0:T(8,128)(2,1)S(1)} %get-tuple-element.59), channel_id=1, source_target_pairs={{0,4},{2,6},{4,0},{6,2},{8,12},{10,14},{12,8},{14,10},{16,20},{18,... | collective-permute-start | bytes 196616 | tf_op jit(solution)/shard_map/ppermute | solution.py:371
  56.5 5.2 %collective-permute-start.13 = (bf16[128,256]{1,0:T(8,128)(2,1)S(1)}, bf16[128,256]{1,0:T(8,128)(2,1)S(1)}, u32[]{:S(2)}, u32[]{:S(2)}) collective-permute-start(bf16[128,256]{1,0:T(8,128)(2,1)S(1)} %get-tuple-element.60), channel_id=1, source_target_pairs={{0,6},{2,4},{4,2},{6,0},{8,14},{10,12},{12,10},{14,8},{16,22},{18,... | collective-permute-start | bytes 196616 | tf_op jit(solution)/shard_map/ppermute | solution.py:371
  57.5 4.2 %copy-start.3 = (bf16[1024,2048]{1,0:T(8,128)(2,1)S(1)}, bf16[1024,2048]{1,0:T(8,128)(2,1)}, u32[]{:S(2)}) copy-start(bf16[1024,2048]{1,0:T(8,128)(2,1)} %w_out.3) | copy-start | bytes 12582916
  63.3 7.2 %collective-permute-start.14 = (bf16[192,2048]{1,0:T(8,128)(2,1)S(1)}, bf16[192,2048]{1,0:T(8,128)(2,1)S(1)}, u32[]{:S(2)}, u32[]{:S(2)}) collective-permute-start(bf16[192,2048]{1,0:T(8,128)(2,1)S(1)} %shard_map.138), channel_id=1, source_target_pairs={{0,1},{1,0},{2,3},{3,2},{4,5},{5,4},{6,7},{7,6},{8,9},{9,8},{10,11... | collective-permute-start | bytes 2359304 | tf_op jit(solution)/shard_map/ppermute | solution.py:485

commit v5 on v4

--- a/solution.py
+++ b/solution.py
@@ -34,6 +34,23 @@
         out.append(part)
         x = x - part.astype(F32)
     return out
+
+
+def turned_fours(fours):
+    half, turned = fours // 2, [False] * fours
+    path = [*range(half), *range(half + 1, fours, 2)]
+    for turn, four in enumerate(path):
+        turned[four] = turn % 2 == 1
+        if four >= half - 1 and four + 1 < fours:
+            turned[four + 1] = not turned[four]
+    return turned
+
+
+def own_quarter():
+    place, fours = lax.axis_index("sp"), lax.axis_size("sp") // QUAD
+    mask = sum(1 << four for four, turned in enumerate(turned_fours(fours)) if turned)
+    turned = lax.rem(lax.shift_right_logical(jnp.int32(mask), place // QUAD), 2)
+    return lax.rem(place, QUAD) ^ ((QUAD - 1) * turned)
 
 
 def spread_matrix(heads):
@@ -140,7 +157,7 @@
         added = dot(edge_b[:, group * STATE : (group + 1) * STATE], weighted[:, lanes], ((0,), (0,)))
         packed[0:STATE, lanes] = (state_in[:, lanes] + added).astype(BF16)
     packed[STATE:, :] = logs_in[...]
-    me = lax.rem(lax.axis_index("sp"), QUAD)
+    me = own_quarter()
     quarter = inner // QUAD
     for bits, slot in enumerate((slot0, slot1, slot2, slot3)):
         slot[...] = packed[:, pl.ds(pl.multiple_of((me ^ bits) * quarter, 128), quarter)]
@@ -320,7 +337,7 @@
     half = span // 2
     core = lax.axis_index("tp")
     rows = pl.ds(pl.multiple_of((core if own else 1 - core) * half, 64), half)
-    me = lax.rem(lax.axis_index("sp"), QUAD)
+    me = own_quarter()
     for bits, ref in enumerate((p0, p1, p2, p3)):
         ends[:, pl.ds(pl.multiple_of((me ^ bits) * quarter, 128), quarter)] = ref[...]
     place = lax.broadcasted_iota(jnp.int32, (quarter, quarter), 0) // HEAD_DIM
@@ -433,9 +450,14 @@
     first, sent, total, log = local_call(quad_total_kernel, [slice_of, payload, *kept], quad, [order], limit=SMALL)
     fours = places // QUAD
     half = fours // 2
+    turned = turned_fours(fours)
 
     def up(x, sources, distance):
-        return move(x, [(i, i + distance * QUAD) for four in sources for i in range(four * QUAD, (four + 1) * QUAD)])
+        route = []
+        for four in sources:
+            other = (QUAD - 1) * (turned[four] != turned[four + distance])
+            route += [(four * QUAD + i, (four + distance) * QUAD + (i ^ other)) for i in range(QUAD)]
+        return move(x, route)
 
     def jump(four, before, last=None):
         if last is None:

time: 71.8 us -> 72.3 us (level)
    ppermute x1, starting transfers between devices: 5.29 us -> 8.08 us  [body(): other = lax.ppermute(theirs, 'tp', [(0, 1), (1, 0)])]
    ppermute x14, starting transfers between devices: 25.3 us -> 23 us  [move(): return lax.ppermute(x, 'sp', route)]
where the time goes in v5:
time: 72.3 us; the launch traced here: 72 us
  starting transfers between devices  31.1 us (43%)
  waiting for transfers between devices  26.9 us (37%)
  Pallas kernels  13.4 us (19%)
    ppermute x14, waiting for transfers between devices, move(): return lax.ppermute(x, 'sp', route)  26.6 us
    ppermute x14, starting transfers between devices, move(): return lax.ppermute(x, 'sp', route)  23 us
    ppermute x1, starting transfers between devices, body(): other = lax.ppermute(theirs, 'tp', [(0, 1), (1, 0)])  8.08 us
    pallas_call x13, Pallas kernels, local_call(): pl.pallas_call(kernel, out_shape=outs, in_specs=whole(len(args)), out_spe...  7.86 us
    pallas_call x1, Pallas kernels, body(): pl.pallas_call(local_kernel, out_shape=outs, in_specs=[pl.BlockSpec(memor...  4.73 us
  transfers between devices with their start and end apart: 15, of which 6 were waited for; matrix products, arithmetic and copies ran while one was open for 0% of the time, Pallas kernels for 13%

profile of v5, /device:TPU:1829, one launch (start us, length us, event | category | flops | bytes accessed | tf_op | source)
XLA Modules:
  0.0 72.0 jit_solution(532156928435412312)
XLA Ops:
  0.0 0.8 %tail.1 = bf16[16,1536]{1,0:T(8,128)(2,1)S(1)} custom-call(bf16[384,1024]{1,0:T(8,128)(2,1)} %values.1, bf16[384,256]{1,0:T(8,128)(2,1)} %b_in.1, bf16[384,256]{1,0:T(8,128)(2,1)} %c_in.1), custom_call_target="tpu_custom_call" | custom-call | tf_op jit(solution)/shard_map/tail/pallas_call | solution.py:393
  0.8 2.9 %collective-permute-start = (bf16[16,1536]{1,0:T(8,128)(2,1)S(1)}, bf16[16,1536]{1,0:T(8,128)(2,1)S(1)}, u32[]{:S(2)}, u32[]{:S(2)}) collective-permute-start(bf16[16,1536]{1,0:T(8,128)(2,1)S(1)} %tail.1), channel_id=1, source_target_pairs={{0,2},{2,4},{4,6},{6,8},{8,10},{10,12},{12,14},{14,16},{16,18},{18... | collective-permute-start | bytes 147464 | tf_op jit(solution)/shard_map/ppermute | solution.py:388
  3.7 0.0 copy-start
  3.7 0.0 copy-start.1
  3.7 0.0 copy-start.2
  3.7 4.7 %local.1 = (bf16[384,1024]{1,0:T(8,128)(2,1)S(1)}, bf16[384,256]{1,0:T(8,128)(2,1)S(1)}, bf16[384,256]{1,0:T(8,128)(2,1)S(1)}, f32[16,384]{1,0:T(8,128)S(1)}, f3...) custom-call(bf16[384,1024]{1,0:T(8,128)(2,1)} %values.1, ...), custom_call_target="tpu_custom_call" | custom-call | flops 4000000000 | bytes 4000000 | tf_op jit(solution)/shard_map/local/pallas_call | solution.py:412
  8.5 0.0 copy-start.4
  8.5 0.0 collective-permute-done.halo
  8.5 0.0 copy-done
  8.5 0.3 shard_map.127
  8.9 1.1 %collective-permute-start.1 = (bf16[144,256]{1,0:T(8,128)(2,1)S(1)}, bf16[144,256]{1,0:T(8,128)(2,1)S(1)}, u32[]{:S(2)}, u32[]{:S(2)}) collective-permute-start(bf16[144,256]{1,0:T(8,128)(2,1)S(1)} %get-tuple-element.50), channel_id=1, source_target_pairs={{0,2},{2,0},{4,6},{6,4},{8,10},{10,8},{12,14},{14,12},{16,18},{18,... | collective-permute-start | bytes 221192 | tf_op jit(solution)/shard_map/ppermute | solution.py:388
  9.9 0.8 %collective-permute-start.2 = (bf16[144,256]{1,0:T(8,128)(2,1)S(1)}, bf16[144,256]{1,0:T(8,128)(2,1)S(1)}, u32[]{:S(2)}, u32[]{:S(2)}) collective-permute-start(bf16[144,256]{1,0:T(8,128)(2,1)S(1)} %get-tuple-element.51), channel_id=1, source_target_pairs={{0,4},{2,6},{4,0},{6,2},{8,12},{10,14},{12,8},{14,10},{16,20},{18,... | collective-permute-start | bytes 221192 | tf_op jit(solution)/shard_map/ppermute | solution.py:388
  10.8 1.8 %collective-permute-start.3 = (bf16[144,256]{1,0:T(8,128)(2,1)S(1)}, bf16[144,256]{1,0:T(8,128)(2,1)S(1)}, u32[]{:S(2)}, u32[]{:S(2)}) collective-permute-start(bf16[144,256]{1,0:T(8,128)(2,1)S(1)} %get-tuple-element.52), channel_id=1, source_target_pairs={{0,6},{2,4},{4,2},{6,0},{8,14},{10,12},{12,10},{14,8},{16,22},{18,... | collective-permute-start | bytes 221192 | tf_op jit(solution)/shard_map/ppermute | solution.py:388
  12.6 0.0 collective-permute-done.1.r1.refs_9_
  12.6 2.3 %collective-permute-done.2.r2.refs_10_ = bf16[144,256]{1,0:T(8,128)(2,1)S(1)} collective-permute-done((bf16[144,256]{1,0:T(8,128)(2,1)S(1)}, bf16[144,256]{1,0:T(8,128)(2,1)S(1)}, u32[]{:S(2)}, u32[]{:S(2)}) %collective-permute-start.2) | collective-permute-done | bytes 73760 | tf_op jit(solution)/shard_map/ppermute | solution.py:388
  14.8 1.7 %collective-permute-done.3.r3.refs_11_ = bf16[144,256]{1,0:T(8,128)(2,1)S(1)} collective-permute-done((bf16[144,256]{1,0:T(8,128)(2,1)S(1)}, bf16[144,256]{1,0:T(8,128)(2,1)S(1)}, u32[]{:S(2)}, u32[]{:S(2)}) %collective-permute-start.3) | collective-permute-done | bytes 73760 | tf_op jit(solution)/shard_map/ppermute | solution.py:388
  16.5 0.1 shard_map.130
  16.7 0.7 collective-permute-start.4
  17.3 0.0 collective-permute-done.4.refs_0_
  17.4 0.7 collective-permute-start.5
  18.0 0.0 collective-permute-done.5.refs_0_.refs_1_
  18.1 0.7 collective-permute-start.6
  18.8 1.3 %collective-permute-start.8 = (bf16[144,256]{1,0:T(8,128)(2,1)S(1)}, bf16[144,256]{1,0:T(8,128)(2,1)S(1)}, u32[]{:S(2)}, u32[]{:S(2)}) collective-permute-start(bf16[144,256]{1,0:T(8,128)(2,1)S(1)} %get-tuple-element.56), channel_id=1, source_target_pairs={{32,40},{34,42},{36,44},{38,46},{48,56},{50,58},{52,60},{54,62},{3... | collective-permute-start | bytes 221192 | tf_op jit(solution)/shard_map/ppermute | solution.py:388
  20.1 0.0 collective-permute-done.6.refs_0_.refs_2_
  20.1 0.7 collective-permute-start.7
  20.8 7.0 %collective-permute-done.8.last.refs_7_ = bf16[144,256]{1,0:T(8,128)(2,1)S(1)} collective-permute-done((bf16[144,256]{1,0:T(8,128)(2,1)S(1)}, bf16[144,256]{1,0:T(8,128)(2,1)S(1)}, u32[]{:S(2)}, u32[]{:S(2)}) %collective-permute-start.8) | collective-permute-done | bytes 73760 | tf_op jit(solution)/shard_map/ppermute | solution.py:388
  27.8 0.0 collective-permute-done.7.before.refs_3_
  27.8 1.3 %collective-permute-start.9 = (bf16[128,256]{1,0:T(8,128)(2,1)S(1)}, bf16[128,256]{1,0:T(8,128)(2,1)S(1)}, u32[]{:S(2)}, u32[]{:S(2)}) collective-permute-start(bf16[128,256]{1,0:T(8,128)(2,1)S(1)} %shard_map.134.refs_1_), channel_id=1, source_target_pairs={{40,62},{42,60},{44,58},{46,56},{41,63},{43,61},{45,59},{47,57},{1... | collective-permute-start | bytes 196616 | tf_op jit(solution)/shard_map/ppermute | solution.py:388
  29.1 0.7 collective-permute-start.10
  29.8 0.0 copy-done.4
  29.8 0.0 copy-start.5
  29.8 0.4 shard_map.128
  30.3 0.2 copy-done.5
  30.5 0.0 collective-permute-done.10.refs_5_.refs_6_
  30.5 15.1 %collective-permute-done.9.refs_4_ = bf16[128,256]{1,0:T(8,128)(2,1)S(1)} collective-permute-done((bf16[128,256]{1,0:T(8,128)(2,1)S(1)}, bf16[128,256]{1,0:T(8,128)(2,1)S(1)}, u32[]{:S(2)}, u32[]{:S(2)}) %collective-permute-start.9) | collective-permute-done | bytes 65568 | tf_op jit(solution)/shard_map/ppermute | solution.py:388
  45.6 0.2 shard_map.136
  45.7 8.3 %collective-permute-start.11 = (bf16[128,256]{1,0:T(8,128)(2,1)S(1)}, bf16[128,256]{1,0:T(8,128)(2,1)S(1)}, u32[]{:S(2)}, u32[]{:S(2)}) collective-permute-start(bf16[128,256]{1,0:T(8,128)(2,1)S(1)} %get-tuple-element.58), channel_id=1, source_target_pairs={{0,2},{2,0},{4,6},{6,4},{8,10},{10,8},{12,14},{14,12},{16,18},{18,... | collective-permute-start | bytes 196616 | tf_op jit(solution)/shard_map/ppermute | solution.py:388
  54.1 0.0 collective-permute-start.12
  54.1 2.2 %collective-permute-start.13 = (bf16[128,256]{1,0:T(8,128)(2,1)S(1)}, bf16[128,256]{1,0:T(8,128)(2,1)S(1)}, u32[]{:S(2)}, u32[]{:S(2)}) collective-permute-start(bf16[128,256]{1,0:T(8,128)(2,1)S(1)} %get-tuple-element.60), channel_id=1, source_target_pairs={{0,6},{2,4},{4,2},{6,0},{8,14},{10,12},{12,10},{14,8},{16,22},{18,... | collective-permute-start | bytes 196616 | tf_op jit(solution)/shard_map/ppermute | solution.py:388
  56.3 2.6 %shard_map.129 = (f32[384,1024]{1,0:T(8,128)S(1)}, bf16[384,256]{1,0:T(8,128)(2,1)S(1)}) custom-call(bf16[384,1024]{1,0:T(8,128)(2,1)S(1)} %get-tuple-element.33.x_act, bf16[384,256]{1,0:T(8,128)(2,1)S(1)} %get-tuple-element.34.b_act, bf16[384,256]{1,0:T(8,128)(2,1)S(1)} %get-tuple-element.35.c_act, bf16[16,1024]{1,0:T(8,128)(2,1)S(1)} %get-tuple-element.40.edge_x, ...), custom_call_target="tpu_custom_call" | custom-call | flops 4000000000 | bytes 2850816 | tf_op jit(solution)/shard_map/pallas_call | solution.py:173
  58.9 0.0 collective-permute-done.11.p1
  58.9 0.5 collective-permute-done.12.p2
  59.4 0.0 collective-permute-done.13.p3
  59.4 1.6 %shard_map.138 = bf16[192,2048]{1,0:T(8,128)(2,1)S(1)} custom-call(f32[384,1024]{1,0:T(8,128)S(1)} %get-tuple-element.46.y_in, f32[384,1024]{1,0:T(8,128)S(1)} %get-tuple-element.47.grow, bf16[384,256]{1,0:T(8,128)(2,1)S(1)} %get-tuple-element.48.c_all, bf16[1,1024]{1,0:T(2,128)(2,1)S(1)} %reshape.12.gain, bf16[128,256]{1,0:T(8,128)(2,1)S(1)} %get-tuple-element.57.p0, ...), custom_call_target="tpu_custom_call" | custom-call | flops 4000000000 | bytes 7800832 | tf_op jit(solution)/shard_map/pallas_call | solution.py:173
  61.0 8.1 %collective-permute-start.14 = (bf16[192,2048]{1,0:T(8,128)(2,1)S(1)}, bf16[192,2048]{1,0:T(8,128)(2,1)S(1)}, u32[]{:S(2)}, u32[]{:S(2)}) collective-permute-start(bf16[192,2048]{1,0:T(8,128)(2,1)S(1)} %shard_map.138), channel_id=1, source_target_pairs={{0,1},{1,0},{2,3},{3,2},{4,5},{5,4},{6,7},{7,6},{8,9},{9,8},{10,11... | collective-permute-start | bytes 2359304 | tf_op jit(solution)/shard_map/ppermute | solution.py:507
  69.1 1.6 %shard_map.137.own = f32[192,2048]{1,0:T(8,128)S(1)} custom-call(f32[384,1024]{1,0:T(8,128)S(1)} %get-tuple-element.46.y_in, f32[384,1024]{1,0:T(8,128)S(1)} %get-tuple-element.47.grow, bf16[384,256]{1,0:T(8,128)(2,1)S(1)} %get-tuple-element.48.c_all, bf16[1,1024]{1,0:T(2,128)(2,1)S(1)} %reshape.12.gain, bf16[128,256]{1,0:T(8,128)(2,1)S(1)} %get-tuple-element.57.p0, ...), custom_call_target="tpu_custom_call" | custom-call | flops 4000000000 | bytes 7800832 | tf_op jit(solution)/shard_map/pallas_call | solution.py:173
  70.7 0.3 collective-permute-done.14.other
  71.0 1.0 %shard_map.139 = bf16[192,2048]{1,0:T(8,128)(2,1)} custom-call(f32[192,2048]{1,0:T(8,128)S(1)} %shard_map.137.own, bf16[192,2048]{1,0:T(8,128)(2,1)S(1)} %collective-permute-done.14.other), custom_call_target="tpu_custom_call" | custom-call | bytes 2359296 | tf_op jit(solution)/shard_map/pallas_call | solution.py:173
  (10 shorter events, 0.1 us)
Async XLA Ops:
  0.8 7.7 %collective-permute-start = (bf16[16,1536]{1,0:T(8,128)(2,1)S(1)}, bf16[16,1536]{1,0:T(8,128)(2,1)S(1)}, u32[]{:S(2)}, u32[]{:S(2)}) collective-permute-start(bf16[16,1536]{1,0:T(8,128)(2,1)S(1)} %tail.1), channel_id=1, source_target_pairs={{0,2},{2,4},{4,6},{6,8},{8,10},{10,12},{12,14},{14,16},{16,18},{18... | collective-permute-start | bytes 147464 | tf_op jit(solution)/shard_map/ppermute | solution.py:388
  3.7 4.8 %copy-start = (bf16[4,1024]{1,0:T(4,128)(2,1)S(1)}, bf16[4,1024]{1,0:T(4,128)(2,1)}, u32[]{:S(2)}) copy-start(bf16[4,1024]{1,0:T(4,128)(2,1)} %conv_x.1) | copy-start | bytes 24580
  3.7 4.8 %copy-start.1 = (bf16[4,256]{1,0:T(4,128)(2,1)S(1)}, bf16[4,256]{1,0:T(4,128)(2,1)}, u32[]{:S(2)}) copy-start(bf16[4,256]{1,0:T(4,128)(2,1)} %conv_b.1) | copy-start | bytes 6148
  3.7 4.8 %copy-start.2 = (bf16[4,256]{1,0:T(4,128)(2,1)S(1)}, bf16[4,256]{1,0:T(4,128)(2,1)}, u32[]{:S(2)}) copy-start(bf16[4,256]{1,0:T(4,128)(2,1)} %conv_c.1) | copy-start | bytes 6148
  8.5 21.3 %copy-start.4 = (bf16[384,1024]{1,0:T(8,128)(2,1)S(1)}, bf16[384,1024]{1,0:T(8,128)(2,1)}, u32[]{:S(2)}) copy-start(bf16[384,1024]{1,0:T(8,128)(2,1)} %gate.1) | copy-start | bytes 2359300
  8.9 3.7 %collective-permute-start.1 = (bf16[144,256]{1,0:T(8,128)(2,1)S(1)}, bf16[144,256]{1,0:T(8,128)(2,1)S(1)}, u32[]{:S(2)}, u32[]{:S(2)}) collective-permute-start(bf16[144,256]{1,0:T(8,128)(2,1)S(1)} %get-tuple-element.50), channel_id=1, source_target_pairs={{0,2},{2,0},{4,6},{6,4},{8,10},{10,8},{12,14},{14,12},{16,18},{18,... | collective-permute-start | bytes 221192 | tf_op jit(solution)/shard_map/ppermute | solution.py:388
  9.9 4.9 %collective-permute-start.2 = (bf16[144,256]{1,0:T(8,128)(2,1)S(1)}, bf16[144,256]{1,0:T(8,128)(2,1)S(1)}, u32[]{:S(2)}, u32[]{:S(2)}) collective-permute-start(bf16[144,256]{1,0:T(8,128)(2,1)S(1)} %get-tuple-element.51), channel_id=1, source_target_pairs={{0,4},{2,6},{4,0},{6,2},{8,12},{10,14},{12,8},{14,10},{16,20},{18,... | collective-permute-start | bytes 221192 | tf_op jit(solution)/shard_map/ppermute | solution.py:388
  10.8 5.8 %collective-permute-start.3 = (bf16[144,256]{1,0:T(8,128)(2,1)S(1)}, bf16[144,256]{1,0:T(8,128)(2,1)S(1)}, u32[]{:S(2)}, u32[]{:S(2)}) collective-permute-start(bf16[144,256]{1,0:T(8,128)(2,1)S(1)} %get-tuple-element.52), channel_id=1, source_target_pairs={{0,6},{2,4},{4,2},{6,0},{8,14},{10,12},{12,10},{14,8},{16,22},{18,... | collective-permute-start | bytes 221192 | tf_op jit(solution)/shard_map/ppermute | solution.py:388
  16.7 0.7 collective-permute-start.4
  17.4 0.7 collective-permute-start.5
  18.1 2.0 %collective-permute-start.6 = (bf16[128,256]{1,0:T(8,128)(2,1)S(1)}, bf16[128,256]{1,0:T(8,128)(2,1)S(1)}, u32[]{:S(2)}, u32[]{:S(2)}) collective-permute-start(bf16[128,256]{1,0:T(8,128)(2,1)S(1)} %shard_map.132), channel_id=1, source_target_pairs={{16,30},{18,28},{20,26},{22,24},{17,31},{19,29},{21,27},{23,25},{8... | collective-permute-start | bytes 196616 | tf_op jit(solution)/shard_map/ppermute | solution.py:388
  18.8 9.0 %collective-permute-start.8 = (bf16[144,256]{1,0:T(8,128)(2,1)S(1)}, bf16[144,256]{1,0:T(8,128)(2,1)S(1)}, u32[]{:S(2)}, u32[]{:S(2)}) collective-permute-start(bf16[144,256]{1,0:T(8,128)(2,1)S(1)} %get-tuple-element.56), channel_id=1, source_target_pairs={{32,40},{34,42},{36,44},{38,46},{48,56},{50,58},{52,60},{54,62},{3... | collective-permute-start | bytes 221192 | tf_op jit(solution)/shard_map/ppermute | solution.py:388
  20.1 7.7 %collective-permute-start.7 = (bf16[128,256]{1,0:T(8,128)(2,1)S(1)}, bf16[128,256]{1,0:T(8,128)(2,1)S(1)}, u32[]{:S(2)}, u32[]{:S(2)}) collective-permute-start(bf16[128,256]{1,0:T(8,128)(2,1)S(1)} %shard_map.133.refs_0_), channel_id=1, source_target_pairs={{24,46},{26,44},{28,42},{30,40},{25,47},{27,45},{29,43},{31,41},{8... | collective-permute-start | bytes 196616 | tf_op jit(solution)/shard_map/ppermute | solution.py:388
  27.8 17.7 %collective-permute-start.9 = (bf16[128,256]{1,0:T(8,128)(2,1)S(1)}, bf16[128,256]{1,0:T(8,128)(2,1)S(1)}, u32[]{:S(2)}, u32[]{:S(2)}) collective-permute-start(bf16[128,256]{1,0:T(8,128)(2,1)S(1)} %shard_map.134.refs_1_), channel_id=1, source_target_pairs={{40,62},{42,60},{44,58},{46,56},{41,63},{43,61},{45,59},{47,57},{1... | collective-permute-start | bytes 196616 | tf_op jit(solution)/shard_map/ppermute | solution.py:388
  29.1 1.4 %collective-permute-start.10 = (bf16[128,256]{1,0:T(8,128)(2,1)S(1)}, bf16[128,256]{1,0:T(8,128)(2,1)S(1)}, u32[]{:S(2)}, u32[]{:S(2)}) collective-permute-start(bf16[128,256]{1,0:T(8,128)(2,1)S(1)} %shard_map.135), channel_id=1, source_target_pairs={{24,38},{26,36},{28,34},{30,32},{40,54},{42,52},{44,50},{46,48},{2... | collective-permute-start | bytes 196616 | tf_op jit(solution)/shard_map/ppermute | solution.py:388
  29.8 0.7 copy-start.5
  45.7 13.1 %collective-permute-start.11 = (bf16[128,256]{1,0:T(8,128)(2,1)S(1)}, bf16[128,256]{1,0:T(8,128)(2,1)S(1)}, u32[]{:S(2)}, u32[]{:S(2)}) collective-permute-start(bf16[128,256]{1,0:T(8,128)(2,1)S(1)} %get-tuple-element.58), channel_id=1, source_target_pairs={{0,2},{2,0},{4,6},{6,4},{8,10},{10,8},{12,14},{14,12},{16,18},{18,... | collective-permute-start | bytes 196616 | tf_op jit(solution)/shard_map/ppermute | solution.py:388
  54.1 5.3 %collective-permute-start.12 = (bf16[128,256]{1,0:T(8,128)(2,1)S(1)}, bf16[128,256]{1,0:T(8,128)(2,1)S(1)}, u32[]{:S(2)}, u32[]{:S(2)}) collective-permute-start(bf16[128,256]{1,0:T(8,128)(2,1)S(1)} %get-tuple-element.59), channel_id=1, source_target_pairs={{0,4},{2,6},{4,0},{6,2},{8,12},{10,14},{12,8},{14,10},{16,20},{18,... | collective-permute-start | bytes 196616 | tf_op jit(solution)/shard_map/ppermute | solution.py:388
  54.1 5.3 %collective-permute-start.13 = (bf16[128,256]{1,0:T(8,128)(2,1)S(1)}, bf16[128,256]{1,0:T(8,128)(2,1)S(1)}, u32[]{:S(2)}, u32[]{:S(2)}) collective-permute-start(bf16[128,256]{1,0:T(8,128)(2,1)S(1)} %get-tuple-element.60), channel_id=1, source_target_pairs={{0,6},{2,4},{4,2},{6,0},{8,14},{10,12},{12,10},{14,8},{16,22},{18,... | collective-permute-start | bytes 196616 | tf_op jit(solution)/shard_map/ppermute | solution.py:388
  56.3 3.1 %copy-start.3 = (bf16[1024,2048]{1,0:T(8,128)(2,1)S(1)}, bf16[1024,2048]{1,0:T(8,128)(2,1)}, u32[]{:S(2)}) copy-start(bf16[1024,2048]{1,0:T(8,128)(2,1)} %w_out.3) | copy-start | bytes 12582916
  61.0 10.0 %collective-permute-start.14 = (bf16[192,2048]{1,0:T(8,128)(2,1)S(1)}, bf16[192,2048]{1,0:T(8,128)(2,1)S(1)}, u32[]{:S(2)}, u32[]{:S(2)}) collective-permute-start(bf16[192,2048]{1,0:T(8,128)(2,1)S(1)} %shard_map.138), channel_id=1, source_target_pairs={{0,1},{1,0},{2,3},{3,2},{4,5},{5,4},{6,7},{7,6},{8,9},{9,8},{10,11... | collective-permute-start | bytes 2359304 | tf_op jit(solution)/shard_map/ppermute | solution.py:507
